TPU v7x, 32 devices: a whole 2x2x4 slice. The times are simulated.
32 devices in a mesh: fs: 16 (over z, y, x), tp: 2 (over core).
Axes of the slice: x: 2, y: 2, z: 4, core: 2. Of those that a mesh axis runs over, the one named last changes fastest.
Arguments:
- tokens: bfloat16 [2048, 2048], P('fs'), may hold values from -6 to 6
- norm_gain: float32 [2048], replicated, may hold values from 0.1 to 1.9
- w_query: bfloat16 [2048, 1024], P('fs', 'tp'), may hold values from -0.125 to 0.125
- w_key: bfloat16 [2048, 1024], P('fs', 'tp'), may hold values from -0.125 to 0.125
- w_value: bfloat16 [2048, 2048], P('fs', 'tp'), may hold values from -0.125 to 0.125
- w_gate: bfloat16 [2048, 2048], P('fs', 'tp'), may hold values from -0.125 to 0.125
- mixer_gain: float32 [2048], P('tp'), may hold values from 0.1 to 1.9
- w_out: bfloat16 [2048, 2048], P('tp', 'fs'), may hold values from -0.125 to 0.125
- channel_gain: float32 [2048], replicated, may hold values from 0.1 to 1.9
- w_left: bfloat16 [2048, 3072], P('fs', 'tp'), may hold values from -0.125 to 0.125
- w_right: bfloat16 [2048, 3072], P('fs', 'tp'), may hold values from -0.125 to 0.125
- taps_left: float32 [3, 3072], P(None, 'tp'), may hold values from -3.5 to 3.5
- taps_right: float32 [3, 3072], P(None, 'tp'), may hold values from -3.5 to 3.5
- w_down: bfloat16 [3072, 2048], P('tp', 'fs'), may hold values from -0.109375 to 0.109375
Outputs:
- layer_out: bfloat16 [2048, 2048], P('fs')
All inputs are finite; a program needn't handle non-finite values.
Results may differ from a plain program's by a relative error of at most 0.018.
Values may be sent and summed in bfloat16 or wider, within the bound.
A program may use at most 64 MiB of HBM per device.

v0:
```python
import functools

import jax
import jax.numpy as jnp
import numpy as np
from jax import lax
from jax.experimental import pallas as pl
from jax.experimental.pallas import tpu as pltpu
from jax.sharding import PartitionSpec as P

DK = 128
DV = 256
BLOCK = 128
MESH = pl.DeviceIdType.MESH


highest = lax.Precision.HIGHEST


def scale_rows(rows_in, gain_vec):
    floats = rows_in.astype(jnp.float32)
    factor = lax.rsqrt(jnp.mean(floats * floats, axis=-1, keepdims=True) + 1e-06)
    return (floats * factor * gain_vec).astype(jnp.bfloat16)


def decays(first_head, count):
    head_ids = first_head + jnp.arange(count, dtype=jnp.float32)
    return jnp.log(1.0 - 2.0 ** (-5.0 - head_ids))


def rotate(heads_in, positions):
    width = heads_in.shape[-1]
    half = width // 2
    freqs = 10000.0 ** (-jnp.arange(half, dtype=jnp.float32) / half)
    angles = positions[:, None] * freqs[None, :]
    cosine = jnp.cos(angles)
    sine = jnp.sin(angles)
    first_half = heads_in[..., :half]
    second_half = heads_in[..., half:]
    return jnp.concatenate(
        [first_half * cosine - second_half * sine, first_half * sine + second_half * cosine],
        axis=-1,
    )


def retention(queries, keys_in, values_in, log_gamma):
    head_count, length, key_width = queries.shape
    value_width = values_in.shape[-1]
    blocks = length // BLOCK
    queries = queries.reshape(head_count, blocks, BLOCK, key_width)
    keys_in = keys_in.reshape(head_count, blocks, BLOCK, key_width)
    values_in = values_in.reshape(head_count, blocks, BLOCK, value_width)
    offsets = jnp.arange(BLOCK, dtype=jnp.float32)
    distance = offsets[:, None] - offsets[None, :]
    weights = jnp.where(
        distance >= 0, jnp.exp(log_gamma[:, None, None] * jnp.maximum(distance, 0.0)), 0.0
    )
    scores = jnp.einsum("hbnd,hbmd->hbnm", queries, keys_in, precision=highest) * weights[:, None]
    inner = jnp.einsum("hbnm,hbme->hbne", scores, values_in, precision=highest)
    key_weight = jnp.exp(log_gamma[:, None] * (BLOCK - 1 - offsets)[None, :])
    contrib = jnp.einsum(
        "hbjd,hbje->hbde", keys_in * key_weight[:, None, :, None], values_in, precision=highest
    )
    block_decay = jnp.exp(log_gamma * BLOCK)[:, None, None]

    def advance(state, contrib_block):
        return (state * block_decay + contrib_block, state)

    _, states = lax.scan(
        advance,
        jnp.zeros((head_count, key_width, value_width), jnp.float32),
        jnp.moveaxis(contrib, 1, 0),
    )
    states = jnp.moveaxis(states, 0, 1)
    query_weight = jnp.exp(log_gamma[:, None] * (offsets + 1.0)[None, :])
    carried = (
        jnp.einsum("hbnd,hbde->hbne", queries, states, precision=highest)
        * query_weight[:, None, :, None]
    )
    return (inner + carried).reshape(head_count, length, value_width)


def head_norm(retained):
    return retained * lax.rsqrt(jnp.mean(retained * retained, axis=-1, keepdims=True) + 1e-06)


def causal_taps(values_in, taps):
    length = values_in.shape[-2]
    padded = jnp.pad(values_in.astype(jnp.float32), ((taps.shape[0] - 1, 0), (0, 0)))
    result = padded[0:length] * taps[0]
    for tap_index in range(1, taps.shape[0]):
        result = result + padded[tap_index : tap_index + length] * taps[tap_index]
    return result


def fold_single(source, weight_piece):
    return jnp.dot(source, weight_piece, preferred_element_type=jnp.float32)


def collect_single(source, weight):
    return fold_single(source, lax.all_gather(weight, "fs", axis=0, tiled=True))


def plain_body(
    tokens,
    norm_gain,
    w_query,
    w_key,
    w_value,
    w_gate,
    mixer_gain,
    w_out,
    channel_gain,
    w_left,
    w_right,
    taps_left,
    taps_right,
    w_down,
):
    length = tokens.shape[0]
    normed = scale_rows(tokens, norm_gain)
    queries = collect_single(normed, w_query)
    keys_proj = collect_single(normed, w_key)
    values_proj = collect_single(normed, w_value)
    gates = collect_single(normed, w_gate)
    queries = queries.astype(jnp.bfloat16)
    keys_proj = keys_proj.astype(jnp.bfloat16)
    values_proj = values_proj.astype(jnp.bfloat16)
    gates = gates.astype(jnp.bfloat16)
    heads_here = w_query.shape[1] // DK
    first_head = (lax.axis_index("tp") * heads_here).astype(jnp.float32)
    log_gamma = decays(first_head, heads_here)
    positions = jnp.arange(length, dtype=jnp.float32)

    def split_heads(rows_in, width):
        return rows_in.astype(jnp.float32).reshape(length, heads_here, width).transpose(1, 0, 2)

    retained = head_norm(
        retention(
            rotate(split_heads(queries, DK), positions),
            rotate(split_heads(keys_proj, DK), positions),
            split_heads(values_proj, DV),
            log_gamma,
        )
    )
    retained = retained.transpose(1, 0, 2).reshape(length, heads_here * DV)
    hidden = (retained * mixer_gain * jax.nn.silu(gates.astype(jnp.float32))).astype(jnp.bfloat16)
    rows_own = length // lax.axis_size("tp")
    first_row = lax.axis_index("tp") * rows_own
    out_whole = lax.all_gather(w_out, "fs", axis=1, tiled=True)
    mixer_total = lax.psum_scatter(
        jnp.dot(hidden, out_whole, preferred_element_type=jnp.float32).astype(jnp.bfloat16),
        "tp",
        scatter_dimension=0,
        tiled=True,
    ).astype(jnp.float32)
    residual = lax.dynamic_slice_in_dim(tokens, first_row, rows_own, 0)
    middle_own = (residual.astype(jnp.float32) + mixer_total).astype(jnp.bfloat16)
    middle = lax.all_gather(middle_own, "tp", axis=0, tiled=True)
    normed_mid = scale_rows(middle, channel_gain)
    left = collect_single(normed_mid, w_left)
    right = collect_single(normed_mid, w_right)
    left = left.astype(jnp.bfloat16)
    right = right.astype(jnp.bfloat16)
    gated = (jax.nn.silu(causal_taps(left, taps_left)) * causal_taps(right, taps_right)).astype(
        jnp.bfloat16
    )
    down_whole = lax.all_gather(w_down, "fs", axis=1, tiled=True)
    channel_part = jnp.dot(gated, down_whole, preferred_element_type=jnp.float32)
    channel_total = lax.psum(channel_part.astype(jnp.bfloat16), "tp").astype(jnp.float32)
    return (middle.astype(jnp.float32) + channel_total).astype(jnp.bfloat16)


def log_gammas(head_count):
    table = np.log(1.0 - 2.0 ** (-5.0 - np.arange(head_count, dtype=np.float64)))
    return np.repeat(table[:, None], BLOCK, axis=1).astype(np.float32)


def turning(length, width):
    half = width // 2
    freqs = np.float32(10000.0) ** (-np.arange(half, dtype=np.float32) / np.float32(half))
    angles = (np.arange(length, dtype=np.float32)[:, None] * freqs[None, :]).astype(np.float64)
    cosine, sine = np.cos(angles), np.sin(angles)
    return (
        np.concatenate([cosine, cosine], axis=1).astype(np.float32),
        np.concatenate([-sine, sine], axis=1).astype(np.float32),
    )


def silu(v):
    return v / (1.0 + jnp.exp(-v))


def normed_rows(floats, gain):
    factor = lax.rsqrt(jnp.mean(floats * floats, axis=-1, keepdims=True) + 1e-06)
    return (floats * factor * gain).astype(jnp.bfloat16)


def layer_kernel(
    n_fs,
    groups,
    tokens,
    norm_gain,
    wq,
    wk,
    wv,
    wg,
    mixer_gain,
    wo,
    channel_gain,
    wl,
    wr,
    taps_left,
    taps_right,
    wd,
    cos_t,
    sin_t,
    gammas,
    out,
    w1,
    wout,
    wlr,
    wdown,
    nt,
    nm,
    qkvg,
    hid,
    gated,
    part1,
    part2,
    xb1,
    xb2,
    sb1,
    sb2,
    rb1,
    rb2,
    mid,
    acc,
    both,
    fin,
    fin_in,
    s1_send,
    s1_recv,
    self_sem,
    s2_send,
    s2_recv,
    a_send,
    a_recv,
    f_send,
    f_recv,
    x_send,
    x_recv,
    r_send,
    r_recv,
    o_send,
    o_recv,
):
    fs, tp = lax.axis_index("fs"), lax.axis_index("tp")
    planes = n_fs // groups
    z, q = fs // planes, lax.rem(fs, planes)
    other = 1 - tp
    length, width = tokens.shape
    own = length // 2
    few = own // 2
    later = range(1, groups)
    everyone = range(groups)
    kb = wq.shape[0]
    nb = wo.shape[1]
    cq, cv, cf = wq.shape[1] // groups, wv.shape[1] // groups, wl.shape[1] // groups

    def zpeer(step):
        return lax.rem(z + step, groups)

    def zback(step):
        return lax.rem(z + groups - step, groups)

    def zdev(target):
        return {"fs": target * planes + q, "tp": tp}

    partner = {"fs": fs, "tp": other}

    def lanes(index, size):
        return pl.ds(pl.multiple_of(index * size, 128), size)

    def rows(index, size):
        return pl.ds(pl.multiple_of(index * size, size), size)

    def region(cls, f):
        if cls == 0:
            return w1.at[rows(f, kb), :]
        if cls == 1:
            return wout.at[:, lanes(f, nb)]
        if cls == 2:
            return wlr.at[rows(f, kb), :]
        return wdown.at[:, lanes(f, nb)]

    pieces = (
        (0, lambda c: wq.at[:, lanes(c, cq)], lambda f: w1.at[rows(f, kb), pl.ds(0, cq)]),
        (0, lambda c: wk.at[:, lanes(c, cq)], lambda f: w1.at[rows(f, kb), pl.ds(cq, cq)]),
        (0, lambda c: wv.at[:, lanes(c, cv)], lambda f: w1.at[rows(f, kb), pl.ds(2 * cq, cv)]),
        (0, lambda c: wg.at[:, lanes(c, cv)], lambda f: w1.at[rows(f, kb), pl.ds(2 * cq + cv, cv)]),
        (1, lambda c: wo.at[rows(c, cv), :], lambda f: wout.at[:, lanes(f, nb)]),
        (2, lambda c: wl.at[:, lanes(c, cf)], lambda f: wlr.at[rows(f, kb), pl.ds(0, cf)]),
        (2, lambda c: wr.at[:, lanes(c, cf)], lambda f: wlr.at[rows(f, kb), pl.ds(cf, cf)]),
        (3, lambda c: wd.at[rows(c, cf), :], lambda f: wdown.at[:, lanes(f, nb)]),
    )

    barrier = pltpu.get_barrier_semaphore()
    for step in range(1, groups):
        pl.semaphore_signal(barrier, inc=1, device_id=zdev(zpeer(step)), device_id_type=MESH)
    qx = q + 1 - 2 * lax.rem(q, 2)
    qy = q + 2 - 4 * (q // 2)
    to_x = {"fs": z * planes + qx, "tp": tp}
    to_y = {"fs": z * planes + qy, "tp": tp}
    for device in (to_x, to_y):
        pl.semaphore_signal(barrier, inc=1, device_id=device, device_id_type=MESH)
    pl.semaphore_signal(barrier, inc=1, device_id=partner, device_id_type=MESH)

    keeps = []
    for i, (cls, src, dst) in enumerate(pieces):
        keep = pltpu.make_async_copy(src(z), dst(fs), self_sem.at[i])
        keep.start()
        keeps.append(keep)

    def own_rows(seq, half):
        return pl.ds(pl.multiple_of(seq * length + half * own, own), own)

    my_half = pl.ds(pl.multiple_of(tp * own, own), own)
    nt[own_rows(z, tp), :] = normed_rows(tokens[my_half, :].astype(jnp.float32), norm_gain[...])
    pl.semaphore_wait(barrier, groups - 1 + 2 + 1)

    def remote(src, dst, ssem, rsem, device):
        return pltpu.make_async_remote_copy(
            src_ref=src, dst_ref=dst, send_sem=ssem, recv_sem=rsem,
            device_id=device, device_id_type=MESH,
        )

    pending = []

    def go(copy):
        copy.start()
        pending.append(copy)

    def spread(buf, which, place):
        mine = buf.at[place(z, tp), :]
        for step in later:
            go(remote(mine, mine, a_send.at[which, step], a_recv.at[which, step], zdev(zpeer(step))))
        go(remote(mine, mine, f_send.at[which, 0], f_recv.at[which, 0], partner))

    def pass_on(buf, which, place):
        for step in later:
            got = buf.at[place(zback(step), tp), :]
            remote(got, got, a_send.at[which, step], a_recv.at[which, step], zdev(zpeer(step))).wait_recv()
            go(remote(got, got, f_send.at[which, step], f_recv.at[which, step], partner))

    def await_pass(buf, which, place):
        for step in everyone:
            got = buf.at[place(zback(step), other), :]
            remote(got, got, f_send.at[which, step], f_recv.at[which, step], partner).wait_recv()

    def in_half(half):
        def place(seq, core):
            return pl.ds(pl.multiple_of(half * groups * own + seq * own + core * few, few), few)
        return place

    def first_leg(cls):
        for step in range(1, groups):
            for i, (c, src, dst) in enumerate(pieces):
                if c == cls:
                    target = zpeer(step)
                    go(remote(src(target), dst(fs), s1_send.at[i, step], s1_recv.at[i, step], zdev(target)))

    def half_of(cls, f, half):
        block = region(cls, f)
        size = (kb, cv, kb, cf)[cls] // 2
        return block.at[pl.ds(half * size, size), :]

    hops = ((0, to_x), (1, to_y), (1, to_x), (0, to_y))

    def hop_copy(cls, step, from_q, half, slot, device):
        ref = half_of(cls, zback(step) * planes + from_q, half)
        return remote(ref, ref, s2_send.at[cls, step, slot], s2_recv.at[cls, step, slot], device)

    def direct(cls, step):
        f = zback(step) * planes + q
        for i, (c, src, dst) in enumerate(pieces):
            if c == cls:
                if step == 0:
                    keeps[i].wait()
                else:
                    remote(src(z), dst(f), s1_send.at[i, step], s1_recv.at[i, step], zdev(zpeer(step))).wait_recv()
        for slot, (half, device) in enumerate(hops):
            go(hop_copy(cls, step, q, half, slot, device))

    def relay(cls, step):
        hop_copy(cls, step, qx, 0, 0, to_x).wait_recv()
        go(hop_copy(cls, step, qx, 0, 4, to_y))
        hop_copy(cls, step, qy, 1, 1, to_y).wait_recv()
        go(hop_copy(cls, step, qy, 1, 5, to_x))

    def await_leg(cls):
        diagonal = planes - 1 - q
        for step in range(groups):
            hop_copy(cls, step, qx, 1, 2, to_x).wait_recv()
            hop_copy(cls, step, qy, 0, 3, to_y).wait_recv()
            hop_copy(cls, step, diagonal, 0, 4, to_y).wait_recv()
            hop_copy(cls, step, diagonal, 1, 5, to_x).wait_recv()

    first_leg(0)
    spread(nt, 0, own_rows)
    first_leg(1)
    first_leg(2)
    first_leg(3)
    direct(0, 0)
    direct(2, 0)
    relay(0, 0)
    for step in later:
        direct(0, step)
    for step in later:
        relay(0, step)
    direct(1, 0)
    pass_on(nt, 0, own_rows)
    await_pass(nt, 0, own_rows)
    await_leg(0)

    head = tp * groups + z
    log_gamma = gammas[pl.ds(head, 1), :]
    distance = (
        lax.broadcasted_iota(jnp.int32, (length, length), 0)
        - lax.broadcasted_iota(jnp.int32, (length, length), 1)
    ).astype(jnp.float32)
    decay = jnp.where(distance >= 0, jnp.exp(log_gamma * jnp.maximum(distance, 0.0)), 0.0)
    chunk = 2 * length if (groups % 2 == 0) else length

    @pl.loop(0, groups * length // chunk)
    def _(at):
        span = rows(at, chunk)
        qkvg[span, :] = jnp.dot(
            nt[span, :], w1[...], preferred_element_type=jnp.float32
        ).astype(jnp.bfloat16)

    for step in later:
        direct(1, step)
    relay(2, 0)
    direct(3, 0)

    @pl.loop(0, groups)
    def _(at):
        span = rows(at, length)
        block = qkvg[span, :].astype(jnp.float32)

        def turn(x):
            return x * cos_t[...] + pltpu.roll(x, cq // 2, 1) * sin_t[...]

        rq = turn(block[:, :cq])
        rk = turn(block[:, cq : 2 * cq])
        scores = lax.dot_general(
            rq, rk, (((1,), (1,)), ((), ())), precision=highest, preferred_element_type=jnp.float32
        ) * decay
        kept = jnp.dot(
            scores, block[:, 2 * cq : 2 * cq + cv], precision=highest,
            preferred_element_type=jnp.float32,
        )
        kept = kept * lax.rsqrt(jnp.mean(kept * kept, axis=-1, keepdims=True) + 1e-06)
        gain = mixer_gain[:, lanes(z, cv)]
        whole = (kept * gain * silu(block[:, 2 * cq + cv :])).astype(jnp.bfloat16)
        hid[rows(at, own), :] = whole[:own]
        hid[rows(at + groups, own), :] = whole[own:]

    def multiply(left, weight, part, xb, which, half):
        value = jnp.dot(
            left[rows(half, groups * own), :], weight[...], preferred_element_type=jnp.float32
        ).astype(jnp.bfloat16)
        for g in everyone:
            part[half, 0, g] = value[g * own : g * own + few]
            part[half, 1, g] = value[g * own + few : (g + 1) * own]
        go(remote(part.at[half, other], xb.at[half], x_send.at[which, half], x_recv.at[which, half], partner))

    def reduce_pair(part, xb, sb, rb, acc, which, half):
        remote(part.at[half, other], xb.at[half], x_send.at[which, half], x_recv.at[which, half], partner).wait_recv()

        def pair(g):
            return part[half, tp, g].astype(jnp.float32) + xb[half, g].astype(jnp.float32)

        for step in later:
            sb[half, step] = pair(zpeer(step)).astype(jnp.bfloat16)
            go(remote(sb.at[half, step], rb.at[half, step], r_send.at[which, half, step],
                      r_recv.at[which, half, step], zdev(zpeer(step))))
        acc[half] = pair(z)

    def collect(sb, rb, acc, which, half):
        value = acc[half]
        for step in later:
            remote(sb.at[half, step], rb.at[half, step], r_send.at[which, half, step],
                   r_recv.at[which, half, step], zdev(zpeer(step))).wait_recv()
            value = value + rb[half, step].astype(jnp.float32)
        return value

    def natural(half, core):
        return pl.ds(pl.multiple_of(half * own + core * few, few), few)

    for step in everyone:
        relay(1, step)
    await_leg(1)
    multiply(hid, wout, part1, xb1, 0, 0)
    multiply(hid, wout, part1, xb1, 0, 1)
    reduce_pair(part1, xb1, sb1, rb1, acc, 0, 0)
    reduce_pair(part1, xb1, sb1, rb1, acc, 0, 1)
    for step in later:
        direct(2, step)
    for step in later:
        relay(2, step)
    for half in range(2):
        middle = (
            tokens[natural(half, tp), :].astype(jnp.float32) + collect(sb1, rb1, acc, 0, half)
        ).astype(jnp.bfloat16).astype(jnp.float32)
        mid[half] = middle
        nm[in_half(half)(z, tp), :] = normed_rows(middle, channel_gain[...])
        spread(nm, 1 + half, in_half(half))
    for step in later:
        direct(3, step)
    for step in everyone:
        relay(3, step)

    place = lax.rem(lax.broadcasted_iota(jnp.int32, (groups * own, 1), 0), own)

    def convolve(half, low, taps):
        x = both[half, :, low : low + cf].astype(jnp.float32)
        count = taps.shape[0]
        weights = taps[:, lanes(z, cf)]
        result = x * weights[count - 1 :, :]
        for back in range(1, count):
            if half:
                before = both[0, :, low : low + cf].astype(jnp.float32)
                before = pltpu.roll(before, back + (groups - 1) * own, 0)
            else:
                before = 0.0
            moved = jnp.where(place >= back, pltpu.roll(x, back, 0), before)
            result = result + moved * weights[count - 1 - back : count - back, :]
        return result

    for half in range(2):
        pass_on(nm, 1 + half, in_half(half))
        await_pass(nm, 1 + half, in_half(half))
        if not half:
            await_leg(2)
        both[half] = jnp.dot(
            nm[rows(half, groups * own), :], wlr[...], preferred_element_type=jnp.float32
        ).astype(jnp.bfloat16)
        gated[rows(half, groups * own), :] = (
            silu(convolve(half, 0, taps_left)) * convolve(half, cf, taps_right)
        ).astype(jnp.bfloat16)
        if not half:
            await_leg(3)
        multiply(gated, wdown, part2, xb2, 1, half)
        reduce_pair(part2, xb2, sb2, rb2, acc, 1, half)
    for half in range(2):
        mine = natural(half, tp)
        value = (mid[half] + collect(sb2, rb2, acc, 1, half)).astype(jnp.bfloat16)
        fin[half] = value
        go(remote(fin.at[half], fin_in.at[half], o_send.at[half], o_recv.at[half], partner))
        out[mine, :] = value
    for half in range(2):
        remote(fin.at[half], fin_in.at[half], o_send.at[half], o_recv.at[half], partner).wait_recv()
        out[natural(half, other), :] = fin_in[half]
    for copy in pending:
        copy.wait_send()


def body(n_fs, *args):
    (tokens, norm_gain, w_query, w_key, w_value, w_gate, mixer_gain, w_out, channel_gain,
     w_left, w_right, taps_left, taps_right, w_down) = args
    groups = w_query.shape[1] // DK
    if (
        groups < 2
        or n_fs % groups
        or n_fs != 4 * groups
        or lax.axis_size("tp") != 2
        or tokens.shape[0] != BLOCK
        or (w_left.shape[1] // groups) % 128
        or w_left.shape[1] % groups
        or w_out.shape[1] % 128
        or w_query.shape[0] % 16
    ):
        return plain_body(*args)
    length, width = tokens.shape
    heads = groups * lax.axis_size("tp")
    cq, cv, cf = w_query.shape[1] // groups, w_value.shape[1] // groups, w_left.shape[1] // groups
    planes = n_fs // groups
    own = length // 2
    few = own // 2
    cos_t, sin_t = turning(length, DK)
    vmem = pl.BlockSpec(memory_space=pltpu.VMEM)
    held = pl.BlockSpec(memory_space=pl.ANY)
    bf, f32, dma = jnp.bfloat16, jnp.float32, pltpu.SemaphoreType.DMA
    return pl.pallas_call(
        functools.partial(layer_kernel, n_fs, groups),
        out_shape=jax.ShapeDtypeStruct(tokens.shape, bf),
        in_specs=[vmem] * 2 + [held] * 4 + [vmem, held, vmem] + [held] * 2 + [vmem] * 2 + [held] + [vmem] * 3,
        out_specs=vmem,
        scratch_shapes=[
            pltpu.VMEM((width, 2 * cq + 2 * cv), bf),
            pltpu.VMEM((cv, width), bf),
            pltpu.VMEM((width, 2 * cf), bf),
            pltpu.VMEM((cf, width), bf),
            pltpu.VMEM((groups * length, width), bf),
            pltpu.VMEM((groups * length, width), bf),
            pltpu.VMEM((groups * length, 2 * cq + 2 * cv), bf),
            pltpu.VMEM((groups * length, cv), bf),
            pltpu.VMEM((groups * length, cf), bf),
            pltpu.VMEM((2, 2, groups, few, width), bf),
            pltpu.VMEM((2, 2, groups, few, width), bf),
            pltpu.VMEM((2, groups, few, width), bf),
            pltpu.VMEM((2, groups, few, width), bf),
            pltpu.VMEM((2, groups, few, width), bf),
            pltpu.VMEM((2, groups, few, width), bf),
            pltpu.VMEM((2, groups, few, width), bf),
            pltpu.VMEM((2, groups, few, width), bf),
            pltpu.VMEM((2, few, width), f32),
            pltpu.VMEM((2, few, width), f32),
            pltpu.VMEM((2, groups * own, 2 * cf), bf),
            pltpu.VMEM((2, few, width), bf),
            pltpu.VMEM((2, few, width), bf),
            dma((8, groups)),
            dma((8, groups)),
            dma((8,)),
            dma((4, groups, 6)),
            dma((4, groups, 6)),
            dma((3, groups)),
            dma((3, groups)),
            dma((3, groups)),
            dma((3, groups)),
            dma((2, 2)),
            dma((2, 2)),
            dma((2, 2, groups)),
            dma((2, 2, groups)),
            dma((2,)),
            dma((2,)),
        ],
        compiler_params=pltpu.CompilerParams(
            collective_id=0, has_side_effects=True, vmem_limit_bytes=60 * 1024 * 1024
        ),
    )(
        tokens, norm_gain[None], w_query, w_key, w_value, w_gate, mixer_gain[None], w_out,
        channel_gain[None], w_left, w_right, taps_left, taps_right, w_down,
        cos_t, sin_t, log_gammas(heads),
    )


def solution(mesh):
    placed = (
        P("fs", None),
        P(),
        P("fs", "tp"),
        P("fs", "tp"),
        P("fs", "tp"),
        P("fs", "tp"),
        P("tp"),
        P("tp", "fs"),
        P(),
        P("fs", "tp"),
        P("fs", "tp"),
        P(None, "tp"),
        P(None, "tp"),
        P("tp", "fs"),
    )
    return jax.shard_map(
        functools.partial(body, mesh.shape["fs"]), mesh=mesh, in_specs=placed, out_specs=P("fs", None), check_vma=False)
```

profile of v0, /device:TPU:0, one launch (start us, length us, event | category | flops | bytes accessed | tf_op | source)
XLA Modules:
  0.0 156.8 jit_solution(8705208096262288449)
XLA Ops:
  0.0 154.9 %shard_map.163 = bf16[128,2048]{1,0:T(8,128)(2,1)} custom-call(bf16[128,2048]{1,0:T(8,128)(2,1)} %tokens.1, f32[1,2048]{1,0:T(1,128)} %bitcast.3, bf16[128,512]{1,0:T(8,128)(2,1)} %wq.1, bf16[128,512]{1,0:T(8,128)(2,1)} %wk.1, bf16[128,1024]{1,0:T(8,128)(2,1)} %wv.1, bf16[128,1024]{1,0:T(8,128)(2,1)} %wg.1, f32[1,1024]{1,0:T(1,128)} %bitcast.5, ...), custom_call_target="tpu_custom_call" | custom-call | tf_op jit(solution)/shard_map/pallas_call | solution.py:596
  154.9 1.9 %copy.19 = bf16[128,2048]{1,0:T(8,128)(2,1)} copy(bf16[128,2048]{1,0:T(8,128)(2,1)} %shard_map.163) | data formatting | bytes 1048576
where the time goes:
time: 159 us; the launch traced here: 157 us
  Pallas kernels  155 us (97%)
  local copies, waits for them, and re-layouts  1.88 us (1%)
    pallas_call x1, Pallas kernels, body(): pl.pallas_call(functools.partial(layer_kernel, n_fs, groups), out_shape=j...  155 us

commit v1 on v0

v1 whole, which is shorter than its diff:
```python
import functools

import jax
import jax.numpy as jnp
import numpy as np
from jax import lax
from jax.experimental import pallas as pl
from jax.experimental.pallas import tpu as pltpu
from jax.sharding import PartitionSpec as P

DK = 128
DV = 256
BLOCK = 128
MESH = pl.DeviceIdType.MESH


highest = lax.Precision.HIGHEST


def scale_rows(rows_in, gain_vec):
    floats = rows_in.astype(jnp.float32)
    factor = lax.rsqrt(jnp.mean(floats * floats, axis=-1, keepdims=True) + 1e-06)
    return (floats * factor * gain_vec).astype(jnp.bfloat16)


def decays(first_head, count):
    head_ids = first_head + jnp.arange(count, dtype=jnp.float32)
    return jnp.log(1.0 - 2.0 ** (-5.0 - head_ids))


def rotate(heads_in, positions):
    width = heads_in.shape[-1]
    half = width // 2
    freqs = 10000.0 ** (-jnp.arange(half, dtype=jnp.float32) / half)
    angles = positions[:, None] * freqs[None, :]
    cosine = jnp.cos(angles)
    sine = jnp.sin(angles)
    first_half = heads_in[..., :half]
    second_half = heads_in[..., half:]
    return jnp.concatenate(
        [first_half * cosine - second_half * sine, first_half * sine + second_half * cosine],
        axis=-1,
    )


def retention(queries, keys_in, values_in, log_gamma):
    head_count, length, key_width = queries.shape
    value_width = values_in.shape[-1]
    blocks = length // BLOCK
    queries = queries.reshape(head_count, blocks, BLOCK, key_width)
    keys_in = keys_in.reshape(head_count, blocks, BLOCK, key_width)
    values_in = values_in.reshape(head_count, blocks, BLOCK, value_width)
    offsets = jnp.arange(BLOCK, dtype=jnp.float32)
    distance = offsets[:, None] - offsets[None, :]
    weights = jnp.where(
        distance >= 0, jnp.exp(log_gamma[:, None, None] * jnp.maximum(distance, 0.0)), 0.0
    )
    scores = jnp.einsum("hbnd,hbmd->hbnm", queries, keys_in, precision=highest) * weights[:, None]
    inner = jnp.einsum("hbnm,hbme->hbne", scores, values_in, precision=highest)
    key_weight = jnp.exp(log_gamma[:, None] * (BLOCK - 1 - offsets)[None, :])
    contrib = jnp.einsum(
        "hbjd,hbje->hbde", keys_in * key_weight[:, None, :, None], values_in, precision=highest
    )
    block_decay = jnp.exp(log_gamma * BLOCK)[:, None, None]

    def advance(state, contrib_block):
        return (state * block_decay + contrib_block, state)

    _, states = lax.scan(
        advance,
        jnp.zeros((head_count, key_width, value_width), jnp.float32),
        jnp.moveaxis(contrib, 1, 0),
    )
    states = jnp.moveaxis(states, 0, 1)
    query_weight = jnp.exp(log_gamma[:, None] * (offsets + 1.0)[None, :])
    carried = (
        jnp.einsum("hbnd,hbde->hbne", queries, states, precision=highest)
        * query_weight[:, None, :, None]
    )
    return (inner + carried).reshape(head_count, length, value_width)


def head_norm(retained):
    return retained * lax.rsqrt(jnp.mean(retained * retained, axis=-1, keepdims=True) + 1e-06)


def causal_taps(values_in, taps):
    length = values_in.shape[-2]
    padded = jnp.pad(values_in.astype(jnp.float32), ((taps.shape[0] - 1, 0), (0, 0)))
    result = padded[0:length] * taps[0]
    for tap_index in range(1, taps.shape[0]):
        result = result + padded[tap_index : tap_index + length] * taps[tap_index]
    return result


def fold_single(source, weight_piece):
    return jnp.dot(source, weight_piece, preferred_element_type=jnp.float32)


def collect_single(source, weight):
    return fold_single(source, lax.all_gather(weight, "fs", axis=0, tiled=True))


def plain_body(
    tokens,
    norm_gain,
    w_query,
    w_key,
    w_value,
    w_gate,
    mixer_gain,
    w_out,
    channel_gain,
    w_left,
    w_right,
    taps_left,
    taps_right,
    w_down,
):
    length = tokens.shape[0]
    normed = scale_rows(tokens, norm_gain)
    queries = collect_single(normed, w_query)
    keys_proj = collect_single(normed, w_key)
    values_proj = collect_single(normed, w_value)
    gates = collect_single(normed, w_gate)
    queries = queries.astype(jnp.bfloat16)
    keys_proj = keys_proj.astype(jnp.bfloat16)
    values_proj = values_proj.astype(jnp.bfloat16)
    gates = gates.astype(jnp.bfloat16)
    heads_here = w_query.shape[1] // DK
    first_head = (lax.axis_index("tp") * heads_here).astype(jnp.float32)
    log_gamma = decays(first_head, heads_here)
    positions = jnp.arange(length, dtype=jnp.float32)

    def split_heads(rows_in, width):
        return rows_in.astype(jnp.float32).reshape(length, heads_here, width).transpose(1, 0, 2)

    retained = head_norm(
        retention(
            rotate(split_heads(queries, DK), positions),
            rotate(split_heads(keys_proj, DK), positions),
            split_heads(values_proj, DV),
            log_gamma,
        )
    )
    retained = retained.transpose(1, 0, 2).reshape(length, heads_here * DV)
    hidden = (retained * mixer_gain * jax.nn.silu(gates.astype(jnp.float32))).astype(jnp.bfloat16)
    rows_own = length // lax.axis_size("tp")
    first_row = lax.axis_index("tp") * rows_own
    out_whole = lax.all_gather(w_out, "fs", axis=1, tiled=True)
    mixer_total = lax.psum_scatter(
        jnp.dot(hidden, out_whole, preferred_element_type=jnp.float32).astype(jnp.bfloat16),
        "tp",
        scatter_dimension=0,
        tiled=True,
    ).astype(jnp.float32)
    residual = lax.dynamic_slice_in_dim(tokens, first_row, rows_own, 0)
    middle_own = (residual.astype(jnp.float32) + mixer_total).astype(jnp.bfloat16)
    middle = lax.all_gather(middle_own, "tp", axis=0, tiled=True)
    normed_mid = scale_rows(middle, channel_gain)
    left = collect_single(normed_mid, w_left)
    right = collect_single(normed_mid, w_right)
    left = left.astype(jnp.bfloat16)
    right = right.astype(jnp.bfloat16)
    gated = (jax.nn.silu(causal_taps(left, taps_left)) * causal_taps(right, taps_right)).astype(
        jnp.bfloat16
    )
    down_whole = lax.all_gather(w_down, "fs", axis=1, tiled=True)
    channel_part = jnp.dot(gated, down_whole, preferred_element_type=jnp.float32)
    channel_total = lax.psum(channel_part.astype(jnp.bfloat16), "tp").astype(jnp.float32)
    return (middle.astype(jnp.float32) + channel_total).astype(jnp.bfloat16)


def log_gammas(head_count):
    table = np.log(1.0 - 2.0 ** (-5.0 - np.arange(head_count, dtype=np.float64)))
    return np.repeat(table[:, None], BLOCK, axis=1).astype(np.float32)


def turning(length, width):
    half = width // 2
    freqs = np.float32(10000.0) ** (-np.arange(half, dtype=np.float32) / np.float32(half))
    angles = (np.arange(length, dtype=np.float32)[:, None] * freqs[None, :]).astype(np.float64)
    cosine, sine = np.cos(angles), np.sin(angles)
    return (
        np.concatenate([cosine, cosine], axis=1).astype(np.float32),
        np.concatenate([-sine, sine], axis=1).astype(np.float32),
    )


def silu(v):
    return v / (1.0 + jnp.exp(-v))


def normed_rows(floats, gain):
    factor = lax.rsqrt(jnp.mean(floats * floats, axis=-1, keepdims=True) + 1e-06)
    return (floats * factor * gain).astype(jnp.bfloat16)


HOP, SUM, SWAP = 3, 4, 5
CHUNKS = 4
NT_PARTS = 2
CLASS_OF = (0, 0, 0, 1, 2, 3, 4, 5)
STAGES = (
    (0, 0),
    (0, 1),
    (1, 0),
    (1, 1),
    (2, 0),
    (2, 1),
    (2, 2),
    (2, 3),
    (3, 0),
    (3, 1),
    (3, 2),
    (3, 3),
    (4, 0),
    (5, 0),
    (4, 1),
    (5, 1),
    (4, 2),
    (5, 2),
    (4, 3),
    (5, 3),
    (6, 0),
    (6, 1),
    (6, 2),
    (6, 3),
)
PLAN = (
    (
        (
            (1, 0, 0, 0, 0, 0), (1, 1, 0, 0, 0, 0), (1, 3, 0, 0, 0), (1, 3, 0, 0, 1), (1, 1, 0, 1, 0, 0),
            (0, 1, 0, 0, 0, 0), (1, 3, 0, 0, 2), (1, 3, 0, 0, 3), (1, 0, 0, 1, 0, 0), (1, 3, 1, 0, 0),
            (1, 3, 1, 0, 1), (0, 3, 0, 0, 0), (0, 3, 0, 0, 1), (1, 3, 0, 0, 5), (1, 3, 0, 0, 4), (0, 0, 0, 0, 1, 1),
            (1, 1, 0, 0, 1, 1), (1, 3, 1, 0, 2), (1, 3, 1, 0, 3), (0, 3, 1, 0, 0), (0, 3, 1, 0, 1), (1, 2, 2, 3),
            (1, 3, 1, 0, 5), (1, 3, 1, 0, 4), (0, 1, 0, 0, 1, 1), (1, 3, 2, 0, 0), (1, 3, 2, 0, 1), (1, 3, 2, 0, 2),
            (1, 3, 2, 0, 3), (0, 0, 0, 1, 1, 1), (1, 1, 0, 1, 1, 1), (1, 3, 3, 0, 0), (1, 3, 3, 0, 1), (1, 2, 2, 1),
            (1, 3, 3, 0, 2), (1, 3, 3, 0, 3), (0, 3, 2, 0, 0), (0, 3, 2, 0, 1), (1, 2, 2, 2), (1, 3, 2, 0, 5),
            (1, 3, 2, 0, 4), (1, 3, 4, 0, 0), (1, 3, 4, 0, 1), (0, 3, 3, 0, 0), (0, 3, 3, 0, 1), (1, 3, 3, 0, 5),
            (1, 3, 3, 0, 4), (0, 0, 0, 0, 1, 2), (1, 1, 0, 0, 1, 2), (1, 2, 0, 3), (1, 3, 4, 0, 2), (1, 3, 4, 0, 3),
            (0, 1, 0, 0, 1, 2), (0, 3, 4, 0, 0), (0, 3, 4, 0, 1), (1, 3, 4, 0, 5), (1, 3, 4, 0, 4), (1, 2, 0, 1),
            (0, 0, 0, 1, 1, 2), (1, 1, 0, 1, 1, 2), (1, 2, 1, 3), (1, 3, 5, 0, 0), (1, 3, 5, 0, 1), (1, 3, 5, 0, 2),
            (1, 3, 5, 0, 3), (1, 2, 3, 3), (0, 2, 0, 3), (0, 3, 5, 0, 0), (0, 3, 5, 0, 1), (1, 3, 5, 0, 5),
            (1, 3, 5, 0, 4), (0, 0, 0, 0, 1, 3), (1, 1, 0, 0, 1, 3), (1, 2, 0, 2), (0, 2, 1, 3), (0, 2, 2, 3),
            (1, 3, 0, 3, 0), (1, 3, 0, 3, 1), (0, 1, 0, 0, 1, 3), (0, 1, 0, 1, 0, 0), (0, 1, 0, 1, 1, 1),
            (0, 1, 0, 1, 1, 2), (1, 2, 4, 3), (1, 3, 0, 3, 2), (1, 3, 0, 3, 3), (0, 3, 0, 3, 0), (0, 3, 0, 3, 1),
            (1, 3, 0, 3, 5), (1, 3, 0, 3, 4), (0, 2, 3, 3), (1, 2, 1, 1), (1, 3, 1, 3, 0), (1, 3, 1, 3, 1),
            (1, 2, 3, 1), (1, 3, 1, 3, 2), (1, 3, 1, 3, 3), (0, 0, 0, 1, 1, 3), (1, 1, 0, 1, 1, 3), (1, 2, 4, 1),
            (0, 3, 1, 3, 0), (0, 3, 1, 3, 1), (1, 3, 1, 3, 5), (1, 3, 1, 3, 4), (0, 2, 0, 2), (0, 1, 0, 1, 1, 3),
            (0, 3, 0, 0, 2), (0, 3, 0, 0, 3), (0, 3, 0, 0, 4), (0, 3, 0, 0, 5), (1, 2, 1, 2), (0, 2, 4, 3),
            (1, 3, 2, 3, 0), (1, 3, 2, 3, 1), (0, 2, 0, 1), (1, 3, 2, 3, 2), (1, 3, 2, 3, 3), (0, 2, 1, 1),
            (0, 2, 2, 1), (1, 2, 3, 2), (1, 3, 0, 1, 0), (1, 3, 0, 1, 1), (0, 3, 2, 3, 0), (0, 3, 2, 3, 1),
            (1, 3, 0, 1, 2), (1, 3, 0, 1, 3), (0, 2, 3, 1), (1, 2, 4, 2), (0, 2, 1, 2), (0, 2, 2, 2), (1, 3, 0, 2, 0),
            (1, 3, 0, 2, 1), (0, 3, 0, 1, 0), (0, 3, 0, 1, 1), (1, 3, 0, 1, 5), (1, 3, 0, 1, 4), (0, 2, 4, 1),
            (0, 3, 0, 1, 2), (0, 3, 0, 1, 3), (1, 2, 5, 3), (0, 2, 3, 2), (1, 3, 0, 2, 2), (1, 3, 0, 2, 3),
            (0, 3, 0, 2, 0), (0, 3, 0, 2, 1), (1, 3, 0, 2, 5), (1, 3, 0, 2, 4), (0, 3, 0, 1, 4), (0, 3, 0, 1, 5),
            (0, 2, 4, 2), (1, 3, 1, 1, 0), (1, 3, 1, 1, 1), (0, 2, 5, 1), (0, 3, 0, 2, 2), (0, 3, 0, 2, 3),
            (1, 3, 1, 1, 2), (1, 3, 1, 1, 3), (1, 2, 7, 3), (1, 3, 1, 2, 0), (1, 3, 1, 2, 1), (0, 3, 0, 2, 4),
            (0, 3, 0, 2, 5), (0, 3, 0, 3, 2), (0, 3, 0, 3, 3), (0, 3, 0, 3, 4), (0, 3, 0, 3, 5), (0, 3, 1, 0, 2),
            (0, 3, 1, 0, 3), (0, 3, 1, 0, 4), (0, 3, 1, 0, 5), (1, 3, 1, 2, 2), (1, 3, 1, 2, 3), (0, 3, 1, 1, 0),
            (0, 3, 1, 1, 1), (1, 3, 1, 1, 5), (1, 3, 1, 1, 4), (0, 3, 1, 1, 2), (0, 3, 1, 1, 3), (1, 3, 2, 3, 5),
            (1, 3, 2, 3, 4), (0, 3, 1, 2, 0), (0, 3, 1, 2, 1), (1, 3, 1, 2, 5), (1, 3, 1, 2, 4), (0, 2, 7, 1),
            (0, 2, 5, 3), (1, 3, 2, 1, 0), (1, 3, 2, 1, 1), (1, 2, 5, 1), (0, 3, 1, 1, 4), (0, 3, 1, 1, 5),
            (0, 3, 1, 2, 2), (0, 3, 1, 2, 3), (1, 3, 2, 1, 2), (1, 3, 2, 1, 3), (1, 3, 2, 2, 0), (1, 3, 2, 2, 1),
            (0, 3, 1, 2, 4), (0, 3, 1, 2, 5), (0, 3, 1, 3, 2), (0, 3, 1, 3, 3), (0, 3, 1, 3, 4), (0, 3, 1, 3, 5),
        ),
        (
            (1, 3, 2, 2, 2), (1, 3, 2, 2, 3), (1, 2, 7, 1), (0, 3, 2, 1, 0), (0, 3, 2, 1, 1), (1, 3, 2, 1, 5),
            (1, 3, 2, 1, 4),
        ),
        (
            (1, 3, 3, 1, 0), (1, 3, 3, 1, 1), (0, 3, 2, 2, 0), (0, 3, 2, 2, 1), (0, 2, 7, 3),
        ),
        (
            (1, 3, 2, 2, 5), (1, 3, 2, 2, 4), (1, 2, 5, 2), (1, 3, 3, 1, 2), (1, 3, 3, 1, 3), (0, 2, 5, 2),
            (1, 3, 3, 3, 0), (1, 3, 3, 3, 1),
        ),
        (
            (0, 3, 3, 1, 0), (0, 3, 3, 1, 1), (1, 2, 7, 2), (1, 3, 3, 1, 5), (1, 3, 3, 1, 4), (0, 2, 7, 2),
            (1, 3, 3, 3, 2), (1, 3, 3, 3, 3), (0, 3, 2, 0, 2), (0, 3, 2, 0, 3), (0, 3, 2, 0, 4), (0, 3, 2, 0, 5),
            (0, 3, 2, 1, 2), (0, 3, 2, 1, 3), (0, 3, 2, 1, 4), (0, 3, 2, 1, 5), (0, 3, 2, 2, 2), (0, 3, 2, 2, 3),
            (0, 3, 2, 2, 4), (0, 3, 2, 2, 5), (0, 3, 2, 3, 2), (0, 3, 2, 3, 3), (0, 3, 2, 3, 4), (0, 3, 2, 3, 5),
        ),
        (
        ),
        (
            (1, 2, 6, 3),
        ),
        (
            (0, 3, 3, 3, 0), (0, 3, 3, 3, 1), (1, 3, 3, 3, 5), (1, 3, 3, 3, 4),
        ),
        (
            (0, 5, 0, 0), (1, 3, 3, 2, 0), (1, 3, 3, 2, 1), (1, 4, 0, 0, 0, 3), (0, 5, 0, 1), (1, 3, 3, 2, 2),
            (1, 3, 3, 2, 3), (0, 5, 0, 2), (1, 4, 0, 0, 0, 2), (1, 3, 5, 1, 0), (1, 3, 5, 1, 1), (0, 5, 0, 3),
            (0, 3, 3, 2, 0), (0, 3, 3, 2, 1), (1, 3, 3, 2, 5), (1, 3, 3, 2, 4), (1, 4, 0, 0, 0, 1), (0, 2, 6, 3),
            (1, 3, 4, 3, 0), (1, 3, 4, 3, 1), (1, 4, 0, 3, 0, 3), (0, 3, 5, 1, 0), (0, 3, 5, 1, 1), (1, 3, 4, 3, 2),
            (1, 3, 4, 3, 3), (0, 2, 6, 1), (1, 4, 0, 3, 0, 2), (1, 3, 4, 1, 0), (1, 3, 4, 1, 1), (0, 3, 4, 3, 0),
            (0, 3, 4, 3, 1), (1, 3, 4, 3, 5), (1, 3, 4, 3, 4), (1, 4, 0, 3, 0, 1), (1, 3, 4, 1, 2), (1, 3, 4, 1, 3),
            (1, 4, 0, 1, 0, 3), (0, 2, 6, 2), (0, 3, 4, 1, 0), (0, 3, 4, 1, 1), (1, 3, 4, 1, 5), (1, 3, 4, 1, 4),
            (1, 4, 0, 1, 0, 2), (1, 3, 4, 2, 0), (1, 3, 4, 2, 1), (1, 3, 4, 2, 2), (1, 3, 4, 2, 3),
            (1, 4, 0, 1, 0, 1), (1, 3, 5, 1, 5), (1, 3, 5, 1, 4), (1, 4, 0, 2, 0, 3), (0, 4, 0, 0, 1, 0),
        ),
        (
            (1, 1, 1, 0, 0, 0), (0, 3, 4, 2, 0), (0, 3, 4, 2, 1), (1, 3, 4, 2, 5), (1, 3, 4, 2, 4),
            (1, 0, 1, 0, 0, 0), (1, 3, 5, 1, 2), (1, 3, 5, 1, 3), (0, 0, 1, 0, 1, 1), (1, 1, 1, 0, 1, 1),
            (1, 3, 5, 3, 0), (1, 3, 5, 3, 1), (1, 4, 0, 2, 0, 2), (1, 3, 5, 3, 2), (1, 3, 5, 3, 3),
            (1, 4, 0, 2, 0, 1), (1, 3, 5, 2, 0), (1, 3, 5, 2, 1), (0, 0, 1, 0, 1, 2), (1, 1, 1, 0, 1, 2),
            (1, 2, 6, 1), (0, 3, 5, 3, 0), (0, 3, 5, 3, 1), (1, 3, 5, 3, 5), (1, 3, 5, 3, 4), (1, 3, 5, 2, 2),
            (1, 3, 5, 2, 3), (0, 4, 0, 1, 1, 0),
        ),
        (
            (1, 1, 1, 1, 0, 0), (1, 0, 1, 1, 0, 0), (0, 3, 5, 2, 0), (0, 3, 5, 2, 1), (1, 3, 5, 2, 5),
            (1, 3, 5, 2, 4), (0, 0, 1, 1, 1, 1), (1, 1, 1, 1, 1, 1), (1, 2, 6, 2), (0, 4, 0, 2, 1, 0),
        ),
        (
            (0, 4, 0, 3, 1, 0),
        ),
        (
            (1, 1, 1, 2, 0, 0), (0, 1, 1, 0, 0, 0), (0, 1, 1, 0, 1, 1), (0, 1, 1, 0, 1, 2), (1, 1, 1, 3, 0, 0),
            (1, 0, 1, 3, 0, 0), (0, 0, 1, 0, 1, 3), (1, 1, 1, 0, 1, 3), (1, 0, 1, 2, 0, 0), (0, 1, 1, 0, 1, 3),
            (0, 3, 3, 0, 2), (0, 3, 3, 0, 3), (0, 3, 3, 0, 4), (0, 3, 3, 0, 5), (0, 3, 3, 1, 2), (0, 3, 3, 1, 3),
            (0, 3, 3, 1, 4), (0, 3, 3, 1, 5), (0, 3, 3, 2, 2), (0, 3, 3, 2, 3), (0, 3, 3, 2, 4), (0, 3, 3, 2, 5),
            (0, 3, 3, 3, 2), (0, 3, 3, 3, 3), (0, 3, 3, 3, 4), (0, 3, 3, 3, 5), (0, 3, 4, 0, 2), (0, 3, 4, 0, 3),
            (0, 3, 4, 0, 4), (0, 3, 4, 0, 5), (0, 3, 4, 1, 2), (0, 3, 4, 1, 3), (0, 3, 4, 1, 4), (0, 3, 4, 1, 5),
            (0, 3, 4, 2, 2), (0, 3, 4, 2, 3), (0, 3, 4, 2, 4), (0, 3, 4, 2, 5), (0, 3, 4, 3, 2), (0, 3, 4, 3, 3),
            (0, 3, 4, 3, 4), (0, 3, 4, 3, 5),
        ),
        (
            (0, 0, 1, 1, 1, 2), (1, 1, 1, 1, 1, 2), (0, 3, 5, 0, 2), (0, 3, 5, 0, 3), (0, 3, 5, 0, 4),
            (0, 3, 5, 0, 5), (0, 3, 5, 1, 2), (0, 3, 5, 1, 3), (0, 3, 5, 1, 4), (0, 3, 5, 1, 5), (0, 3, 5, 2, 2),
            (0, 3, 5, 2, 3), (0, 3, 5, 2, 4), (0, 3, 5, 2, 5), (0, 3, 5, 3, 2), (0, 3, 5, 3, 3), (0, 3, 5, 3, 4),
            (0, 3, 5, 3, 5),
        ),
        (
            (0, 1, 1, 1, 0, 0), (0, 1, 1, 1, 1, 1), (0, 1, 1, 1, 1, 2), (0, 0, 1, 2, 1, 1), (1, 1, 1, 2, 1, 1),
            (0, 5, 1, 0), (1, 4, 1, 0, 0, 3), (0, 0, 1, 3, 1, 1), (1, 1, 1, 3, 1, 1), (1, 4, 1, 0, 0, 2),
            (0, 0, 1, 1, 1, 3), (1, 1, 1, 1, 1, 3), (1, 4, 1, 0, 0, 1), (0, 1, 1, 1, 1, 3),
        ),
        (
            (0, 0, 1, 3, 1, 2), (1, 1, 1, 3, 1, 2),
        ),
        (
            (0, 1, 1, 2, 0, 0), (0, 1, 1, 2, 1, 1), (0, 0, 1, 2, 1, 2), (1, 1, 1, 2, 1, 2), (0, 5, 1, 1),
            (1, 4, 1, 1, 0, 3), (0, 0, 1, 3, 1, 3), (1, 1, 1, 3, 1, 3), (0, 1, 1, 2, 1, 2), (1, 4, 1, 1, 0, 2),
            (0, 0, 1, 2, 1, 3), (1, 1, 1, 2, 1, 3), (0, 1, 1, 2, 1, 3),
        ),
        (
            (1, 4, 1, 1, 0, 1),
        ),
        (
            (0, 1, 1, 3, 0, 0), (0, 1, 1, 3, 1, 1), (0, 1, 1, 3, 1, 2), (0, 1, 1, 3, 1, 3),
        ),
        (
        ),
        (
            (0, 5, 1, 2), (1, 4, 1, 2, 0, 3), (0, 5, 1, 3), (1, 4, 1, 3, 0, 3), (0, 4, 1, 0, 1, 0),
        ),
        (
            (1, 4, 1, 2, 0, 2), (1, 4, 1, 3, 0, 2), (0, 4, 1, 1, 1, 0),
        ),
        (
            (1, 4, 1, 2, 0, 1), (1, 4, 1, 3, 0, 1), (0, 4, 1, 2, 1, 0),
        ),
        (
            (0, 4, 1, 3, 1, 0),
        ),
        (
        ),
    ),
    (
        (
            (1, 0, 0, 0, 0, 0), (1, 0, 0, 0, 1, 0), (1, 1, 0, 0, 0, 0), (1, 3, 0, 1, 0), (1, 3, 0, 1, 1),
            (1, 1, 0, 1, 0, 0), (0, 1, 0, 0, 0, 0), (1, 3, 0, 1, 2), (1, 3, 0, 1, 3), (1, 0, 0, 1, 0, 0),
            (1, 0, 0, 1, 1, 0), (1, 3, 1, 1, 0), (1, 3, 1, 1, 1), (0, 3, 0, 1, 0), (0, 3, 0, 1, 1), (1, 3, 0, 1, 5),
            (1, 3, 0, 1, 4), (0, 0, 0, 0, 0, 1), (0, 0, 0, 0, 1, 1), (1, 1, 0, 0, 0, 1), (1, 3, 1, 1, 2),
            (1, 3, 1, 1, 3), (1, 1, 0, 0, 1, 1), (0, 3, 1, 1, 0), (0, 3, 1, 1, 1), (1, 0, 0, 0, 0, 1),
            (1, 0, 0, 0, 1, 1), (1, 3, 1, 1, 5), (1, 3, 1, 1, 4), (0, 1, 0, 0, 0, 1), (1, 3, 2, 1, 0),
            (1, 3, 2, 1, 1), (0, 1, 0, 0, 1, 1), (1, 3, 2, 1, 2), (1, 3, 2, 1, 3), (0, 0, 0, 1, 0, 1),
            (0, 0, 0, 1, 1, 1), (1, 1, 0, 1, 0, 1), (1, 3, 3, 1, 0), (1, 3, 3, 1, 1), (1, 1, 0, 1, 1, 1),
            (1, 3, 3, 1, 2), (1, 3, 3, 1, 3), (0, 3, 2, 1, 0), (0, 3, 2, 1, 1), (1, 0, 0, 1, 0, 1),
            (1, 0, 0, 1, 1, 1), (1, 3, 2, 1, 5), (1, 3, 2, 1, 4), (1, 3, 4, 1, 0), (1, 3, 4, 1, 1), (0, 3, 3, 1, 0),
            (0, 3, 3, 1, 1), (1, 3, 3, 1, 5), (1, 3, 3, 1, 4), (0, 0, 0, 0, 1, 2), (1, 1, 0, 0, 1, 2),
            (1, 0, 0, 0, 1, 2), (1, 3, 4, 1, 2), (1, 3, 4, 1, 3), (0, 1, 0, 0, 1, 2), (0, 1, 0, 1, 0, 0),
            (0, 1, 0, 1, 0, 1), (0, 1, 0, 1, 1, 1), (0, 3, 4, 1, 0), (0, 3, 4, 1, 1), (1, 3, 4, 1, 5),
            (1, 3, 4, 1, 4), (1, 2, 2, 2), (1, 3, 5, 1, 0), (1, 3, 5, 1, 1), (1, 3, 5, 1, 2), (1, 3, 5, 1, 3),
            (0, 0, 0, 1, 1, 2), (0, 2, 0, 0), (1, 1, 0, 1, 1, 2), (1, 2, 2, 3), (1, 0, 0, 1, 1, 2), (0, 3, 5, 1, 0),
            (0, 3, 5, 1, 1), (1, 3, 5, 1, 5), (1, 3, 5, 1, 4), (0, 1, 0, 1, 1, 2), (1, 2, 0, 2), (1, 2, 0, 3),
            (0, 2, 0, 3), (0, 2, 0, 2), (1, 2, 1, 2), (1, 2, 2, 0), (1, 2, 3, 2), (1, 2, 0, 0), (1, 2, 4, 2),
            (1, 2, 1, 0), (0, 2, 1, 0), (0, 2, 2, 0), (0, 2, 1, 2), (0, 2, 2, 2), (1, 3, 0, 0, 0), (1, 3, 0, 0, 1),
            (1, 2, 3, 0), (1, 2, 1, 3), (0, 2, 3, 0), (0, 2, 3, 2), (1, 3, 0, 0, 2), (1, 3, 0, 0, 3), (1, 2, 3, 3),
            (1, 2, 4, 0), (0, 2, 4, 0), (0, 2, 4, 2), (1, 3, 0, 2, 0), (1, 3, 0, 2, 1), (0, 3, 0, 0, 0),
            (0, 3, 0, 0, 1), (1, 3, 0, 0, 5), (1, 3, 0, 0, 4), (0, 3, 0, 0, 2), (0, 3, 0, 0, 3), (1, 2, 4, 3),
            (1, 2, 5, 0), (0, 2, 1, 3), (0, 2, 2, 3), (1, 3, 0, 2, 2), (1, 3, 0, 2, 3), (0, 3, 0, 2, 0),
            (0, 3, 0, 2, 1), (1, 3, 0, 2, 5), (1, 3, 0, 2, 4), (0, 3, 0, 0, 4), (0, 3, 0, 0, 5), (0, 3, 0, 1, 2),
            (0, 3, 0, 1, 3), (0, 3, 0, 1, 4), (0, 3, 0, 1, 5), (1, 2, 5, 2), (0, 2, 3, 3), (1, 3, 0, 3, 0),
            (1, 3, 0, 3, 1), (0, 3, 0, 2, 2), (0, 3, 0, 2, 3), (1, 2, 7, 0), (1, 3, 0, 3, 2), (1, 3, 0, 3, 3),
            (0, 3, 0, 2, 4), (0, 3, 0, 2, 5), (0, 2, 4, 3), (1, 3, 1, 0, 0), (1, 3, 1, 0, 1), (0, 3, 0, 3, 0),
            (0, 3, 0, 3, 1), (1, 3, 0, 3, 5), (1, 3, 0, 3, 4), (1, 2, 7, 2), (0, 3, 0, 3, 2), (0, 3, 0, 3, 3),
            (1, 3, 1, 0, 2), (1, 3, 1, 0, 3), (0, 3, 1, 0, 0), (0, 3, 1, 0, 1), (0, 2, 5, 2), (1, 3, 1, 0, 5),
            (1, 3, 1, 0, 4), (1, 3, 1, 2, 0), (1, 3, 1, 2, 1), (0, 3, 0, 3, 4), (0, 3, 0, 3, 5), (1, 3, 1, 2, 2),
            (1, 3, 1, 2, 3), (0, 3, 1, 0, 2), (0, 3, 1, 0, 3), (1, 3, 1, 3, 0), (1, 3, 1, 3, 1), (1, 2, 5, 3),
            (0, 3, 1, 0, 4), (0, 3, 1, 0, 5), (0, 3, 1, 1, 2), (0, 3, 1, 1, 3), (0, 3, 1, 1, 4), (0, 3, 1, 1, 5),
            (1, 3, 1, 3, 2), (1, 3, 1, 3, 3), (0, 3, 1, 2, 0), (0, 3, 1, 2, 1), (1, 3, 1, 2, 5), (1, 3, 1, 2, 4),
            (0, 3, 1, 2, 2), (0, 3, 1, 2, 3), (0, 2, 7, 2), (1, 3, 2, 0, 0), (1, 3, 2, 0, 1), (1, 2, 7, 3),
            (0, 3, 1, 3, 0), (0, 3, 1, 3, 1), (1, 3, 1, 3, 5), (1, 3, 1, 3, 4), (1, 3, 2, 0, 2), (1, 3, 2, 0, 3),
            (0, 3, 1, 2, 4), (0, 3, 1, 2, 5), (0, 3, 1, 3, 2), (0, 3, 1, 3, 3), (0, 2, 5, 0), (1, 3, 2, 2, 0),
            (1, 3, 2, 2, 1), (0, 3, 2, 0, 0), (0, 3, 2, 0, 1), (1, 3, 2, 0, 5), (1, 3, 2, 0, 4), (0, 3, 1, 3, 4),
            (0, 3, 1, 3, 5),
        ),
        (
            (1, 3, 2, 2, 2), (1, 3, 2, 2, 3), (0, 2, 7, 0), (1, 3, 2, 3, 0), (1, 3, 2, 3, 1),
        ),
        (
            (0, 3, 2, 2, 0), (0, 3, 2, 2, 1), (1, 3, 2, 2, 5), (1, 3, 2, 2, 4), (1, 3, 2, 3, 2), (1, 3, 2, 3, 3),
        ),
        (
            (1, 3, 3, 2, 0), (1, 3, 3, 2, 1), (0, 3, 2, 3, 0), (0, 3, 2, 3, 1), (0, 2, 5, 3), (1, 3, 2, 3, 5),
            (1, 3, 2, 3, 4),
        ),
        (
            (1, 3, 3, 2, 2), (1, 3, 3, 2, 3), (1, 3, 3, 0, 0), (1, 3, 3, 0, 1), (0, 2, 7, 3), (0, 3, 3, 2, 0),
            (0, 3, 3, 2, 1), (0, 3, 2, 0, 2), (0, 3, 2, 0, 3), (0, 3, 2, 0, 4), (0, 3, 2, 0, 5), (0, 3, 2, 1, 2),
            (0, 3, 2, 1, 3), (0, 3, 2, 1, 4), (0, 3, 2, 1, 5), (0, 3, 2, 2, 2), (0, 3, 2, 2, 3), (0, 3, 2, 2, 4),
            (0, 3, 2, 2, 5), (0, 3, 2, 3, 2), (0, 3, 2, 3, 3), (1, 2, 6, 2), (1, 2, 6, 0), (0, 3, 2, 3, 4),
            (0, 3, 2, 3, 5),
        ),
        (
            (1, 3, 3, 2, 5), (1, 3, 3, 2, 4),
        ),
        (
        ),
        (
        ),
        (
            (1, 3, 3, 0, 2), (1, 3, 3, 0, 3), (1, 2, 6, 3), (0, 5, 0, 0), (0, 4, 0, 0, 0, 2), (0, 3, 3, 0, 0),
            (0, 3, 3, 0, 1), (1, 3, 3, 0, 5), (1, 3, 3, 0, 4), (0, 5, 0, 1), (0, 4, 0, 0, 0, 1), (1, 3, 3, 3, 0),
            (1, 3, 3, 3, 1), (0, 5, 0, 2), (0, 2, 6, 2), (1, 4, 0, 0, 0, 2), (1, 3, 3, 3, 2), (1, 3, 3, 3, 3),
            (0, 5, 0, 3), (0, 4, 0, 0, 0, 0), (1, 3, 4, 2, 0), (1, 3, 4, 2, 1), (1, 4, 0, 0, 0, 1),
            (0, 4, 0, 3, 0, 2), (0, 3, 3, 3, 0), (0, 3, 3, 3, 1), (1, 3, 3, 3, 5), (1, 3, 3, 3, 4),
            (1, 4, 0, 3, 0, 2), (0, 4, 0, 3, 0, 1), (1, 3, 4, 2, 2), (1, 3, 4, 2, 3), (0, 4, 0, 0, 1, 1),
            (1, 4, 0, 0, 1, 1), (1, 4, 0, 3, 0, 1), (0, 3, 4, 2, 0), (0, 3, 4, 2, 1), (1, 3, 4, 2, 5),
            (1, 3, 4, 2, 4), (0, 4, 0, 0, 1, 0),
        ),
        (
            (1, 0, 1, 0, 1, 0), (1, 1, 1, 0, 0, 0), (1, 3, 5, 2, 0), (1, 3, 5, 2, 1), (1, 0, 1, 0, 0, 0),
            (0, 4, 0, 1, 0, 2), (0, 4, 0, 3, 1, 1), (1, 4, 0, 3, 1, 1), (1, 3, 5, 2, 2), (1, 3, 5, 2, 3),
            (1, 4, 0, 1, 0, 2), (0, 4, 0, 1, 0, 1), (1, 3, 5, 0, 0), (1, 3, 5, 0, 1), (1, 4, 0, 1, 0, 1),
            (0, 3, 5, 2, 0), (0, 3, 5, 2, 1), (1, 3, 5, 2, 5), (1, 3, 5, 2, 4), (0, 4, 0, 1, 0, 0),
            (0, 0, 1, 0, 1, 1), (1, 0, 1, 0, 1, 1), (1, 1, 1, 0, 1, 1), (1, 3, 5, 0, 2), (1, 3, 5, 0, 3),
            (0, 4, 0, 2, 0, 2), (0, 4, 0, 1, 1, 1), (1, 4, 0, 2, 0, 2), (1, 4, 0, 1, 1, 1), (0, 3, 5, 0, 0),
            (0, 3, 5, 0, 1), (1, 3, 5, 0, 5), (1, 3, 5, 0, 4), (0, 0, 1, 0, 0, 1), (1, 1, 1, 0, 0, 1),
            (1, 3, 5, 3, 0), (1, 3, 5, 3, 1), (0, 4, 0, 1, 1, 0),
        ),
        (
            (1, 0, 1, 0, 0, 1), (1, 0, 1, 1, 1, 0), (1, 1, 1, 1, 0, 0), (1, 3, 5, 3, 2), (1, 3, 5, 3, 3),
            (0, 4, 0, 2, 0, 1), (1, 0, 1, 1, 0, 0), (0, 4, 0, 2, 1, 1), (1, 4, 0, 2, 1, 1), (0, 4, 0, 2, 0, 0),
            (1, 4, 0, 2, 0, 1), (0, 3, 5, 3, 0), (0, 3, 5, 3, 1), (1, 3, 5, 3, 5), (1, 3, 5, 3, 4),
            (0, 0, 1, 0, 1, 2), (1, 1, 1, 0, 1, 2), (1, 0, 1, 0, 1, 2), (0, 2, 6, 0), (1, 3, 4, 0, 0),
            (1, 3, 4, 0, 1), (0, 0, 1, 1, 1, 1), (1, 1, 1, 1, 1, 1), (1, 0, 1, 1, 1, 1), (1, 3, 4, 0, 2),
            (1, 3, 4, 0, 3), (0, 0, 1, 1, 0, 1), (1, 0, 1, 1, 0, 1), (1, 1, 1, 1, 0, 1), (0, 4, 0, 2, 1, 0),
        ),
        (
            (0, 4, 0, 3, 0, 0), (0, 4, 0, 3, 1, 0),
        ),
        (
            (1, 0, 1, 2, 1, 0), (1, 1, 1, 2, 0, 0), (0, 1, 1, 0, 0, 0), (0, 1, 1, 0, 0, 1), (0, 1, 1, 0, 1, 1),
            (0, 1, 1, 0, 1, 2), (0, 3, 3, 0, 2), (0, 3, 3, 0, 3), (0, 3, 3, 0, 4), (0, 3, 3, 0, 5), (0, 3, 3, 1, 2),
            (0, 3, 3, 1, 3), (0, 3, 3, 1, 4), (0, 3, 3, 1, 5), (0, 3, 3, 2, 2), (0, 3, 3, 2, 3), (0, 3, 3, 2, 4),
            (0, 3, 3, 2, 5), (0, 3, 3, 3, 2), (0, 3, 3, 3, 3), (0, 3, 3, 3, 4), (0, 3, 3, 3, 5), (1, 1, 1, 3, 0, 0),
            (1, 0, 1, 3, 0, 0), (1, 0, 1, 3, 1, 0), (0, 3, 4, 0, 0), (0, 3, 4, 0, 1), (1, 3, 4, 0, 5),
            (1, 3, 4, 0, 4), (0, 3, 4, 0, 2), (0, 3, 4, 0, 3), (1, 0, 1, 2, 0, 0), (0, 2, 6, 3), (1, 3, 4, 3, 0),
            (1, 3, 4, 3, 1), (0, 0, 1, 1, 1, 2), (1, 0, 1, 1, 1, 2), (1, 1, 1, 1, 1, 2), (0, 0, 1, 3, 0, 1),
            (1, 1, 1, 3, 0, 1), (1, 3, 4, 3, 2), (1, 3, 4, 3, 3), (1, 0, 1, 3, 0, 1), (0, 3, 4, 0, 4),
            (0, 3, 4, 0, 5), (0, 3, 4, 1, 2), (0, 3, 4, 1, 3), (0, 3, 4, 1, 4), (0, 3, 4, 1, 5), (0, 3, 4, 2, 2),
            (0, 3, 4, 2, 3), (0, 3, 4, 2, 4), (0, 3, 4, 2, 5), (0, 0, 1, 3, 1, 1), (1, 0, 1, 3, 1, 1),
            (1, 1, 1, 3, 1, 1), (0, 0, 1, 2, 0, 1), (1, 1, 1, 2, 0, 1), (1, 0, 1, 2, 0, 1), (0, 3, 4, 3, 0),
            (0, 3, 4, 3, 1), (1, 3, 4, 3, 5), (1, 3, 4, 3, 4), (0, 0, 1, 2, 1, 1), (1, 0, 1, 2, 1, 1),
            (1, 1, 1, 2, 1, 1), (0, 3, 4, 3, 2), (0, 3, 4, 3, 3), (0, 0, 1, 3, 1, 2), (1, 0, 1, 3, 1, 2),
            (1, 1, 1, 3, 1, 2), (0, 0, 1, 2, 1, 2), (1, 0, 1, 2, 1, 2), (1, 1, 1, 2, 1, 2), (0, 3, 4, 3, 4),
            (0, 3, 4, 3, 5),
        ),
        (
            (0, 3, 5, 0, 2), (0, 3, 5, 0, 3), (0, 3, 5, 0, 4), (0, 3, 5, 0, 5), (0, 3, 5, 1, 2), (0, 3, 5, 1, 3),
            (0, 3, 5, 1, 4), (0, 3, 5, 1, 5), (0, 3, 5, 2, 2), (0, 3, 5, 2, 3), (0, 3, 5, 2, 4), (0, 3, 5, 2, 5),
            (0, 3, 5, 3, 2), (0, 3, 5, 3, 3), (0, 3, 5, 3, 4), (0, 3, 5, 3, 5),
        ),
        (
            (0, 1, 1, 1, 0, 0), (0, 1, 1, 1, 0, 1), (0, 1, 1, 1, 1, 1), (0, 1, 1, 1, 1, 2),
        ),
        (
        ),
        (
            (0, 1, 1, 2, 0, 0), (0, 1, 1, 2, 0, 1), (0, 1, 1, 2, 1, 1), (0, 1, 1, 2, 1, 2),
        ),
        (
            (0, 5, 1, 0), (0, 4, 1, 0, 0, 1), (0, 4, 1, 0, 0, 2), (1, 4, 1, 0, 0, 2),
        ),
        (
            (0, 1, 1, 3, 0, 0), (0, 1, 1, 3, 0, 1), (0, 1, 1, 3, 1, 1), (0, 1, 1, 3, 1, 2),
        ),
        (
            (0, 5, 1, 1), (1, 4, 1, 0, 0, 1),
        ),
        (
            (0, 4, 1, 0, 0, 0), (0, 4, 1, 1, 0, 2), (0, 5, 1, 2), (1, 4, 1, 1, 0, 2), (0, 4, 1, 0, 1, 1),
            (1, 4, 1, 0, 1, 1), (0, 4, 1, 1, 0, 1), (0, 5, 1, 3), (1, 4, 1, 1, 0, 1), (0, 4, 1, 0, 1, 0),
        ),
        (
            (0, 4, 1, 1, 0, 0), (0, 4, 1, 1, 1, 1), (1, 4, 1, 1, 1, 1), (0, 4, 1, 1, 1, 0),
        ),
        (
            (0, 4, 1, 2, 0, 2), (1, 4, 1, 2, 0, 2), (0, 4, 1, 3, 0, 2), (1, 4, 1, 3, 0, 2), (0, 4, 1, 2, 0, 1),
            (1, 4, 1, 2, 0, 1), (0, 4, 1, 2, 1, 1), (1, 4, 1, 2, 1, 1), (0, 4, 1, 3, 0, 1), (1, 4, 1, 3, 0, 1),
            (0, 4, 1, 3, 1, 1), (1, 4, 1, 3, 1, 1), (0, 4, 1, 2, 0, 0), (0, 4, 1, 2, 1, 0),
        ),
        (
            (0, 4, 1, 3, 0, 0), (0, 4, 1, 3, 1, 0),
        ),
        (
        ),
    ),
)

def layer_kernel(
    n_fs,
    groups,
    tokens,
    norm_gain,
    wq,
    wk,
    wv,
    wg,
    mixer_gain,
    wo,
    channel_gain,
    wl,
    wr,
    taps_left,
    taps_right,
    wd,
    cos_t,
    sin_t,
    gammas,
    out,
    w1,
    wout,
    wlr,
    wdown,
    nt,
    nm,
    qkvg,
    hid,
    gated,
    part1,
    part2,
    xb1,
    xb2,
    sb1,
    sb2,
    rb1,
    rb2,
    mid,
    acc,
    both,
    fin,
    fin_in,
    s1_send,
    s1_recv,
    self_sem,
    s2_send,
    s2_recv,
    a_send,
    a_recv,
    f_send,
    f_recv,
    x_send,
    x_recv,
    r_send,
    r_recv,
    o_send,
    o_recv,
):
    fs, tp = lax.axis_index("fs"), lax.axis_index("tp")
    planes = n_fs // groups
    z, q = fs // planes, lax.rem(fs, planes)
    other = 1 - tp
    length, width = tokens.shape
    own = length // 2
    part_rows = own // NT_PARTS
    span_c = length // CHUNKS
    few = span_c // 2
    kb = wq.shape[0]
    nb = wo.shape[1]
    cq, cv, cf = wq.shape[1] // groups, wv.shape[1] // groups, wl.shape[1] // groups
    upper = z * 2 >= groups
    place_z = jnp.where(upper, groups - 1 - z, z)

    def real(plane):
        return jnp.where(upper, groups - 1 - plane, plane)

    def flip(side):
        return jnp.where(upper, 1 - side, side)

    def zdev(target):
        return {"fs": target * planes + q, "tp": tp}

    partner = {"fs": fs, "tp": other}

    def lanes(index, size):
        return pl.ds(pl.multiple_of(index * size, 128), size)

    def rows(index, size):
        return pl.ds(pl.multiple_of(index * size, size), size)

    pieces = (
        (lambda c: wq.at[:, lanes(c, cq)], lambda f: w1.at[rows(f, kb), pl.ds(0, cq)]),
        (lambda c: wk.at[:, lanes(c, cq)], lambda f: w1.at[rows(f, kb), pl.ds(cq, cq)]),
        (lambda c: wv.at[:, lanes(c, cv)], lambda f: w1.at[rows(f, kb), pl.ds(2 * cq, cv)]),
        (lambda c: wg.at[:, lanes(c, cv)], lambda f: w1.at[rows(f, kb), pl.ds(2 * cq + cv, cv)]),
        (lambda c: wo.at[rows(c, cv), :], lambda f: wout.at[:, lanes(f, nb)]),
        (lambda c: wl.at[:, lanes(c, cf)], lambda f: wlr.at[rows(f, kb), pl.ds(0, cf)]),
        (lambda c: wr.at[:, lanes(c, cf)], lambda f: wlr.at[rows(f, kb), pl.ds(cf, cf)]),
        (lambda c: wd.at[rows(c, cf), :], lambda f: wdown.at[:, lanes(f, nb)]),
    )
    starts = (0, cq, 2 * cq, 2 * cq + cv, 0, 0, cf, 0)
    widths = (cq, cq, cv, cv, 0, cf, cf, 0)

    def half_of(cls, f, half):
        members = [i for i in range(len(pieces)) if CLASS_OF[i] == cls]
        low = starts[members[0]]
        wide = sum(widths[i] for i in members)
        if members[0] < 4:
            return w1.at[pl.ds(pl.multiple_of(f * kb + half * (kb // 2), kb // 2), kb // 2), pl.ds(low, wide)]
        if members[0] == 4:
            return wout.at[pl.ds(half * (cv // 2), cv // 2), lanes(f, nb)]
        if members[0] < 7:
            return wlr.at[pl.ds(pl.multiple_of(f * kb + half * (kb // 2), kb // 2), kb // 2), pl.ds(low, wide)]
        return wdown.at[pl.ds(half * (cf // 2), cf // 2), lanes(f, nb)]

    barrier = pltpu.get_barrier_semaphore()
    for step in range(1, groups):
        pl.semaphore_signal(barrier, inc=1, device_id=zdev(lax.rem(z + step, groups)), device_id_type=MESH)
    qx = q + 1 - 2 * lax.rem(q, 2)
    qy = q + 2 - 4 * (q // 2)
    diagonal = planes - 1 - q
    to_x = {"fs": z * planes + qx, "tp": tp}
    to_y = {"fs": z * planes + qy, "tp": tp}
    for device in (to_x, to_y):
        pl.semaphore_signal(barrier, inc=1, device_id=device, device_id_type=MESH)
    pl.semaphore_signal(barrier, inc=1, device_id=partner, device_id_type=MESH)

    keeps = []
    for i, (src, dst) in enumerate(pieces):
        keep = pltpu.make_async_copy(src(z), dst(fs), self_sem.at[i])
        keep.start()
        keeps.append(keep)

    my_half = pl.ds(pl.multiple_of(tp * own, own), own)
    nt[pl.ds(pl.multiple_of(z * length + tp * own, own), own), :] = normed_rows(
        tokens[my_half, :].astype(jnp.float32), norm_gain[...]
    )
    pl.semaphore_wait(barrier, groups - 1 + 2 + 1)

    def remote(src, dst, ssem, rsem, device):
        return pltpu.make_async_remote_copy(
            src_ref=src, dst_ref=dst, send_sem=ssem, recv_sem=rsem,
            device_id=device, device_id_type=MESH,
        )

    def block(key, c, seq, core):
        if key:
            first = c * groups * span_c + seq * span_c + core * few
            return nm.at[pl.ds(pl.multiple_of(first, few), few), :]
        first = seq * length + core * own + c * part_rows
        return nt.at[pl.ds(pl.multiple_of(first, part_rows), part_rows), :]

    part, xb, sb, rb = (part1, part2), (xb1, xb2), (sb1, sb2), (rb1, rb2)

    def pair(which, c, g):
        return part[which][c, tp, g].astype(jnp.float32) + xb[which][c, g].astype(jnp.float32)

    def exchange(which, c):
        return remote(part[which].at[c, other], xb[which].at[c], x_send.at[which, c], x_recv.at[which, c], partner)

    def gather_copy(me, key, c, side, d, landing):
        move = 1 - 2 * side
        ref = block(key, c, real(me - move * d), tp)
        at = key + c + key * (NT_PARTS - 1)
        if landing:
            return remote(ref, ref, a_send.at[at, 0, 0], a_recv.at[at, flip(side), d], partner)
        return remote(
            ref, ref, a_send.at[at, flip(side), d], a_recv.at[at, flip(side), d + 1], zdev(real(me + move))
        )

    def core_copy(me, key, c, side, d, landing):
        move = 1 - 2 * side
        ref = block(key, c, real(me - move * d), other if landing else tp)
        at = key + c + key * (NT_PARTS - 1)
        where_side = flip(side) if d else 0
        return remote(ref, ref, f_send.at[at, where_side, d], f_recv.at[at, where_side, d], partner)

    def weight_copy(me, i, plane, landing):
        src, dst = pieces[i]
        far = real(plane)
        if landing:
            return remote(src(z), dst(far * planes + q), s1_send.at[i, far], s1_recv.at[i, far], zdev(far))
        return remote(src(far), dst(fs), s1_send.at[i, far], s1_recv.at[i, z], zdev(far))

    def hop_copy(me, cls, plane, slot, landing):
        origin = ((q, q, q, q, qx, qy), (qx, qy, qx, qy, diagonal, diagonal))[landing][slot]
        source = real(plane)
        ref = half_of(cls, source * planes + origin, (0, 1, 1, 0, 0, 1)[slot])
        device = (to_x, to_y, to_x, to_y, to_y, to_x)[slot]
        return remote(ref, ref, s2_send.at[cls, source, slot], s2_recv.at[cls, source, slot], device)

    def sum_copy(me, which, c, side, d, landing):
        ref = sb[which].at[c, flip(side), d]
        at = d if landing else d - 1
        device = partner if landing else zdev(real(me + 1 - 2 * side))
        return remote(
            ref, rb[which].at[c, flip(side), at], r_send.at[which, c, flip(side), d],
            r_recv.at[which, c, flip(side), at], device,
        )

    makers = (gather_copy, core_copy, weight_copy, hop_copy, sum_copy)

    def act(me, op):
        sends, kind, args = op[0], op[1], op[2:]
        if kind == SWAP:
            exchange(*args).wait_recv()
            return
        if not sends:
            makers[kind](me, *args, True).wait_recv()
            return
        if kind == HOP and args[1] == me and args[2] == 0:
            for i, keep in enumerate(keeps):
                if CLASS_OF[i] == args[0]:
                    keep.wait()
        if kind == SUM:
            which, c, side, d = args
            move = 1 - 2 * side
            value = pair(which, c, real(me + move * d))
            if 0 <= me - move < groups:
                value = value + rb[which][c, flip(side), d].astype(jnp.float32)
            sb[which][c, flip(side), d] = value.astype(jnp.bfloat16)
        makers[kind](me, *args, False).start()

    def perform(stage):
        for me, ops in enumerate(PLAN):
            @pl.when(place_z == me)
            def _():
                for op in ops[stage]:
                    act(me, op)

    pending = []

    def multiply(left, weight, which, c):
        value = jnp.dot(
            left[rows(c, groups * span_c), :], weight[...], preferred_element_type=jnp.float32
        ).astype(jnp.bfloat16)
        for g in range(groups):
            part[which][c, 0, g] = value[g * span_c : g * span_c + few]
            part[which][c, 1, g] = value[g * span_c + few : (g + 1) * span_c]
        copy = exchange(which, c)
        copy.start()
        pending.append(copy)

    def collect(which, c):
        acc[c] = pair(which, c, z)
        for side, has in ((0, z > 0), (1, z < groups - 1)):
            @pl.when(has)
            def _():
                acc[c] = acc[c] + rb[which][c, side, 0].astype(jnp.float32)
        return acc[c]

    def natural(c, core):
        return pl.ds(pl.multiple_of(c * span_c + core * few, few), few)

    head = tp * groups + z
    chunk = groups * length // 2

    def project(at):
        span = rows(at, chunk)
        qkvg[span, :] = jnp.dot(
            nt[span, :], w1[...], preferred_element_type=jnp.float32
        ).astype(jnp.bfloat16)

    def retain(first):
        log_gamma = gammas[pl.ds(head, 1), :]
        distance = (
            lax.broadcasted_iota(jnp.int32, (length, length), 0)
            - lax.broadcasted_iota(jnp.int32, (length, length), 1)
        ).astype(jnp.float32)
        decay = jnp.where(distance >= 0, jnp.exp(log_gamma * jnp.maximum(distance, 0.0)), 0.0)

        @pl.loop(first * groups // 2, (first + 1) * groups // 2)
        def _(at):
            span = rows(at, length)
            held = qkvg[span, :].astype(jnp.float32)

            def turn(x):
                return x * cos_t[...] + pltpu.roll(x, cq // 2, 1) * sin_t[...]

            rq = turn(held[:, :cq])
            rk = turn(held[:, cq : 2 * cq])
            scores = lax.dot_general(
                rq, rk, (((1,), (1,)), ((), ())), precision=highest, preferred_element_type=jnp.float32
            ) * decay
            kept = jnp.dot(
                scores, held[:, 2 * cq : 2 * cq + cv], precision=highest,
                preferred_element_type=jnp.float32,
            )
            kept = kept * lax.rsqrt(jnp.mean(kept * kept, axis=-1, keepdims=True) + 1e-06)
            gain = mixer_gain[:, lanes(z, cv)]
            whole = (kept * gain * silu(held[:, 2 * cq + cv :])).astype(jnp.bfloat16)
            for c in range(CHUNKS):
                hid[rows(at + c * groups, span_c), :] = whole[c * span_c : (c + 1) * span_c]

    def renorm(c):
        middle = (
            tokens[natural(c, tp), :].astype(jnp.float32) + collect(0, c)
        ).astype(jnp.bfloat16).astype(jnp.float32)
        mid[c] = middle
        first = c * groups * span_c + z * span_c + tp * few
        nm[pl.ds(pl.multiple_of(first, few), few), :] = normed_rows(middle, channel_gain[...])

    place = lax.rem(lax.broadcasted_iota(jnp.int32, (groups * span_c, 1), 0), span_c)

    def convolve(c, low, taps):
        x = both[c, :, low : low + cf].astype(jnp.float32)
        count = taps.shape[0]
        weights = taps[:, lanes(z, cf)]
        result = x * weights[count - 1 :, :]
        for back in range(1, count):
            if c:
                before = both[c - 1, :, low : low + cf].astype(jnp.float32)
                before = pltpu.roll(before, back + (groups - 1) * span_c, 0)
            else:
                before = 0.0
            moved = jnp.where(place >= back, pltpu.roll(x, back, 0), before)
            result = result + moved * weights[count - 1 - back : count - back, :]
        return result

    def mix(c):
        both[c] = jnp.dot(
            nm[rows(c, groups * span_c), :], wlr[...], preferred_element_type=jnp.float32
        ).astype(jnp.bfloat16)
        gated[rows(c, groups * span_c), :] = (
            silu(convolve(c, 0, taps_left)) * convolve(c, cf, taps_right)
        ).astype(jnp.bfloat16)

    def finish(c):
        value = (mid[c] + collect(1, c)).astype(jnp.bfloat16)
        fin[c] = value
        copy = remote(fin.at[c], fin_in.at[c], o_send.at[c], o_recv.at[c], partner)
        copy.start()
        pending.append(copy)
        out[natural(c, tp), :] = value

    steps = (
        project,
        retain,
        lambda c: multiply(hid, wout, 0, c),
        renorm,
        mix,
        lambda c: multiply(gated, wdown, 1, c),
        finish,
    )
    perform(0)
    for stage, (name, index) in enumerate(STAGES):
        steps[name](index)
        perform(stage + 1)
    for c in range(CHUNKS):
        remote(fin.at[c], fin_in.at[c], o_send.at[c], o_recv.at[c], partner).wait_recv()
        out[natural(c, other), :] = fin_in[c]
    for copy in pending:
        copy.wait_send()
    for me, ops in enumerate(PLAN):
        @pl.when(place_z == me)
        def _():
            for stage in ops:
                for op in stage:
                    if op[0]:
                        makers[op[1]](me, *op[2:], False).wait_send()


def body(n_fs, *args):
    (tokens, norm_gain, w_query, w_key, w_value, w_gate, mixer_gain, w_out, channel_gain,
     w_left, w_right, taps_left, taps_right, w_down) = args
    groups = w_query.shape[1] // DK
    if (
        groups != 2 * len(PLAN)
        or n_fs % groups
        or n_fs != 4 * groups
        or lax.axis_size("tp") != 2
        or tokens.shape[0] != BLOCK
        or (w_left.shape[1] // groups) % 128
        or w_left.shape[1] % groups
        or w_out.shape[1] % 128
        or w_query.shape[0] % 32
        or tokens.shape[0] % (32 * CHUNKS)
    ):
        return plain_body(*args)
    length, width = tokens.shape
    heads = groups * lax.axis_size("tp")
    cq, cv, cf = w_query.shape[1] // groups, w_value.shape[1] // groups, w_left.shape[1] // groups
    planes = n_fs // groups
    span_c = length // CHUNKS
    few = span_c // 2
    classes = max(CLASS_OF) + 1
    cos_t, sin_t = turning(length, DK)
    vmem = pl.BlockSpec(memory_space=pltpu.VMEM)
    held = pl.BlockSpec(memory_space=pl.ANY)
    bf, f32, dma = jnp.bfloat16, jnp.float32, pltpu.SemaphoreType.DMA
    return pl.pallas_call(
        functools.partial(layer_kernel, n_fs, groups),
        out_shape=jax.ShapeDtypeStruct(tokens.shape, bf),
        in_specs=[vmem] * 2 + [held] * 4 + [vmem, held, vmem] + [held] * 2 + [vmem] * 2 + [held] + [vmem] * 3,
        out_specs=vmem,
        scratch_shapes=[
            pltpu.VMEM((width, 2 * cq + 2 * cv), bf),
            pltpu.VMEM((cv, width), bf),
            pltpu.VMEM((width, 2 * cf), bf),
            pltpu.VMEM((cf, width), bf),
            pltpu.VMEM((groups * length, width), bf),
            pltpu.VMEM((groups * length, width), bf),
            pltpu.VMEM((groups * length, 2 * cq + 2 * cv), bf),
            pltpu.VMEM((groups * length, cv), bf),
            pltpu.VMEM((groups * length, cf), bf),
            pltpu.VMEM((CHUNKS, 2, groups, few, width), bf),
            pltpu.VMEM((CHUNKS, 2, groups, few, width), bf),
            pltpu.VMEM((CHUNKS, groups, few, width), bf),
            pltpu.VMEM((CHUNKS, groups, few, width), bf),
            pltpu.VMEM((CHUNKS, 2, groups, few, width), bf),
            pltpu.VMEM((CHUNKS, 2, groups, few, width), bf),
            pltpu.VMEM((CHUNKS, 2, groups, few, width), bf),
            pltpu.VMEM((CHUNKS, 2, groups, few, width), bf),
            pltpu.VMEM((CHUNKS, few, width), f32),
            pltpu.VMEM((CHUNKS, few, width), f32),
            pltpu.VMEM((CHUNKS, groups * span_c, 2 * cf), bf),
            pltpu.VMEM((CHUNKS, few, width), bf),
            pltpu.VMEM((CHUNKS, few, width), bf),
            dma((8, groups)),
            dma((8, groups)),
            dma((8,)),
            dma((classes, groups, 6)),
            dma((classes, groups, 6)),
            dma((NT_PARTS + CHUNKS, 2, groups)),
            dma((NT_PARTS + CHUNKS, 2, groups)),
            dma((NT_PARTS + CHUNKS, 2, groups)),
            dma((NT_PARTS + CHUNKS, 2, groups)),
            dma((2, CHUNKS)),
            dma((2, CHUNKS)),
            dma((2, CHUNKS, 2, groups)),
            dma((2, CHUNKS, 2, groups)),
            dma((CHUNKS,)),
            dma((CHUNKS,)),
        ],
        compiler_params=pltpu.CompilerParams(
            collective_id=0, has_side_effects=True, vmem_limit_bytes=60 * 1024 * 1024
        ),
    )(
        tokens, norm_gain[None], w_query, w_key, w_value, w_gate, mixer_gain[None], w_out,
        channel_gain[None], w_left, w_right, taps_left, taps_right, w_down,
        cos_t, sin_t, log_gammas(heads),
    )


def solution(mesh):
    placed = (
        P("fs", None),
        P(),
        P("fs", "tp"),
        P("fs", "tp"),
        P("fs", "tp"),
        P("fs", "tp"),
        P("tp"),
        P("tp", "fs"),
        P(),
        P("fs", "tp"),
        P("fs", "tp"),
        P(None, "tp"),
        P(None, "tp"),
        P("tp", "fs"),
    )
    return jax.shard_map(
        functools.partial(body, mesh.shape["fs"]), mesh=mesh, in_specs=placed, out_specs=P("fs", None), check_vma=False)
```

time: 159 us -> 131 us (0.82); the launches traced: 157 us -> 131 us
  Pallas kernels: 155 us -> 129 us
    pallas_call x1, Pallas kernels: 155 us -> 129 us  [body(): pl.pallas_call(functools.partial(layer_kernel, n_fs, groups), out_shape=j...]
where the time goes in v1:
time: 131 us
  Pallas kernels  129 us (98%)
  local copies, waits for them, and re-layouts  1.88 us (1%)
    pallas_call x1, Pallas kernels, body(): pl.pallas_call(functools.partial(layer_kernel, n_fs, groups), out_shape=j...  129 us

profile of v1, /device:TPU:0, one launch (start us, length us, event | category | flops | bytes accessed | tf_op | source)
XLA Modules:
  0.0 130.6 jit_solution(17653264694786820633)
XLA Ops:
  0.0 128.7 %shard_map.163 = bf16[128,2048]{1,0:T(8,128)(2,1)} custom-call(bf16[128,2048]{1,0:T(8,128)(2,1)} %tokens.1, f32[1,2048]{1,0:T(1,128)} %bitcast.3, bf16[128,512]{1,0:T(8,128)(2,1)} %wq.1, bf16[128,512]{1,0:T(8,128)(2,1)} %wk.1, bf16[128,1024]{1,0:T(8,128)(2,1)} %wv.1, bf16[128,1024]{1,0:T(8,128)(2,1)} %wg.1, f32[1,1024]{1,0:T(1,128)} %bitcast.5, ...), custom_call_target="tpu_custom_call" | custom-call | tf_op jit(solution)/shard_map/pallas_call | solution.py:915
  128.7 1.9 %copy.19 = bf16[128,2048]{1,0:T(8,128)(2,1)} copy(bf16[128,2048]{1,0:T(8,128)(2,1)} %shard_map.163) | data formatting | bytes 1048576

commit v2 on v1

v2 whole, which is shorter than its diff:
```python
import functools

import jax
import jax.numpy as jnp
import numpy as np
from jax import lax
from jax.experimental import pallas as pl
from jax.experimental.pallas import tpu as pltpu
from jax.sharding import PartitionSpec as P

DK = 128
DV = 256
BLOCK = 128
MESH = pl.DeviceIdType.MESH


highest = lax.Precision.HIGHEST


def scale_rows(rows_in, gain_vec):
    floats = rows_in.astype(jnp.float32)
    factor = lax.rsqrt(jnp.mean(floats * floats, axis=-1, keepdims=True) + 1e-06)
    return (floats * factor * gain_vec).astype(jnp.bfloat16)


def decays(first_head, count):
    head_ids = first_head + jnp.arange(count, dtype=jnp.float32)
    return jnp.log(1.0 - 2.0 ** (-5.0 - head_ids))


def rotate(heads_in, positions):
    width = heads_in.shape[-1]
    half = width // 2
    freqs = 10000.0 ** (-jnp.arange(half, dtype=jnp.float32) / half)
    angles = positions[:, None] * freqs[None, :]
    cosine = jnp.cos(angles)
    sine = jnp.sin(angles)
    first_half = heads_in[..., :half]
    second_half = heads_in[..., half:]
    return jnp.concatenate(
        [first_half * cosine - second_half * sine, first_half * sine + second_half * cosine],
        axis=-1,
    )


def retention(queries, keys_in, values_in, log_gamma):
    head_count, length, key_width = queries.shape
    value_width = values_in.shape[-1]
    blocks = length // BLOCK
    queries = queries.reshape(head_count, blocks, BLOCK, key_width)
    keys_in = keys_in.reshape(head_count, blocks, BLOCK, key_width)
    values_in = values_in.reshape(head_count, blocks, BLOCK, value_width)
    offsets = jnp.arange(BLOCK, dtype=jnp.float32)
    distance = offsets[:, None] - offsets[None, :]
    weights = jnp.where(
        distance >= 0, jnp.exp(log_gamma[:, None, None] * jnp.maximum(distance, 0.0)), 0.0
    )
    scores = jnp.einsum("hbnd,hbmd->hbnm", queries, keys_in, precision=highest) * weights[:, None]
    inner = jnp.einsum("hbnm,hbme->hbne", scores, values_in, precision=highest)
    key_weight = jnp.exp(log_gamma[:, None] * (BLOCK - 1 - offsets)[None, :])
    contrib = jnp.einsum(
        "hbjd,hbje->hbde", keys_in * key_weight[:, None, :, None], values_in, precision=highest
    )
    block_decay = jnp.exp(log_gamma * BLOCK)[:, None, None]

    def advance(state, contrib_block):
        return (state * block_decay + contrib_block, state)

    _, states = lax.scan(
        advance,
        jnp.zeros((head_count, key_width, value_width), jnp.float32),
        jnp.moveaxis(contrib, 1, 0),
    )
    states = jnp.moveaxis(states, 0, 1)
    query_weight = jnp.exp(log_gamma[:, None] * (offsets + 1.0)[None, :])
    carried = (
        jnp.einsum("hbnd,hbde->hbne", queries, states, precision=highest)
        * query_weight[:, None, :, None]
    )
    return (inner + carried).reshape(head_count, length, value_width)


def head_norm(retained):
    return retained * lax.rsqrt(jnp.mean(retained * retained, axis=-1, keepdims=True) + 1e-06)


def causal_taps(values_in, taps):
    length = values_in.shape[-2]
    padded = jnp.pad(values_in.astype(jnp.float32), ((taps.shape[0] - 1, 0), (0, 0)))
    result = padded[0:length] * taps[0]
    for tap_index in range(1, taps.shape[0]):
        result = result + padded[tap_index : tap_index + length] * taps[tap_index]
    return result


def fold_single(source, weight_piece):
    return jnp.dot(source, weight_piece, preferred_element_type=jnp.float32)


def collect_single(source, weight):
    return fold_single(source, lax.all_gather(weight, "fs", axis=0, tiled=True))


def plain_body(
    tokens,
    norm_gain,
    w_query,
    w_key,
    w_value,
    w_gate,
    mixer_gain,
    w_out,
    channel_gain,
    w_left,
    w_right,
    taps_left,
    taps_right,
    w_down,
):
    length = tokens.shape[0]
    normed = scale_rows(tokens, norm_gain)
    queries = collect_single(normed, w_query)
    keys_proj = collect_single(normed, w_key)
    values_proj = collect_single(normed, w_value)
    gates = collect_single(normed, w_gate)
    queries = queries.astype(jnp.bfloat16)
    keys_proj = keys_proj.astype(jnp.bfloat16)
    values_proj = values_proj.astype(jnp.bfloat16)
    gates = gates.astype(jnp.bfloat16)
    heads_here = w_query.shape[1] // DK
    first_head = (lax.axis_index("tp") * heads_here).astype(jnp.float32)
    log_gamma = decays(first_head, heads_here)
    positions = jnp.arange(length, dtype=jnp.float32)

    def split_heads(rows_in, width):
        return rows_in.astype(jnp.float32).reshape(length, heads_here, width).transpose(1, 0, 2)

    retained = head_norm(
        retention(
            rotate(split_heads(queries, DK), positions),
            rotate(split_heads(keys_proj, DK), positions),
            split_heads(values_proj, DV),
            log_gamma,
        )
    )
    retained = retained.transpose(1, 0, 2).reshape(length, heads_here * DV)
    hidden = (retained * mixer_gain * jax.nn.silu(gates.astype(jnp.float32))).astype(jnp.bfloat16)
    rows_own = length // lax.axis_size("tp")
    first_row = lax.axis_index("tp") * rows_own
    out_whole = lax.all_gather(w_out, "fs", axis=1, tiled=True)
    mixer_total = lax.psum_scatter(
        jnp.dot(hidden, out_whole, preferred_element_type=jnp.float32).astype(jnp.bfloat16),
        "tp",
        scatter_dimension=0,
        tiled=True,
    ).astype(jnp.float32)
    residual = lax.dynamic_slice_in_dim(tokens, first_row, rows_own, 0)
    middle_own = (residual.astype(jnp.float32) + mixer_total).astype(jnp.bfloat16)
    middle = lax.all_gather(middle_own, "tp", axis=0, tiled=True)
    normed_mid = scale_rows(middle, channel_gain)
    left = collect_single(normed_mid, w_left)
    right = collect_single(normed_mid, w_right)
    left = left.astype(jnp.bfloat16)
    right = right.astype(jnp.bfloat16)
    gated = (jax.nn.silu(causal_taps(left, taps_left)) * causal_taps(right, taps_right)).astype(
        jnp.bfloat16
    )
    down_whole = lax.all_gather(w_down, "fs", axis=1, tiled=True)
    channel_part = jnp.dot(gated, down_whole, preferred_element_type=jnp.float32)
    channel_total = lax.psum(channel_part.astype(jnp.bfloat16), "tp").astype(jnp.float32)
    return (middle.astype(jnp.float32) + channel_total).astype(jnp.bfloat16)


def log_gammas(head_count):
    table = np.log(1.0 - 2.0 ** (-5.0 - np.arange(head_count, dtype=np.float64)))
    return np.repeat(table[:, None], BLOCK, axis=1).astype(np.float32)


def turning(length, width):
    half = width // 2
    freqs = np.float32(10000.0) ** (-np.arange(half, dtype=np.float32) / np.float32(half))
    angles = (np.arange(length, dtype=np.float32)[:, None] * freqs[None, :]).astype(np.float64)
    cosine, sine = np.cos(angles), np.sin(angles)
    return (
        np.concatenate([cosine, cosine], axis=1).astype(np.float32),
        np.concatenate([-sine, sine], axis=1).astype(np.float32),
    )


def silu(v):
    return v / (1.0 + jnp.exp(-v))


def normed_rows(floats, gain):
    factor = lax.rsqrt(jnp.mean(floats * floats, axis=-1, keepdims=True) + 1e-06)
    return (floats * factor * gain).astype(jnp.bfloat16)


HOP, SUM, SWAP, WEIGHTS, HOPS, CORES = 3, 4, 5, 6, 7, 8
CHUNKS = 4
NT_PARTS = 2
CLASS_OF = (0, 0, 0, 1, 2, 3, 4, 5)
STAGES = (
    (7, 0),
    (0, 0),
    (0, 1),
    (1, 0),
    (1, 1),
    (2, 0),
    (2, 1),
    (2, 2),
    (2, 3),
    (3, 0),
    (3, 1),
    (3, 2),
    (3, 3),
    (4, 0),
    (5, 0),
    (4, 1),
    (5, 1),
    (4, 2),
    (5, 2),
    (4, 3),
    (5, 3),
    (6, 0),
    (6, 1),
    (6, 2),
    (6, 3),
)
PLAN = (
    (
        (
            (1, 3, 1, 0, 0), (1, 3, 1, 0, 3), (1, 3, 1, 0, 2), (1, 3, 1, 0, 1), (1, 3, 0, 0, 0), (1, 3, 0, 0, 1),
        ),
        (
            (1, 2, 2, 3), (1, 3, 0, 0, 3), (1, 0, 0, 0, 0, 0), (1, 3, 4, 0, 0), (1, 3, 4, 0, 1), (0, 3, 0, 0, 0),
            (0, 3, 1, 0, 1), (1, 3, 1, 0, 5), (0, 3, 0, 0, 1), (1, 0, 0, 1, 0, 0), (1, 3, 0, 0, 2), (1, 3, 4, 0, 3),
            (1, 3, 0, 0, 4), (0, 3, 1, 0, 0), (1, 3, 1, 0, 4), (1, 3, 2, 0, 0), (1, 3, 3, 0, 0), (0, 0, 0, 0, 1, 1),
            (1, 3, 2, 0, 1), (1, 1, 0, 0, 0, 0), (1, 3, 2, 0, 3), (1, 3, 3, 0, 1), (1, 3, 4, 0, 2),
            (1, 1, 0, 0, 1, 1), (0, 3, 2, 0, 0), (1, 2, 2, 1), (0, 3, 2, 0, 1), (1, 1, 0, 1, 0, 0), (1, 3, 5, 0, 0),
            (1, 2, 2, 2), (1, 3, 5, 0, 2), (0, 3, 4, 0, 1), (1, 3, 3, 0, 3), (1, 2, 1, 3), (0, 0, 0, 0, 1, 2),
            (0, 3, 3, 0, 1), (1, 3, 2, 0, 4), (1, 2, 3, 3), (1, 1, 0, 0, 1, 2), (0, 3, 3, 0, 0), (0, 3, 4, 0, 0),
            (1, 3, 0, 0, 5), (1, 2, 0, 3), (0, 0, 0, 1, 1, 1), (0, 3, 5, 0, 0), (1, 3, 5, 0, 1), (1, 3, 3, 0, 5),
            (0, 3, 5, 0, 1), (1, 3, 3, 0, 4), (1, 3, 5, 0, 3), (0, 0, 0, 1, 1, 2), (1, 3, 4, 0, 5),
            (1, 1, 0, 1, 1, 1), (1, 3, 5, 0, 5), (1, 2, 3, 1), (1, 3, 5, 0, 4), (1, 3, 4, 0, 4), (0, 6, 1, 3),
            (1, 3, 1, 3, 1), (1, 3, 1, 3, 2), (1, 2, 4, 3), (1, 3, 1, 3, 3), (1, 3, 1, 3, 0), (1, 1, 0, 1, 1, 2),
            (0, 6, 0, 3), (1, 3, 0, 3, 0), (1, 2, 1, 1), (1, 3, 3, 0, 2), (1, 3, 0, 3, 2), (1, 3, 0, 3, 1),
            (0, 0, 0, 0, 1, 3), (0, 3, 1, 3, 0), (0, 3, 1, 3, 1), (1, 3, 1, 3, 5), (1, 3, 0, 3, 3), (1, 3, 1, 3, 4),
            (1, 2, 0, 1), (1, 1, 0, 0, 1, 3), (1, 2, 4, 1), (0, 3, 0, 3, 0), (1, 3, 0, 3, 4), (1, 2, 1, 2),
            (1, 2, 3, 2), (0, 3, 0, 3, 1), (1, 3, 0, 3, 5), (0, 6, 2, 3), (1, 3, 2, 3, 1), (1, 3, 2, 3, 0),
            (0, 0, 0, 1, 1, 3), (1, 1, 0, 1, 1, 3), (1, 3, 2, 3, 2), (1, 3, 2, 0, 2), (1, 3, 2, 3, 3), (0, 6, 1, 1),
            (1, 3, 1, 1, 2), (1, 3, 1, 1, 1), (1, 3, 1, 1, 3), (1, 3, 1, 1, 0), (0, 3, 2, 3, 1), (1, 3, 2, 3, 5),
            (1, 2, 0, 2), (0, 6, 0, 1), (1, 3, 0, 1, 0), (1, 2, 4, 2), (1, 3, 0, 1, 2), (1, 3, 0, 1, 1),
            (1, 3, 0, 1, 3), (0, 3, 1, 1, 1), (0, 3, 1, 1, 0), (1, 3, 1, 1, 4), (1, 3, 1, 1, 5), (0, 6, 2, 1),
            (0, 3, 0, 1, 0), (0, 6, 1, 2), (1, 2, 7, 3), (0, 3, 0, 1, 1), (1, 2, 5, 3), (0, 3, 2, 3, 0),
            (1, 3, 0, 1, 5), (1, 3, 0, 1, 4), (0, 6, 0, 2), (1, 3, 0, 2, 0), (1, 3, 0, 2, 1), (1, 3, 0, 2, 3),
            (1, 3, 0, 2, 2), (1, 2, 5, 1), (1, 3, 1, 2, 0), (1, 3, 1, 2, 1), (0, 6, 2, 2), (0, 6, 5, 1),
            (0, 3, 0, 2, 1), (1, 3, 1, 2, 3), (0, 3, 0, 2, 0), (1, 3, 0, 2, 5), (1, 3, 0, 2, 4), (1, 3, 1, 2, 2),
            (0, 3, 1, 2, 0), (0, 3, 1, 2, 1), (1, 3, 1, 2, 5), (1, 3, 1, 2, 4), (1, 3, 2, 1, 1), (0, 6, 5, 3),
            (1, 3, 2, 1, 0), (1, 3, 2, 0, 5), (1, 3, 2, 3, 4), (1, 3, 2, 2, 1), (1, 3, 2, 2, 0), (1, 2, 7, 1),
            (0, 6, 3, 1), (1, 3, 2, 1, 3), (1, 3, 3, 1, 0), (1, 3, 2, 2, 3), (0, 8, 0, 0), (0, 7, 0), (0, 7, 1),
        ),
        (
            (0, 3, 2, 1, 0), (1, 3, 2, 2, 2), (1, 3, 3, 1, 1), (0, 3, 2, 1, 1), (1, 3, 2, 1, 5),
        ),
        (
            (1, 3, 2, 1, 4), (1, 2, 5, 2),
        ),
        (
            (0, 6, 3, 2), (0, 6, 3, 3), (0, 3, 2, 2, 1), (1, 2, 7, 2), (1, 3, 2, 1, 2), (1, 3, 2, 2, 5),
            (0, 3, 2, 2, 0), (1, 3, 3, 3, 0), (1, 3, 2, 2, 4), (1, 3, 3, 3, 1), (1, 3, 3, 1, 3), (1, 3, 5, 3, 2),
        ),
        (
            (0, 6, 5, 2), (0, 3, 3, 1, 1), (0, 3, 3, 1, 0), (1, 3, 3, 2, 3), (1, 3, 3, 2, 0), (1, 3, 3, 2, 1),
            (1, 3, 3, 1, 4), (1, 3, 5, 2, 2), (1, 3, 3, 1, 5), (1, 2, 6, 3), (0, 7, 2),
        ),
        (
            (1, 3, 3, 3, 3), (0, 3, 3, 3, 0),
        ),
        (
        ),
        (
            (1, 3, 3, 3, 4),
        ),
        (
            (0, 5, 0, 0), (1, 3, 5, 1, 1), (0, 3, 3, 3, 1), (1, 3, 3, 3, 5), (1, 4, 0, 0, 0, 3), (1, 4, 0, 0, 0, 2),
            (0, 3, 3, 2, 1), (1, 3, 5, 1, 0), (0, 5, 0, 3), (1, 3, 5, 1, 3), (0, 3, 3, 2, 0), (1, 4, 0, 0, 0, 1),
            (0, 6, 4, 3), (1, 3, 4, 3, 2), (1, 3, 4, 3, 0), (1, 3, 4, 3, 1), (1, 4, 0, 3, 0, 3), (1, 3, 4, 3, 3),
            (0, 3, 5, 1, 1), (1, 4, 0, 3, 0, 2), (0, 6, 4, 1), (1, 3, 4, 1, 2), (1, 3, 4, 1, 1), (1, 3, 4, 1, 0),
            (1, 4, 0, 3, 0, 1), (0, 3, 4, 3, 0), (0, 6, 4, 2), (1, 3, 4, 2, 2), (1, 3, 4, 2, 1), (1, 3, 4, 2, 3),
            (1, 3, 4, 2, 0), (1, 3, 4, 1, 3), (1, 3, 5, 3, 1), (1, 3, 5, 3, 0), (0, 5, 0, 1), (1, 3, 5, 2, 1),
            (1, 4, 0, 1, 0, 3), (1, 3, 3, 3, 2), (0, 5, 0, 2), (0, 3, 4, 3, 1), (1, 3, 5, 1, 2), (0, 3, 4, 1, 0),
            (1, 3, 4, 1, 4), (1, 4, 0, 1, 0, 2), (0, 3, 4, 1, 1), (1, 4, 0, 1, 0, 1), (1, 3, 4, 3, 5),
            (1, 3, 4, 1, 5), (0, 3, 4, 2, 1), (1, 3, 4, 2, 5), (1, 3, 3, 1, 2), (1, 4, 0, 2, 0, 3), (0, 3, 4, 2, 0),
            (1, 3, 4, 2, 4), (1, 3, 5, 2, 0), (0, 4, 0, 0, 1, 0),
        ),
        (
            (0, 0, 1, 0, 1, 1), (1, 3, 4, 3, 4), (1, 4, 0, 2, 0, 2), (1, 3, 3, 2, 2), (1, 3, 5, 1, 5),
            (1, 3, 3, 2, 5), (1, 4, 0, 2, 0, 1), (1, 3, 3, 2, 4), (1, 1, 1, 0, 1, 1), (1, 0, 1, 0, 0, 0),
            (0, 0, 1, 0, 1, 2), (1, 2, 6, 1), (0, 3, 5, 3, 1), (1, 3, 5, 3, 5), (0, 4, 0, 1, 1, 0), (1, 3, 5, 3, 3),
        ),
        (
            (0, 3, 5, 2, 1), (1, 0, 1, 1, 0, 0), (0, 3, 5, 1, 0), (1, 3, 5, 1, 4), (1, 3, 5, 2, 3), (0, 3, 5, 2, 0),
            (1, 1, 1, 0, 1, 2), (1, 3, 5, 2, 5), (0, 0, 1, 1, 1, 1), (1, 2, 6, 2), (0, 4, 0, 2, 1, 0),
            (1, 1, 1, 0, 0, 0), (0, 4, 0, 3, 1, 0),
        ),
        (
            (1, 1, 1, 1, 0, 0), (1, 1, 1, 1, 1, 1),
        ),
        (
            (0, 0, 1, 1, 1, 2), (1, 0, 1, 2, 0, 0), (1, 1, 1, 2, 0, 0), (1, 3, 5, 2, 4), (0, 3, 5, 3, 0),
            (1, 1, 1, 1, 1, 2), (0, 0, 1, 2, 1, 1), (1, 3, 5, 3, 4), (1, 0, 1, 3, 0, 0), (1, 1, 1, 2, 1, 1),
            (0, 0, 1, 0, 1, 3), (1, 1, 1, 0, 1, 3), (0, 0, 1, 3, 1, 1), (0, 8, 1, 0), (0, 7, 3), (0, 7, 4),
        ),
        (
            (0, 0, 1, 2, 1, 2), (1, 1, 1, 3, 0, 0), (0, 7, 5),
        ),
        (
            (0, 0, 1, 1, 1, 3), (1, 1, 1, 1, 1, 3), (0, 5, 1, 0), (1, 1, 1, 2, 1, 2), (1, 4, 1, 0, 0, 3),
            (0, 0, 1, 3, 1, 2), (0, 8, 1, 1),
        ),
        (
        ),
        (
            (1, 4, 1, 0, 0, 2), (0, 0, 1, 2, 1, 3), (1, 1, 1, 2, 1, 3), (1, 1, 1, 3, 1, 2), (1, 4, 1, 0, 0, 1),
            (1, 1, 1, 3, 1, 1), (0, 5, 1, 1), (0, 8, 1, 2),
        ),
        (
            (0, 0, 1, 3, 1, 3), (1, 4, 1, 1, 0, 3), (1, 1, 1, 3, 1, 3),
        ),
        (
            (1, 4, 1, 1, 0, 2), (0, 8, 1, 3),
        ),
        (
        ),
        (
            (0, 5, 1, 2), (1, 4, 1, 2, 0, 3), (0, 5, 1, 3), (1, 4, 1, 3, 0, 3), (1, 4, 1, 2, 0, 2),
            (0, 4, 1, 0, 1, 0), (1, 4, 1, 3, 0, 2), (1, 4, 1, 1, 0, 1),
        ),
        (
            (1, 4, 1, 2, 0, 1), (0, 4, 1, 1, 1, 0),
        ),
        (
            (1, 4, 1, 3, 0, 1), (0, 4, 1, 2, 1, 0),
        ),
        (
            (0, 4, 1, 3, 1, 0),
        ),
        (
        ),
    ),
    (
        (
            (1, 3, 0, 1, 0), (1, 2, 2, 0), (1, 3, 0, 1, 2), (1, 3, 0, 1, 3), (1, 3, 0, 1, 1), (1, 2, 2, 2),
            (1, 3, 1, 1, 0),
        ),
        (
            (1, 3, 1, 1, 2), (1, 1, 0, 0, 0, 0), (1, 3, 1, 1, 1), (1, 0, 0, 0, 1, 0), (1, 0, 0, 1, 1, 0),
            (1, 0, 0, 0, 0, 0), (0, 3, 0, 1, 0), (1, 3, 0, 1, 4), (0, 3, 0, 1, 1), (1, 3, 2, 1, 0), (1, 3, 0, 1, 5),
            (0, 3, 1, 1, 0), (1, 0, 0, 1, 0, 0), (1, 3, 2, 1, 2), (1, 3, 2, 1, 1), (1, 1, 0, 1, 0, 0),
            (1, 3, 2, 1, 3), (0, 0, 0, 0, 1, 1), (0, 3, 2, 1, 0), (0, 0, 0, 0, 0, 1), (1, 3, 3, 1, 0),
            (1, 0, 0, 0, 1, 1), (1, 3, 3, 1, 1), (1, 3, 5, 1, 0), (1, 3, 4, 1, 0), (1, 3, 4, 1, 2), (1, 3, 3, 1, 3),
            (1, 1, 0, 0, 0, 1), (0, 3, 1, 1, 1), (1, 0, 0, 0, 0, 1), (1, 1, 0, 0, 1, 1), (1, 3, 4, 1, 1),
            (0, 3, 2, 1, 1), (1, 3, 2, 1, 4), (1, 3, 4, 1, 3), (0, 0, 0, 1, 0, 1), (1, 1, 0, 1, 0, 1),
            (0, 3, 3, 1, 1), (0, 0, 0, 1, 1, 1), (1, 0, 0, 1, 1, 1), (0, 3, 4, 1, 1), (1, 3, 5, 1, 1),
            (1, 3, 5, 1, 2), (0, 0, 0, 0, 1, 2), (1, 3, 1, 1, 5), (1, 1, 0, 1, 1, 1), (1, 0, 0, 1, 0, 1),
            (0, 3, 3, 1, 0), (1, 2, 2, 3), (1, 3, 2, 1, 5), (1, 3, 1, 1, 4), (0, 3, 5, 1, 0), (1, 0, 0, 0, 1, 2),
            (1, 3, 4, 1, 5), (1, 3, 1, 1, 3), (0, 3, 5, 1, 1), (1, 3, 3, 1, 5), (1, 3, 3, 1, 2), (0, 3, 4, 1, 0),
            (0, 0, 0, 1, 1, 2), (1, 1, 0, 1, 1, 2), (1, 3, 5, 1, 5), (1, 3, 3, 1, 4), (1, 2, 3, 2), (1, 2, 1, 2),
            (1, 2, 0, 2), (1, 1, 0, 0, 1, 2), (1, 3, 4, 1, 4), (1, 3, 5, 1, 4), (1, 2, 4, 2), (1, 0, 0, 1, 1, 2),
            (1, 2, 1, 0), (1, 2, 3, 0), (0, 6, 1, 0), (1, 3, 1, 0, 1), (1, 2, 1, 3), (1, 3, 1, 0, 0), (0, 6, 0, 0),
            (1, 3, 0, 0, 0), (1, 3, 0, 0, 1), (0, 6, 0, 2), (1, 3, 0, 2, 3), (1, 3, 0, 2, 1), (1, 3, 0, 2, 2),
            (1, 3, 0, 2, 0), (1, 3, 0, 0, 3), (1, 3, 0, 0, 2), (1, 2, 0, 0), (1, 2, 3, 3), (0, 3, 1, 0, 1),
            (1, 2, 4, 0), (0, 3, 0, 0, 0), (0, 3, 0, 0, 1), (0, 3, 1, 0, 0), (1, 3, 0, 0, 5), (1, 2, 0, 3),
            (1, 2, 7, 0), (1, 2, 4, 3), (1, 3, 0, 0, 4), (0, 3, 0, 2, 0), (1, 3, 0, 2, 4), (0, 3, 0, 2, 1),
            (1, 3, 0, 2, 5), (0, 6, 2, 0), (1, 2, 5, 0), (1, 2, 7, 2), (0, 6, 1, 2), (0, 6, 0, 3), (1, 3, 0, 3, 1),
            (1, 2, 5, 2), (1, 3, 0, 3, 0), (1, 3, 0, 3, 2), (0, 6, 1, 3), (1, 3, 0, 3, 3), (0, 6, 2, 3),
            (1, 3, 1, 0, 5), (1, 3, 1, 0, 4), (0, 3, 0, 3, 1), (0, 3, 0, 3, 0), (1, 3, 0, 3, 4), (1, 3, 0, 3, 5),
            (1, 3, 1, 0, 3), (1, 3, 1, 0, 2), (1, 3, 1, 2, 0), (1, 3, 1, 2, 1), (1, 3, 1, 2, 2), (1, 3, 1, 2, 3),
            (1, 3, 1, 3, 0), (1, 2, 5, 3), (1, 3, 1, 3, 1), (1, 3, 1, 3, 3), (0, 6, 5, 2), (1, 3, 1, 3, 2),
            (1, 2, 7, 3), (0, 3, 1, 2, 0), (0, 3, 1, 2, 1), (1, 3, 1, 2, 4), (1, 3, 1, 2, 5), (1, 3, 2, 0, 0),
            (1, 3, 2, 0, 1), (0, 3, 1, 3, 0), (0, 6, 3, 2), (0, 3, 1, 3, 1), (1, 3, 1, 3, 5), (1, 3, 1, 3, 4),
            (1, 3, 2, 0, 3), (0, 6, 2, 2), (1, 3, 2, 2, 1), (1, 3, 2, 2, 2), (1, 3, 2, 2, 0), (1, 3, 5, 1, 3),
            (1, 3, 2, 0, 2), (1, 3, 2, 3, 0), (0, 3, 2, 0, 0), (0, 3, 2, 0, 1), (1, 3, 2, 3, 1), (1, 3, 2, 0, 4),
            (1, 3, 2, 3, 3), (1, 3, 2, 2, 3), (0, 8, 0, 0), (0, 7, 0), (0, 7, 1),
        ),
        (
        ),
        (
            (1, 3, 2, 0, 5), (0, 3, 2, 2, 1), (0, 3, 2, 2, 0), (1, 3, 2, 2, 4), (1, 3, 2, 3, 2), (1, 3, 2, 2, 5),
        ),
        (
            (1, 3, 3, 2, 0), (0, 3, 2, 3, 0), (0, 3, 2, 3, 1), (1, 3, 3, 2, 1),
        ),
        (
            (1, 3, 2, 3, 5), (1, 3, 2, 3, 4), (1, 3, 5, 2, 2), (1, 3, 3, 2, 3), (0, 6, 3, 0), (1, 3, 3, 0, 0),
            (1, 3, 3, 0, 1), (1, 3, 5, 2, 1), (1, 3, 5, 2, 0), (1, 2, 6, 2), (0, 3, 3, 2, 1), (0, 6, 3, 3),
            (1, 2, 6, 0), (0, 7, 2),
        ),
        (
            (1, 3, 3, 3, 1), (1, 3, 3, 3, 0),
        ),
        (
            (0, 3, 3, 2, 0),
        ),
        (
        ),
        (
            (1, 3, 3, 2, 5), (1, 2, 6, 3), (1, 3, 3, 3, 3), (0, 4, 0, 0, 0, 2), (1, 3, 3, 0, 2), (1, 3, 3, 0, 3),
            (0, 3, 3, 3, 1), (1, 3, 3, 3, 2), (1, 3, 5, 2, 3), (0, 5, 0, 0), (0, 5, 0, 3), (0, 3, 3, 0, 0),
            (0, 6, 4, 2), (0, 4, 0, 0, 0, 1), (1, 4, 0, 0, 0, 2), (1, 3, 4, 2, 0), (1, 4, 0, 0, 0, 1),
            (0, 4, 0, 0, 0, 0), (1, 3, 4, 2, 1), (0, 4, 0, 3, 0, 2), (1, 3, 4, 2, 2), (1, 4, 0, 3, 0, 2),
            (0, 3, 3, 3, 0), (0, 4, 0, 0, 1, 1), (1, 4, 0, 0, 1, 1), (0, 3, 5, 2, 1), (0, 4, 0, 3, 0, 1),
            (0, 5, 0, 1), (0, 3, 4, 2, 1), (0, 6, 5, 0), (0, 3, 4, 2, 0), (1, 3, 4, 2, 5), (1, 4, 0, 3, 0, 1),
            (1, 3, 5, 0, 0), (1, 3, 3, 2, 4), (0, 3, 3, 0, 1), (1, 3, 3, 0, 5), (0, 4, 0, 0, 1, 0),
        ),
        (
            (1, 0, 1, 0, 1, 0), (0, 4, 0, 3, 1, 1), (1, 3, 4, 2, 4), (1, 0, 1, 0, 0, 0), (1, 3, 5, 0, 1),
            (0, 4, 0, 1, 0, 2), (1, 4, 0, 1, 0, 2), (1, 3, 3, 2, 2), (0, 4, 0, 3, 0, 0), (1, 3, 5, 2, 5),
            (0, 6, 5, 3), (1, 3, 5, 3, 3), (1, 3, 5, 3, 0), (1, 3, 5, 3, 1), (1, 3, 3, 3, 5), (1, 4, 0, 3, 1, 1),
            (1, 3, 4, 2, 3), (0, 4, 0, 1, 0, 1), (1, 3, 5, 3, 2), (1, 3, 5, 0, 3), (0, 3, 5, 2, 0), (1, 3, 5, 2, 4),
            (1, 1, 1, 0, 0, 0), (1, 3, 3, 0, 4), (1, 4, 0, 1, 0, 1), (0, 0, 1, 0, 1, 1), (0, 5, 0, 2),
            (1, 0, 1, 0, 1, 1), (0, 3, 5, 0, 1), (0, 3, 5, 0, 0), (1, 3, 5, 0, 5), (0, 4, 0, 2, 0, 2),
            (0, 4, 0, 1, 1, 1), (0, 4, 0, 1, 0, 0), (1, 4, 0, 1, 1, 1), (1, 4, 0, 2, 0, 2), (0, 4, 0, 3, 1, 0),
            (1, 1, 1, 0, 1, 1), (0, 4, 0, 2, 0, 1), (0, 4, 0, 1, 1, 0),
        ),
        (
            (1, 0, 1, 1, 0, 0), (0, 3, 5, 3, 0), (1, 0, 1, 1, 1, 0), (0, 4, 0, 2, 0, 0), (1, 4, 0, 2, 0, 1),
            (0, 4, 0, 2, 1, 1), (0, 3, 5, 3, 1), (1, 3, 5, 3, 5), (1, 3, 5, 0, 4), (0, 0, 1, 0, 0, 1),
            (1, 0, 1, 0, 0, 1), (1, 4, 0, 2, 1, 1), (1, 3, 3, 3, 4), (0, 0, 1, 1, 1, 1), (1, 0, 1, 1, 1, 1),
            (0, 6, 4, 0), (1, 3, 4, 0, 1), (1, 3, 5, 0, 2), (1, 3, 4, 0, 0), (0, 4, 0, 2, 1, 0), (1, 1, 1, 0, 0, 1),
            (1, 3, 4, 0, 2),
        ),
        (
            (1, 3, 4, 0, 3),
        ),
        (
            (1, 1, 1, 1, 1, 1), (1, 1, 1, 3, 0, 0), (1, 0, 1, 2, 1, 0), (1, 0, 1, 2, 0, 0), (1, 0, 1, 3, 1, 0),
            (0, 0, 1, 0, 1, 2), (1, 1, 1, 0, 1, 2), (1, 3, 5, 3, 4), (0, 0, 1, 1, 0, 1), (1, 1, 1, 1, 0, 0),
            (1, 0, 1, 1, 0, 1), (1, 0, 1, 0, 1, 2), (0, 3, 4, 0, 1), (1, 3, 4, 0, 5), (1, 0, 1, 3, 0, 0),
            (0, 3, 4, 0, 0), (1, 3, 4, 0, 4), (0, 0, 1, 2, 1, 1), (1, 1, 1, 2, 0, 0), (1, 0, 1, 2, 1, 1),
            (0, 6, 4, 3), (1, 3, 4, 3, 1), (1, 3, 4, 3, 0), (1, 1, 1, 1, 0, 1), (0, 0, 1, 2, 0, 1),
            (1, 1, 1, 2, 1, 1), (0, 0, 1, 1, 1, 2), (1, 0, 1, 2, 0, 1), (1, 3, 4, 3, 2), (1, 3, 4, 3, 3),
            (1, 0, 1, 1, 1, 2), (0, 0, 1, 3, 1, 1), (0, 0, 1, 3, 0, 1), (1, 0, 1, 3, 0, 1), (1, 0, 1, 3, 1, 1),
            (0, 3, 4, 3, 0), (1, 1, 1, 3, 0, 1), (0, 3, 4, 3, 1), (1, 3, 4, 3, 4), (1, 3, 4, 3, 5),
            (0, 0, 1, 2, 1, 2), (1, 1, 1, 1, 1, 2), (1, 0, 1, 2, 1, 2), (0, 0, 1, 3, 1, 2), (1, 0, 1, 3, 1, 2),
            (1, 1, 1, 3, 1, 1), (1, 1, 1, 3, 1, 2), (0, 8, 1, 0), (0, 7, 3), (0, 7, 4),
        ),
        (
            (1, 1, 1, 2, 1, 2), (1, 1, 1, 2, 0, 1), (0, 7, 5),
        ),
        (
            (0, 8, 1, 1),
        ),
        (
        ),
        (
            (0, 5, 1, 0), (0, 4, 1, 0, 0, 2), (0, 8, 1, 2),
        ),
        (
            (1, 4, 1, 0, 0, 2), (0, 4, 1, 0, 0, 1),
        ),
        (
            (1, 4, 1, 0, 0, 1), (0, 8, 1, 3),
        ),
        (
            (0, 5, 1, 1),
        ),
        (
            (0, 4, 1, 0, 0, 0), (0, 4, 1, 0, 1, 1), (0, 4, 1, 1, 0, 2), (1, 4, 1, 0, 1, 1), (1, 4, 1, 1, 0, 2),
            (0, 4, 1, 0, 1, 0),
        ),
        (
            (0, 4, 1, 1, 0, 1), (1, 4, 1, 1, 0, 1), (0, 4, 1, 2, 0, 2), (0, 5, 1, 2), (0, 5, 1, 3),
            (1, 4, 1, 2, 0, 2), (0, 4, 1, 1, 1, 1), (1, 4, 1, 1, 1, 1), (0, 4, 1, 3, 0, 2), (1, 4, 1, 3, 0, 2),
            (0, 4, 1, 2, 0, 1), (0, 4, 1, 1, 1, 0), (1, 4, 1, 2, 0, 1), (0, 4, 1, 2, 1, 1), (1, 4, 1, 2, 1, 1),
            (0, 4, 1, 3, 0, 1), (1, 4, 1, 3, 0, 1), (0, 4, 1, 3, 1, 1), (1, 4, 1, 3, 1, 1), (0, 4, 1, 2, 0, 0),
            (0, 4, 1, 1, 0, 0), (0, 4, 1, 2, 1, 0),
        ),
        (
        ),
        (
            (0, 4, 1, 3, 0, 0), (0, 4, 1, 3, 1, 0),
        ),
        (
        ),
    ),
)

OWN_FIRST = {}
for at, ops in enumerate(PLAN):
    for op in (op for stage in ops for op in stage):
        if op[:2] == (1, HOP) and op[3] == at:
            OWN_FIRST.setdefault((op[2], at), op[4])


def layer_kernel(
    n_fs,
    groups,
    tokens_in,
    norm_gain_in,
    wq,
    wk,
    wv,
    wg,
    mixer_gain_in,
    wo,
    channel_gain_in,
    wl,
    wr,
    taps_left_in,
    taps_right_in,
    wd,
    cos_in,
    sin_in,
    gammas_in,
    out,
    tokens,
    norm_gain,
    mixer_gain,
    channel_gain,
    taps_left,
    taps_right,
    cos_t,
    sin_t,
    gammas,
    w1,
    wout,
    wlr,
    wdown,
    nt,
    nm,
    qkvg,
    hid,
    gated,
    part1,
    part2,
    xb1,
    xb2,
    sb1,
    sb2,
    rb1,
    rb2,
    mid,
    acc,
    both,
    fin,
    w_send,
    w_recv,
    self_sem,
    h_send,
    h_recv,
    h_rest,
    a_send,
    a_recv,
    f_send,
    f_recv,
    x_send,
    x_recv,
    r_send,
    r_recv,
    o_send,
    o_recv,
    load_sem,
    store_sem,
):
    fs, tp = lax.axis_index("fs"), lax.axis_index("tp")
    planes = n_fs // groups
    z, q = fs // planes, lax.rem(fs, planes)
    other = 1 - tp
    length, width = tokens_in.shape
    own = length // 2
    part_rows = own // NT_PARTS
    span_c = length // CHUNKS
    few = span_c // 2
    kb = wq.shape[0]
    nb = wo.shape[1]
    cq, cv, cf = wq.shape[1] // groups, wv.shape[1] // groups, wl.shape[1] // groups
    upper = z * 2 >= groups
    place_z = jnp.where(upper, groups - 1 - z, z)

    def real(plane):
        return jnp.where(upper, groups - 1 - plane, plane)

    def flip(side):
        return jnp.where(upper, 1 - side, side)

    def zdev(target):
        return {"fs": target * planes + q, "tp": tp}

    partner = {"fs": fs, "tp": other}

    def lanes(index, size):
        return pl.ds(pl.multiple_of(index * size, 128), size)

    def rows(index, size):
        return pl.ds(pl.multiple_of(index * size, size), size)

    pieces = (
        (lambda c: wq.at[:, lanes(c, cq)], lambda f: w1.at[rows(f, kb), pl.ds(0, cq)]),
        (lambda c: wk.at[:, lanes(c, cq)], lambda f: w1.at[rows(f, kb), pl.ds(cq, cq)]),
        (lambda c: wv.at[:, lanes(c, cv)], lambda f: w1.at[rows(f, kb), pl.ds(2 * cq, cv)]),
        (lambda c: wg.at[:, lanes(c, cv)], lambda f: w1.at[rows(f, kb), pl.ds(2 * cq + cv, cv)]),
        (lambda c: wo.at[rows(c, cv), :], lambda f: wout.at[:, lanes(f, nb)]),
        (lambda c: wl.at[:, lanes(c, cf)], lambda f: wlr.at[rows(f, kb), pl.ds(0, cf)]),
        (lambda c: wr.at[:, lanes(c, cf)], lambda f: wlr.at[rows(f, kb), pl.ds(cf, cf)]),
        (lambda c: wd.at[rows(c, cf), :], lambda f: wdown.at[:, lanes(f, nb)]),
    )
    starts = (0, cq, 2 * cq, 2 * cq + cv, 0, 0, cf, 0)
    widths = (cq, cq, cv, cv, 0, cf, cf, 0)

    def stretch(cls, first, count, half=None):
        members = [i for i in range(len(pieces)) if CLASS_OF[i] == cls]
        low = starts[members[0]]
        wide = sum(widths[i] for i in members)
        if members[0] == 4 or members[0] == 7:
            buf, size = (wout, cv) if members[0] == 4 else (wdown, cf)
            across = pl.ds(pl.multiple_of(first * nb, 128), count * nb)
            if half is None:
                return buf.at[:, across]
            return buf.at[pl.ds(half * (size // 2), size // 2), across]
        buf = w1 if members[0] < 4 else wlr
        if half is None:
            return buf.at[pl.ds(pl.multiple_of(first * kb, kb), count * kb), pl.ds(low, wide)]
        start = pl.multiple_of(first * kb + half * (kb // 2), kb // 2)
        return buf.at[pl.ds(start, kb // 2), pl.ds(low, wide)]

    barrier = pltpu.get_barrier_semaphore()
    for step in range(1, groups):
        pl.semaphore_signal(barrier, inc=1, device_id=zdev(lax.rem(z + step, groups)), device_id_type=MESH)
    qx = q + 1 - 2 * lax.rem(q, 2)
    qy = q + 2 - 4 * (q // 2)
    diagonal = planes - 1 - q
    to_x = {"fs": z * planes + qx, "tp": tp}
    to_y = {"fs": z * planes + qy, "tp": tp}
    for device in (to_x, to_y):
        pl.semaphore_signal(barrier, inc=1, device_id=device, device_id_type=MESH)
    pl.semaphore_signal(barrier, inc=1, device_id=partner, device_id_type=MESH)

    loads = []
    for i, (source, held_here) in enumerate((
        (tokens_in, tokens), (norm_gain_in, norm_gain), (mixer_gain_in, mixer_gain),
        (channel_gain_in, channel_gain), (taps_left_in, taps_left), (taps_right_in, taps_right),
        (cos_in, cos_t), (sin_in, sin_t), (gammas_in, gammas),
    )):
        load = pltpu.make_async_copy(source, held_here, load_sem.at[i])
        load.start()
        loads.append(load)
    keeps = []
    for i, (src, dst) in enumerate(pieces):
        keep = pltpu.make_async_copy(src(z), dst(fs), self_sem.at[i])
        keep.start()
        keeps.append(keep)

    def prepare(_):
        for load in loads:
            load.wait()
        my_half = pl.ds(pl.multiple_of(tp * own, own), own)
        nt[pl.ds(pl.multiple_of(z * length + tp * own, own), own), :] = normed_rows(
            tokens[my_half, :].astype(jnp.float32), norm_gain[...]
        )

    pl.semaphore_wait(barrier, groups - 1 + 2 + 1)

    def remote(src, dst, ssem, rsem, device):
        return pltpu.make_async_remote_copy(
            src_ref=src, dst_ref=dst, send_sem=ssem, recv_sem=rsem,
            device_id=device, device_id_type=MESH,
        )

    def block(key, c, seq, core):
        if key:
            first = c * groups * span_c + seq * span_c + core * few
            return nm.at[pl.ds(pl.multiple_of(first, few), few), :]
        first = seq * length + core * own + c * part_rows
        return nt.at[pl.ds(pl.multiple_of(first, part_rows), part_rows), :]

    part, xb, sb, rb = (part1, part2), (xb1, xb2), (sb1, sb2), (rb1, rb2)

    def pair(which, c, g):
        return part[which][c, tp, g].astype(jnp.float32) + xb[which][c, g].astype(jnp.float32)

    def exchange(which, c):
        return remote(part[which].at[c, other], xb[which].at[c], x_send.at[which], x_recv.at[which, c], partner)

    def gather_copy(me, key, c, side, d, landing=False):
        move = 1 - 2 * side
        source = real(me - move * d)
        ref = block(key, c, source, tp)
        at = c + key * NT_PARTS
        device = partner if landing else zdev(real(me + move))
        return remote(ref, ref, a_send.at[key], a_recv.at[at, source], device)

    def core_copy(me, key, c, side, d):
        move = 1 - 2 * side
        ref = block(key, c, real(me - move * d), tp)
        return remote(ref, ref, f_send.at[key], f_recv.at[key * (1 + c)], partner)

    def weight_copy(me, i, plane):
        src, dst = pieces[i]
        far = real(plane)
        return remote(src(far), dst(fs), w_send.at[i], w_recv.at[CLASS_OF[i], z], zdev(far))

    def hop_copy(me, cls, plane, slot, landing=False):
        origin = (qx, qy)[slot] if landing else (q, q, q, q, qx, qy)[slot]
        source = real(plane)
        ref = stretch(cls, source * planes + origin, 1, (0, 1, 1, 0, 0, 1)[slot])
        device = (to_x, to_y, to_x, to_y, to_y, to_x)[slot]
        landed = h_recv.at[cls, source, slot] if slot < 2 else h_rest.at[cls]
        return remote(ref, ref, h_send.at[cls], landed, device)

    def sum_copy(me, which, c, side, d, landing=False):
        ref = sb[which].at[c, flip(side), d]
        at = d if landing else d - 1
        device = partner if landing else zdev(real(me + 1 - 2 * side))
        return remote(ref, rb[which].at[c, flip(side), at], r_send.at[which], r_recv.at[which, c, flip(side), at], device)

    makers = (gather_copy, core_copy, weight_copy, hop_copy, sum_copy)

    def await_bytes(ref, sem):
        remote(ref, ref, sem, sem, partner).wait_recv()

    def act(me, op):
        sends, kind, args = op[0], op[1], op[2:]
        if not sends:
            if kind == SWAP:
                exchange(*args).wait_recv()
            elif kind == WEIGHTS:
                cls, far = args[0], real(args[1])
                await_bytes(stretch(cls, far * planes + q, 1), w_recv.at[cls, far])
            elif kind == HOPS:
                await_bytes(stretch(args[0], 0, 2 * groups), h_rest.at[args[0]])
            elif kind == CORES:
                key, c = args
                if key:
                    await_bytes(nm.at[pl.ds(0, groups * few), :], f_recv.at[1 + c])
                else:
                    await_bytes(nt.at[pl.ds(0, groups * own), :], f_recv.at[0])
            else:
                makers[kind](me, *args, True).wait_recv()
            return
        if kind == HOP and args[1] == me and args[2] == OWN_FIRST[args[0], me]:
            for i, keep in enumerate(keeps):
                if CLASS_OF[i] == args[0]:
                    keep.wait()
        if kind == SUM:
            which, c, side, d = args
            move = 1 - 2 * side
            value = pair(which, c, real(me + move * d))
            if 0 <= me - move < groups:
                value = value + rb[which][c, flip(side), d].astype(jnp.float32)
            sb[which][c, flip(side), d] = value.astype(jnp.bfloat16)
        makers[kind](me, *args).start()

    def perform(stage):
        for me, ops in enumerate(PLAN):
            @pl.when(place_z == me)
            def _():
                for op in ops[stage]:
                    act(me, op)

    def multiply(left, weight, which, c):
        value = jnp.dot(
            left[rows(c, groups * span_c), :], weight[...], preferred_element_type=jnp.float32
        ).astype(jnp.bfloat16)
        for g in range(groups):
            part[which][c, 0, g] = value[g * span_c : g * span_c + few]
            part[which][c, 1, g] = value[g * span_c + few : (g + 1) * span_c]
        exchange(which, c).start()

    def collect(which, c):
        acc[c] = pair(which, c, z)
        for side, has in ((0, z > 0), (1, z < groups - 1)):
            @pl.when(has)
            def _():
                acc[c] = acc[c] + rb[which][c, side, 0].astype(jnp.float32)
        return acc[c]

    def natural(c, core):
        return pl.ds(pl.multiple_of(c * span_c + core * few, few), few)

    head = tp * groups + z
    chunk = groups * length // 2

    def project(at):
        span = rows(at, chunk)
        qkvg[span, :] = jnp.dot(
            nt[span, :], w1[...], preferred_element_type=jnp.float32
        ).astype(jnp.bfloat16)

    def retain(first):
        log_gamma = gammas[pl.ds(head, 1), :]
        distance = (
            lax.broadcasted_iota(jnp.int32, (length, length), 0)
            - lax.broadcasted_iota(jnp.int32, (length, length), 1)
        ).astype(jnp.float32)
        decay = jnp.where(distance >= 0, jnp.exp(log_gamma * jnp.maximum(distance, 0.0)), 0.0)

        @pl.loop(first * groups // 2, (first + 1) * groups // 2)
        def _(at):
            span = rows(at, length)
            held = qkvg[span, :].astype(jnp.float32)

            def turn(x):
                return x * cos_t[...] + pltpu.roll(x, cq // 2, 1) * sin_t[...]

            rq = turn(held[:, :cq])
            rk = turn(held[:, cq : 2 * cq])
            scores = lax.dot_general(
                rq, rk, (((1,), (1,)), ((), ())), precision=highest, preferred_element_type=jnp.float32
            ) * decay
            kept = jnp.dot(
                scores, held[:, 2 * cq : 2 * cq + cv], precision=highest,
                preferred_element_type=jnp.float32,
            )
            kept = kept * lax.rsqrt(jnp.mean(kept * kept, axis=-1, keepdims=True) + 1e-06)
            gain = mixer_gain[:, lanes(z, cv)]
            whole = (kept * gain * silu(held[:, 2 * cq + cv :])).astype(jnp.bfloat16)
            for c in range(CHUNKS):
                hid[rows(at + c * groups, span_c), :] = whole[c * span_c : (c + 1) * span_c]

    def renorm(c):
        middle = (
            tokens[natural(c, tp), :].astype(jnp.float32) + collect(0, c)
        ).astype(jnp.bfloat16).astype(jnp.float32)
        mid[c] = middle
        first = c * groups * span_c + z * span_c + tp * few
        nm[pl.ds(pl.multiple_of(first, few), few), :] = normed_rows(middle, channel_gain[...])

    place = lax.rem(lax.broadcasted_iota(jnp.int32, (groups * span_c, 1), 0), span_c)

    def convolve(c, low, taps):
        x = both[c, :, low : low + cf].astype(jnp.float32)
        count = taps.shape[0]
        weights = taps[:, lanes(z, cf)]
        result = x * weights[count - 1 :, :]
        for back in range(1, count):
            if c:
                before = both[c - 1, :, low : low + cf].astype(jnp.float32)
                before = pltpu.roll(before, back + (groups - 1) * span_c, 0)
            else:
                before = 0.0
            moved = jnp.where(place >= back, pltpu.roll(x, back, 0), before)
            result = result + moved * weights[count - 1 - back : count - back, :]
        return result

    def mix(c):
        both[c] = jnp.dot(
            nm[rows(c, groups * span_c), :], wlr[...], preferred_element_type=jnp.float32
        ).astype(jnp.bfloat16)
        gated[rows(c, groups * span_c), :] = (
            silu(convolve(c, 0, taps_left)) * convolve(c, cf, taps_right)
        ).astype(jnp.bfloat16)

    def finish(c):
        mine = natural(c, tp)
        fin[c] = (mid[c] + collect(1, c)).astype(jnp.bfloat16)
        remote(fin.at[c], out.at[mine, :], o_send.at[0], o_recv.at[0], partner).start()
        pltpu.make_async_copy(fin.at[c], out.at[mine, :], store_sem.at[0]).start()

    steps = (
        project,
        retain,
        lambda c: multiply(hid, wout, 0, c),
        renorm,
        mix,
        lambda c: multiply(gated, wdown, 1, c),
        finish,
        prepare,
    )
    perform(0)
    for stage, (name, index) in enumerate(STAGES):
        steps[name](index)
        perform(stage + 1)
    await_bytes(fin, o_recv.at[0])
    await_bytes(fin, o_send.at[0])
    for key, buf in ((0, nt), (1, nm)):
        await_bytes(buf.at[pl.ds(0, groups * own), :], f_send.at[key])
        await_bytes(part[key].at[:, 0], x_send.at[key])
        await_bytes(sb[key].at[:, 0, pl.ds(0, groups - 1)], r_send.at[key])
    for cls in range(max(CLASS_OF) + 1):
        await_bytes(stretch(cls, 0, 3 * groups), h_send.at[cls])
    for i, (_, dst) in enumerate(pieces):
        if i == 4 or i == 7:
            ref = (wout if i == 4 else wdown).at[:, pl.ds(0, (groups - 1) * nb)]
        else:
            ref = (w1 if i < 4 else wlr).at[pl.ds(0, (groups - 1) * kb), pl.ds(starts[i], widths[i])]
        await_bytes(ref, w_send.at[i])
    for me, ops in enumerate(PLAN):
        @pl.when(place_z == me)
        def _():
            for key, buf, size in ((0, nt, part_rows), (1, nm, few)):
                count = sum(op[:3] == (1, 0, key) for stage in ops for op in stage)
                await_bytes(buf.at[pl.ds(0, count * size), :], a_send.at[key])
    pltpu.make_async_copy(fin, fin, store_sem.at[0]).wait()


def body(n_fs, *args):
    (tokens, norm_gain, w_query, w_key, w_value, w_gate, mixer_gain, w_out, channel_gain,
     w_left, w_right, taps_left, taps_right, w_down) = args
    groups = w_query.shape[1] // DK
    if (
        groups != 2 * len(PLAN)
        or n_fs % groups
        or n_fs != 4 * groups
        or lax.axis_size("tp") != 2
        or tokens.shape[0] != BLOCK
        or (w_left.shape[1] // groups) % 128
        or w_left.shape[1] % groups
        or w_out.shape[1] % 128
        or w_query.shape[0] % 32
        or tokens.shape[0] % (32 * CHUNKS)
    ):
        return plain_body(*args)
    length, width = tokens.shape
    heads = groups * lax.axis_size("tp")
    cq, cv, cf = w_query.shape[1] // groups, w_value.shape[1] // groups, w_left.shape[1] // groups
    planes = n_fs // groups
    span_c = length // CHUNKS
    few = span_c // 2
    classes = max(CLASS_OF) + 1
    cos_t, sin_t = turning(length, DK)
    gammas = log_gammas(heads)
    held = pl.BlockSpec(memory_space=pl.ANY)
    bf, f32, dma = jnp.bfloat16, jnp.float32, pltpu.SemaphoreType.DMA
    return pl.pallas_call(
        functools.partial(layer_kernel, n_fs, groups),
        out_shape=jax.ShapeDtypeStruct(tokens.shape, bf),
        in_specs=[held] * 17,
        out_specs=held,
        scratch_shapes=[
            pltpu.VMEM(tokens.shape, bf),
            pltpu.VMEM((1, width), f32),
            pltpu.VMEM((1, w_value.shape[1]), f32),
            pltpu.VMEM((1, width), f32),
            pltpu.VMEM(taps_left.shape, f32),
            pltpu.VMEM(taps_right.shape, f32),
            pltpu.VMEM(cos_t.shape, f32),
            pltpu.VMEM(sin_t.shape, f32),
            pltpu.VMEM(gammas.shape, f32),
            pltpu.VMEM((width, 2 * cq + 2 * cv), bf),
            pltpu.VMEM((cv, width), bf),
            pltpu.VMEM((width, 2 * cf), bf),
            pltpu.VMEM((cf, width), bf),
            pltpu.VMEM((groups * length, width), bf),
            pltpu.VMEM((groups * length, width), bf),
            pltpu.VMEM((groups * length, 2 * cq + 2 * cv), bf),
            pltpu.VMEM((groups * length, cv), bf),
            pltpu.VMEM((groups * length, cf), bf),
            pltpu.VMEM((CHUNKS, 2, groups, few, width), bf),
            pltpu.VMEM((CHUNKS, 2, groups, few, width), bf),
            pltpu.VMEM((CHUNKS, groups, few, width), bf),
            pltpu.VMEM((CHUNKS, groups, few, width), bf),
            pltpu.VMEM((CHUNKS, 2, groups, few, width), bf),
            pltpu.VMEM((CHUNKS, 2, groups, few, width), bf),
            pltpu.VMEM((CHUNKS, 2, groups, few, width), bf),
            pltpu.VMEM((CHUNKS, 2, groups, few, width), bf),
            pltpu.VMEM((CHUNKS, few, width), f32),
            pltpu.VMEM((CHUNKS, few, width), f32),
            pltpu.VMEM((CHUNKS, groups * span_c, 2 * cf), bf),
            pltpu.VMEM((CHUNKS, few, width), bf),
            dma((8,)),
            dma((classes, groups)),
            dma((8,)),
            dma((classes,)),
            dma((classes, groups, 2)),
            dma((classes,)),
            dma((2,)),
            dma((NT_PARTS + CHUNKS, groups)),
            dma((2,)),
            dma((1 + CHUNKS,)),
            dma((2,)),
            dma((2, CHUNKS)),
            dma((2,)),
            dma((2, CHUNKS, 2, groups - 1)),
            dma((1,)),
            dma((1,)),
            dma((9,)),
            dma((1,)),
        ],
        compiler_params=pltpu.CompilerParams(
            collective_id=0, has_side_effects=True, vmem_limit_bytes=60 * 1024 * 1024
        ),
    )(
        tokens, norm_gain[None], w_query, w_key, w_value, w_gate, mixer_gain[None], w_out,
        channel_gain[None], w_left, w_right, taps_left, taps_right, w_down,
        cos_t, sin_t, gammas,
    )


def solution(mesh):
    placed = (
        P("fs", None),
        P(),
        P("fs", "tp"),
        P("fs", "tp"),
        P("fs", "tp"),
        P("fs", "tp"),
        P("tp"),
        P("tp", "fs"),
        P(),
        P("fs", "tp"),
        P("fs", "tp"),
        P(None, "tp"),
        P(None, "tp"),
        P("tp", "fs"),
    )
    return jax.shard_map(
        functools.partial(body, mesh.shape["fs"]), mesh=mesh, in_specs=placed, out_specs=P("fs", None), check_vma=False)
```

time: 131 us -> 124 us (0.947)
  Pallas kernels: 129 us -> 122 us
    pallas_call x1, Pallas kernels: 129 us -> 122 us  [body(): pl.pallas_call(functools.partial(layer_kernel, n_fs, groups), out_shape=j...]
where the time goes in v2:
time: 124 us; the launch traced here: 123 us
  Pallas kernels  122 us (98%)
  local copies, waits for them, and re-layouts  1.88 us (2%)
    pallas_call x1, Pallas kernels, body(): pl.pallas_call(functools.partial(layer_kernel, n_fs, groups), out_shape=j...  122 us

profile of v2, /device:TPU:0, one launch (start us, length us, event | category | flops | bytes accessed | tf_op | source)
XLA Modules:
  0.0 123.4 jit_solution(7353498049415366302)
XLA Ops:
  0.0 121.5 %shard_map.163 = bf16[128,2048]{1,0:T(8,128)(2,1)} custom-call(bf16[128,2048]{1,0:T(8,128)(2,1)} %tokens_in.1, f32[1,2048]{1,0:T(1,128)} %bitcast.3, bf16[128,512]{1,0:T(8,128)(2,1)} %wq.1, bf16[128,512]{1,0:T(8,128)(2,1)} %wk.1, bf16[128,1024]{1,0:T(8,128)(2,1)} %wv.1, bf16[128,1024]{1,0:T(8,128)(2,1)} %wg.1, f32[1,1024]{1,0:T(1,128)} %bitcast.5, ...), custom_call_target="tpu_custom_call" | custom-call | tf_op jit(solution)/shard_map/pallas_call | solution.py:926
  121.5 1.9 %copy.19 = bf16[128,2048]{1,0:T(8,128)(2,1)} copy(bf16[128,2048]{1,0:T(8,128)(2,1)} %shard_map.163) | data formatting | bytes 1048576

commit v3 on v2

--- a/solution.py
+++ b/solution.py
@@ -230,118 +230,120 @@
 PLAN = (
     (
         (
-            (1, 3, 1, 0, 0), (1, 3, 1, 0, 3), (1, 3, 1, 0, 2), (1, 3, 1, 0, 1), (1, 3, 0, 0, 0), (1, 3, 0, 0, 1),
-        ),
-        (
-            (1, 2, 2, 3), (1, 3, 0, 0, 3), (1, 0, 0, 0, 0, 0), (1, 3, 4, 0, 0), (1, 3, 4, 0, 1), (0, 3, 0, 0, 0),
-            (0, 3, 1, 0, 1), (1, 3, 1, 0, 5), (0, 3, 0, 0, 1), (1, 0, 0, 1, 0, 0), (1, 3, 0, 0, 2), (1, 3, 4, 0, 3),
-            (1, 3, 0, 0, 4), (0, 3, 1, 0, 0), (1, 3, 1, 0, 4), (1, 3, 2, 0, 0), (1, 3, 3, 0, 0), (0, 0, 0, 0, 1, 1),
-            (1, 3, 2, 0, 1), (1, 1, 0, 0, 0, 0), (1, 3, 2, 0, 3), (1, 3, 3, 0, 1), (1, 3, 4, 0, 2),
-            (1, 1, 0, 0, 1, 1), (0, 3, 2, 0, 0), (1, 2, 2, 1), (0, 3, 2, 0, 1), (1, 1, 0, 1, 0, 0), (1, 3, 5, 0, 0),
-            (1, 2, 2, 2), (1, 3, 5, 0, 2), (0, 3, 4, 0, 1), (1, 3, 3, 0, 3), (1, 2, 1, 3), (0, 0, 0, 0, 1, 2),
-            (0, 3, 3, 0, 1), (1, 3, 2, 0, 4), (1, 2, 3, 3), (1, 1, 0, 0, 1, 2), (0, 3, 3, 0, 0), (0, 3, 4, 0, 0),
-            (1, 3, 0, 0, 5), (1, 2, 0, 3), (0, 0, 0, 1, 1, 1), (0, 3, 5, 0, 0), (1, 3, 5, 0, 1), (1, 3, 3, 0, 5),
-            (0, 3, 5, 0, 1), (1, 3, 3, 0, 4), (1, 3, 5, 0, 3), (0, 0, 0, 1, 1, 2), (1, 3, 4, 0, 5),
-            (1, 1, 0, 1, 1, 1), (1, 3, 5, 0, 5), (1, 2, 3, 1), (1, 3, 5, 0, 4), (1, 3, 4, 0, 4), (0, 6, 1, 3),
-            (1, 3, 1, 3, 1), (1, 3, 1, 3, 2), (1, 2, 4, 3), (1, 3, 1, 3, 3), (1, 3, 1, 3, 0), (1, 1, 0, 1, 1, 2),
-            (0, 6, 0, 3), (1, 3, 0, 3, 0), (1, 2, 1, 1), (1, 3, 3, 0, 2), (1, 3, 0, 3, 2), (1, 3, 0, 3, 1),
-            (0, 0, 0, 0, 1, 3), (0, 3, 1, 3, 0), (0, 3, 1, 3, 1), (1, 3, 1, 3, 5), (1, 3, 0, 3, 3), (1, 3, 1, 3, 4),
-            (1, 2, 0, 1), (1, 1, 0, 0, 1, 3), (1, 2, 4, 1), (0, 3, 0, 3, 0), (1, 3, 0, 3, 4), (1, 2, 1, 2),
-            (1, 2, 3, 2), (0, 3, 0, 3, 1), (1, 3, 0, 3, 5), (0, 6, 2, 3), (1, 3, 2, 3, 1), (1, 3, 2, 3, 0),
-            (0, 0, 0, 1, 1, 3), (1, 1, 0, 1, 1, 3), (1, 3, 2, 3, 2), (1, 3, 2, 0, 2), (1, 3, 2, 3, 3), (0, 6, 1, 1),
-            (1, 3, 1, 1, 2), (1, 3, 1, 1, 1), (1, 3, 1, 1, 3), (1, 3, 1, 1, 0), (0, 3, 2, 3, 1), (1, 3, 2, 3, 5),
-            (1, 2, 0, 2), (0, 6, 0, 1), (1, 3, 0, 1, 0), (1, 2, 4, 2), (1, 3, 0, 1, 2), (1, 3, 0, 1, 1),
-            (1, 3, 0, 1, 3), (0, 3, 1, 1, 1), (0, 3, 1, 1, 0), (1, 3, 1, 1, 4), (1, 3, 1, 1, 5), (0, 6, 2, 1),
-            (0, 3, 0, 1, 0), (0, 6, 1, 2), (1, 2, 7, 3), (0, 3, 0, 1, 1), (1, 2, 5, 3), (0, 3, 2, 3, 0),
-            (1, 3, 0, 1, 5), (1, 3, 0, 1, 4), (0, 6, 0, 2), (1, 3, 0, 2, 0), (1, 3, 0, 2, 1), (1, 3, 0, 2, 3),
-            (1, 3, 0, 2, 2), (1, 2, 5, 1), (1, 3, 1, 2, 0), (1, 3, 1, 2, 1), (0, 6, 2, 2), (0, 6, 5, 1),
-            (0, 3, 0, 2, 1), (1, 3, 1, 2, 3), (0, 3, 0, 2, 0), (1, 3, 0, 2, 5), (1, 3, 0, 2, 4), (1, 3, 1, 2, 2),
-            (0, 3, 1, 2, 0), (0, 3, 1, 2, 1), (1, 3, 1, 2, 5), (1, 3, 1, 2, 4), (1, 3, 2, 1, 1), (0, 6, 5, 3),
-            (1, 3, 2, 1, 0), (1, 3, 2, 0, 5), (1, 3, 2, 3, 4), (1, 3, 2, 2, 1), (1, 3, 2, 2, 0), (1, 2, 7, 1),
-            (0, 6, 3, 1), (1, 3, 2, 1, 3), (1, 3, 3, 1, 0), (1, 3, 2, 2, 3), (0, 8, 0, 0), (0, 7, 0), (0, 7, 1),
-        ),
-        (
-            (0, 3, 2, 1, 0), (1, 3, 2, 2, 2), (1, 3, 3, 1, 1), (0, 3, 2, 1, 1), (1, 3, 2, 1, 5),
-        ),
-        (
-            (1, 3, 2, 1, 4), (1, 2, 5, 2),
-        ),
-        (
-            (0, 6, 3, 2), (0, 6, 3, 3), (0, 3, 2, 2, 1), (1, 2, 7, 2), (1, 3, 2, 1, 2), (1, 3, 2, 2, 5),
-            (0, 3, 2, 2, 0), (1, 3, 3, 3, 0), (1, 3, 2, 2, 4), (1, 3, 3, 3, 1), (1, 3, 3, 1, 3), (1, 3, 5, 3, 2),
-        ),
-        (
-            (0, 6, 5, 2), (0, 3, 3, 1, 1), (0, 3, 3, 1, 0), (1, 3, 3, 2, 3), (1, 3, 3, 2, 0), (1, 3, 3, 2, 1),
-            (1, 3, 3, 1, 4), (1, 3, 5, 2, 2), (1, 3, 3, 1, 5), (1, 2, 6, 3), (0, 7, 2),
-        ),
-        (
-            (1, 3, 3, 3, 3), (0, 3, 3, 3, 0),
-        ),
-        (
-        ),
-        (
-            (1, 3, 3, 3, 4),
-        ),
-        (
-            (0, 5, 0, 0), (1, 3, 5, 1, 1), (0, 3, 3, 3, 1), (1, 3, 3, 3, 5), (1, 4, 0, 0, 0, 3), (1, 4, 0, 0, 0, 2),
-            (0, 3, 3, 2, 1), (1, 3, 5, 1, 0), (0, 5, 0, 3), (1, 3, 5, 1, 3), (0, 3, 3, 2, 0), (1, 4, 0, 0, 0, 1),
-            (0, 6, 4, 3), (1, 3, 4, 3, 2), (1, 3, 4, 3, 0), (1, 3, 4, 3, 1), (1, 4, 0, 3, 0, 3), (1, 3, 4, 3, 3),
-            (0, 3, 5, 1, 1), (1, 4, 0, 3, 0, 2), (0, 6, 4, 1), (1, 3, 4, 1, 2), (1, 3, 4, 1, 1), (1, 3, 4, 1, 0),
-            (1, 4, 0, 3, 0, 1), (0, 3, 4, 3, 0), (0, 6, 4, 2), (1, 3, 4, 2, 2), (1, 3, 4, 2, 1), (1, 3, 4, 2, 3),
-            (1, 3, 4, 2, 0), (1, 3, 4, 1, 3), (1, 3, 5, 3, 1), (1, 3, 5, 3, 0), (0, 5, 0, 1), (1, 3, 5, 2, 1),
-            (1, 4, 0, 1, 0, 3), (1, 3, 3, 3, 2), (0, 5, 0, 2), (0, 3, 4, 3, 1), (1, 3, 5, 1, 2), (0, 3, 4, 1, 0),
-            (1, 3, 4, 1, 4), (1, 4, 0, 1, 0, 2), (0, 3, 4, 1, 1), (1, 4, 0, 1, 0, 1), (1, 3, 4, 3, 5),
-            (1, 3, 4, 1, 5), (0, 3, 4, 2, 1), (1, 3, 4, 2, 5), (1, 3, 3, 1, 2), (1, 4, 0, 2, 0, 3), (0, 3, 4, 2, 0),
-            (1, 3, 4, 2, 4), (1, 3, 5, 2, 0), (0, 4, 0, 0, 1, 0),
-        ),
-        (
-            (0, 0, 1, 0, 1, 1), (1, 3, 4, 3, 4), (1, 4, 0, 2, 0, 2), (1, 3, 3, 2, 2), (1, 3, 5, 1, 5),
-            (1, 3, 3, 2, 5), (1, 4, 0, 2, 0, 1), (1, 3, 3, 2, 4), (1, 1, 1, 0, 1, 1), (1, 0, 1, 0, 0, 0),
-            (0, 0, 1, 0, 1, 2), (1, 2, 6, 1), (0, 3, 5, 3, 1), (1, 3, 5, 3, 5), (0, 4, 0, 1, 1, 0), (1, 3, 5, 3, 3),
-        ),
-        (
-            (0, 3, 5, 2, 1), (1, 0, 1, 1, 0, 0), (0, 3, 5, 1, 0), (1, 3, 5, 1, 4), (1, 3, 5, 2, 3), (0, 3, 5, 2, 0),
-            (1, 1, 1, 0, 1, 2), (1, 3, 5, 2, 5), (0, 0, 1, 1, 1, 1), (1, 2, 6, 2), (0, 4, 0, 2, 1, 0),
-            (1, 1, 1, 0, 0, 0), (0, 4, 0, 3, 1, 0),
-        ),
-        (
-            (1, 1, 1, 1, 0, 0), (1, 1, 1, 1, 1, 1),
-        ),
-        (
-            (0, 0, 1, 1, 1, 2), (1, 0, 1, 2, 0, 0), (1, 1, 1, 2, 0, 0), (1, 3, 5, 2, 4), (0, 3, 5, 3, 0),
-            (1, 1, 1, 1, 1, 2), (0, 0, 1, 2, 1, 1), (1, 3, 5, 3, 4), (1, 0, 1, 3, 0, 0), (1, 1, 1, 2, 1, 1),
-            (0, 0, 1, 0, 1, 3), (1, 1, 1, 0, 1, 3), (0, 0, 1, 3, 1, 1), (0, 8, 1, 0), (0, 7, 3), (0, 7, 4),
-        ),
-        (
-            (0, 0, 1, 2, 1, 2), (1, 1, 1, 3, 0, 0), (0, 7, 5),
-        ),
-        (
-            (0, 0, 1, 1, 1, 3), (1, 1, 1, 1, 1, 3), (0, 5, 1, 0), (1, 1, 1, 2, 1, 2), (1, 4, 1, 0, 0, 3),
-            (0, 0, 1, 3, 1, 2), (0, 8, 1, 1),
-        ),
-        (
-        ),
-        (
-            (1, 4, 1, 0, 0, 2), (0, 0, 1, 2, 1, 3), (1, 1, 1, 2, 1, 3), (1, 1, 1, 3, 1, 2), (1, 4, 1, 0, 0, 1),
-            (1, 1, 1, 3, 1, 1), (0, 5, 1, 1), (0, 8, 1, 2),
-        ),
-        (
-            (0, 0, 1, 3, 1, 3), (1, 4, 1, 1, 0, 3), (1, 1, 1, 3, 1, 3),
-        ),
-        (
-            (1, 4, 1, 1, 0, 2), (0, 8, 1, 3),
+            (1, 2, 0, 3), (1, 2, 3, 1), (1, 2, 3, 3), (1, 3, 4, 0, 0),
+        ),
+        (
+            (1, 3, 0, 0, 0), (0, 6, 1, 1), (1, 3, 1, 1, 1), (1, 3, 1, 1, 3), (1, 3, 1, 1, 2), (1, 3, 3, 0, 0),
+            (1, 3, 1, 1, 0), (1, 2, 2, 3), (1, 2, 1, 3), (1, 3, 3, 0, 1), (1, 3, 0, 0, 2), (1, 3, 1, 0, 0),
+            (1, 3, 1, 0, 1), (1, 3, 1, 0, 3), (0, 6, 1, 3), (1, 3, 1, 3, 3), (1, 3, 1, 3, 2), (1, 3, 0, 0, 1),
+            (1, 0, 0, 0, 0, 0), (1, 0, 0, 1, 0, 0), (0, 3, 0, 0, 0), (1, 3, 5, 0, 0), (1, 3, 5, 0, 1),
+            (1, 3, 1, 3, 0), (1, 3, 4, 0, 1), (0, 6, 0, 1), (1, 3, 0, 1, 2), (1, 3, 0, 1, 0), (1, 3, 0, 1, 3),
+            (1, 3, 0, 1, 1), (1, 2, 0, 1), (1, 3, 0, 0, 3), (1, 3, 1, 3, 1), (0, 3, 1, 1, 1), (1, 3, 1, 1, 5),
+            (0, 6, 2, 1), (0, 3, 3, 0, 1), (1, 3, 2, 1, 0), (1, 3, 2, 1, 3), (1, 3, 2, 1, 2), (1, 3, 1, 0, 2),
+            (0, 6, 0, 3), (1, 3, 2, 0, 0), (1, 3, 0, 3, 3), (1, 3, 0, 3, 1), (1, 3, 2, 1, 1), (1, 2, 1, 1),
+            (1, 2, 4, 3), (1, 3, 0, 3, 0), (0, 3, 0, 0, 1), (1, 3, 0, 3, 2), (1, 3, 2, 0, 2), (1, 2, 2, 1),
+            (1, 3, 0, 0, 5), (0, 3, 0, 1, 0), (1, 3, 0, 1, 4), (1, 2, 3, 2), (1, 2, 4, 1), (0, 6, 2, 3),
+            (0, 3, 1, 3, 1), (1, 3, 1, 3, 5), (1, 3, 2, 3, 1), (1, 2, 0, 2), (0, 6, 1, 2), (1, 3, 1, 2, 2),
+            (1, 3, 0, 0, 4), (1, 3, 2, 3, 3), (0, 6, 5, 1), (1, 3, 2, 3, 0), (1, 3, 1, 2, 1), (1, 3, 1, 2, 3),
+            (0, 3, 0, 1, 1), (1, 3, 0, 1, 5), (0, 3, 0, 3, 1), (1, 3, 1, 2, 0), (0, 0, 0, 0, 1, 1),
+            (1, 1, 0, 0, 1, 1), (0, 3, 1, 3, 0), (0, 3, 0, 3, 0), (1, 3, 2, 0, 1), (1, 2, 1, 2), (1, 1, 0, 1, 0, 0),
+            (0, 6, 3, 1), (1, 3, 3, 1, 2), (1, 3, 3, 1, 1), (1, 3, 3, 0, 3), (1, 3, 1, 3, 4), (1, 3, 0, 3, 4),
+            (1, 3, 0, 3, 5), (1, 1, 0, 0, 0, 0), (0, 3, 5, 0, 1), (1, 3, 5, 0, 5), (0, 6, 4, 1), (1, 3, 4, 1, 0),
+            (1, 3, 4, 1, 1), (1, 2, 2, 2), (1, 3, 3, 0, 2), (1, 2, 4, 2), (1, 2, 5, 2), (0, 3, 1, 2, 0),
+            (0, 3, 2, 0, 0), (1, 3, 3, 1, 0), (0, 3, 1, 1, 0), (1, 3, 1, 1, 4), (1, 3, 5, 1, 1), (0, 3, 1, 0, 1),
+            (1, 3, 1, 2, 4), (0, 6, 0, 2), (1, 3, 1, 0, 5), (1, 3, 0, 2, 1), (1, 2, 6, 1), (1, 3, 0, 2, 0),
+            (0, 6, 2, 2), (1, 3, 2, 2, 0), (1, 3, 2, 2, 1), (0, 3, 1, 2, 1), (0, 3, 1, 0, 0), (0, 3, 4, 0, 0),
+            (1, 3, 1, 2, 5), (0, 0, 0, 0, 1, 3), (1, 1, 0, 0, 1, 3), (1, 3, 1, 0, 4), (1, 2, 7, 1), (1, 3, 0, 2, 3),
+            (1, 3, 0, 2, 2), (0, 0, 0, 1, 1, 2), (1, 1, 0, 1, 1, 2), (0, 3, 0, 2, 1), (1, 3, 0, 2, 5),
+            (0, 3, 0, 2, 0), (1, 3, 0, 2, 4), (1, 3, 2, 2, 3), (1, 2, 5, 1), (0, 0, 0, 1, 1, 1), (1, 1, 0, 1, 1, 1),
+            (1, 3, 3, 1, 3), (0, 0, 0, 0, 1, 2), (1, 1, 0, 0, 1, 2), (0, 3, 2, 0, 1), (1, 2, 5, 3), (0, 3, 4, 1, 1),
+            (0, 3, 2, 2, 0), (1, 2, 7, 3), (1, 3, 2, 2, 4), (0, 3, 2, 2, 1), (0, 3, 2, 1, 0), (0, 3, 2, 1, 1),
+            (1, 3, 2, 3, 2), (1, 3, 2, 2, 5), (1, 3, 2, 0, 3), (0, 7, 1), (0, 0, 0, 1, 1, 3), (1, 1, 0, 1, 1, 3),
+            (0, 3, 2, 3, 1), (1, 3, 2, 3, 5), (1, 3, 2, 1, 5), (1, 3, 5, 1, 3), (1, 3, 5, 1, 0), (1, 3, 2, 0, 5),
+            (0, 3, 2, 3, 0), (1, 3, 2, 3, 4), (1, 2, 7, 2), (1, 3, 2, 2, 2), (1, 3, 2, 0, 4), (1, 3, 2, 1, 4),
+            (0, 8, 0, 0), (0, 7, 0),
+        ),
+        (
+            (0, 3, 5, 1, 1),
+        ),
+        (
+        ),
+        (
+            (1, 2, 6, 3), (1, 3, 4, 1, 2), (0, 3, 4, 0, 1), (1, 3, 4, 0, 5),
+        ),
+        (
+            (0, 3, 5, 1, 0), (1, 3, 4, 1, 5), (0, 3, 5, 0, 0), (1, 3, 4, 0, 3), (0, 6, 5, 2), (1, 3, 5, 2, 3),
+            (1, 3, 5, 1, 5), (0, 6, 3, 3), (1, 3, 5, 2, 2), (0, 7, 2),
+        ),
+        (
+            (0, 6, 3, 2), (1, 3, 3, 2, 3), (1, 3, 5, 2, 1), (1, 3, 3, 3, 0),
+        ),
+        (
+            (1, 3, 5, 2, 0),
+        ),
+        (
+            (0, 6, 5, 3), (1, 3, 5, 3, 1), (1, 3, 5, 3, 3), (1, 3, 5, 3, 0), (0, 5, 0, 0), (1, 4, 0, 0, 0, 2),
+        ),
+        (
+            (1, 4, 0, 0, 0, 3), (0, 5, 0, 3), (1, 4, 0, 3, 0, 3), (0, 3, 3, 1, 1), (1, 3, 4, 0, 4),
+            (1, 4, 0, 0, 0, 1), (1, 3, 5, 1, 2), (1, 3, 3, 2, 0), (1, 3, 3, 2, 1), (0, 6, 4, 3), (1, 3, 3, 2, 2),
+            (1, 3, 4, 3, 2), (0, 5, 0, 1), (1, 4, 0, 1, 0, 3), (1, 3, 4, 3, 1), (1, 3, 4, 3, 0), (0, 5, 0, 2),
+            (1, 3, 3, 3, 3), (1, 4, 0, 1, 0, 2), (1, 4, 0, 2, 0, 3), (0, 3, 5, 2, 1), (1, 3, 5, 0, 2), (0, 6, 4, 2),
+            (1, 3, 4, 2, 0), (1, 3, 3, 3, 2), (1, 3, 3, 3, 1), (1, 3, 4, 0, 2), (1, 3, 4, 2, 3), (1, 4, 0, 3, 0, 2),
+            (1, 3, 5, 3, 2), (1, 3, 3, 1, 5), (0, 3, 3, 2, 0), (1, 3, 3, 2, 4), (1, 3, 4, 2, 1), (1, 3, 5, 1, 4),
+            (0, 3, 3, 0, 0), (1, 4, 0, 1, 0, 1), (1, 4, 0, 2, 0, 2), (0, 4, 0, 0, 1, 0), (1, 3, 3, 0, 4),
+        ),
+        (
+            (0, 3, 4, 3, 0), (0, 0, 1, 0, 1, 1), (1, 0, 1, 0, 0, 0), (1, 3, 4, 2, 2), (0, 3, 3, 1, 0),
+            (0, 3, 3, 3, 0), (1, 3, 3, 1, 4), (1, 3, 5, 0, 3), (0, 3, 4, 2, 0), (0, 3, 4, 2, 1), (1, 3, 3, 3, 4),
+            (1, 4, 0, 3, 0, 1), (0, 3, 4, 1, 0), (1, 3, 5, 2, 5), (0, 3, 5, 3, 1), (1, 4, 0, 2, 0, 1),
+            (0, 4, 0, 1, 1, 0),
+        ),
+        (
+            (1, 1, 1, 1, 0, 0), (1, 3, 4, 2, 4), (0, 3, 3, 3, 1), (1, 0, 1, 1, 0, 0), (1, 2, 6, 2),
+            (1, 1, 1, 0, 0, 0), (1, 3, 4, 3, 4), (1, 3, 4, 2, 5), (0, 3, 4, 3, 1), (1, 3, 4, 3, 5), (1, 3, 5, 3, 5),
+            (1, 3, 3, 3, 5), (1, 3, 4, 3, 3), (0, 3, 5, 2, 0), (1, 3, 5, 2, 4), (0, 3, 3, 2, 1), (0, 3, 5, 3, 0),
+            (1, 3, 3, 2, 5), (0, 4, 0, 2, 1, 0),
+        ),
+        (
+            (1, 3, 4, 1, 4), (1, 0, 1, 2, 0, 0), (0, 4, 0, 3, 1, 0), (1, 3, 4, 1, 3), (1, 3, 5, 3, 4),
+        ),
+        (
+            (1, 0, 1, 3, 0, 0), (1, 1, 1, 3, 0, 0), (1, 3, 3, 0, 5), (1, 1, 1, 0, 1, 1), (0, 0, 1, 1, 1, 1),
+            (1, 3, 5, 0, 4), (0, 0, 1, 1, 1, 2), (0, 0, 1, 0, 1, 2), (1, 1, 1, 1, 1, 2), (1, 1, 1, 0, 1, 2),
+            (0, 0, 1, 0, 1, 3), (1, 1, 1, 0, 1, 3), (0, 8, 1, 0), (0, 7, 3), (0, 7, 4),
+        ),
+        (
+            (0, 7, 5), (1, 1, 1, 1, 1, 1),
+        ),
+        (
+            (0, 0, 1, 1, 1, 3), (1, 1, 1, 1, 1, 3), (1, 1, 1, 2, 0, 0), (0, 5, 1, 0), (1, 4, 1, 0, 0, 2),
+            (1, 4, 1, 0, 0, 1), (0, 8, 1, 1),
+        ),
+        (
+        ),
+        (
+            (1, 4, 1, 0, 0, 3), (0, 0, 1, 2, 1, 3), (1, 1, 1, 2, 1, 3), (0, 0, 1, 2, 1, 2), (0, 0, 1, 3, 1, 1),
+            (1, 1, 1, 3, 1, 1), (1, 1, 1, 2, 1, 2), (0, 0, 1, 2, 1, 1), (1, 1, 1, 2, 1, 1), (0, 5, 1, 1),
+            (1, 4, 1, 1, 0, 2), (0, 0, 1, 3, 1, 2), (1, 1, 1, 3, 1, 2), (1, 4, 1, 1, 0, 3), (1, 4, 1, 1, 0, 1),
+            (0, 0, 1, 3, 1, 3), (1, 1, 1, 3, 1, 3), (0, 8, 1, 2),
+        ),
+        (
+        ),
+        (
+            (0, 8, 1, 3),
         ),
         (
         ),
         (
             (0, 5, 1, 2), (1, 4, 1, 2, 0, 3), (0, 5, 1, 3), (1, 4, 1, 3, 0, 3), (1, 4, 1, 2, 0, 2),
-            (0, 4, 1, 0, 1, 0), (1, 4, 1, 3, 0, 2), (1, 4, 1, 1, 0, 1),
-        ),
-        (
-            (1, 4, 1, 2, 0, 1), (0, 4, 1, 1, 1, 0),
-        ),
-        (
-            (1, 4, 1, 3, 0, 1), (0, 4, 1, 2, 1, 0),
+            (1, 4, 1, 3, 0, 2), (0, 4, 1, 0, 1, 0),
+        ),
+        (
+            (1, 4, 1, 2, 0, 1), (1, 4, 1, 3, 0, 1), (0, 4, 1, 1, 1, 0),
+        ),
+        (
+            (0, 4, 1, 2, 1, 0),
         ),
         (
             (0, 4, 1, 3, 1, 0),
@@ -351,136 +353,133 @@
     ),
     (
         (
-            (1, 3, 0, 1, 0), (1, 2, 2, 0), (1, 3, 0, 1, 2), (1, 3, 0, 1, 3), (1, 3, 0, 1, 1), (1, 2, 2, 2),
-            (1, 3, 1, 1, 0),
-        ),
-        (
-            (1, 3, 1, 1, 2), (1, 1, 0, 0, 0, 0), (1, 3, 1, 1, 1), (1, 0, 0, 0, 1, 0), (1, 0, 0, 1, 1, 0),
-            (1, 0, 0, 0, 0, 0), (0, 3, 0, 1, 0), (1, 3, 0, 1, 4), (0, 3, 0, 1, 1), (1, 3, 2, 1, 0), (1, 3, 0, 1, 5),
-            (0, 3, 1, 1, 0), (1, 0, 0, 1, 0, 0), (1, 3, 2, 1, 2), (1, 3, 2, 1, 1), (1, 1, 0, 1, 0, 0),
-            (1, 3, 2, 1, 3), (0, 0, 0, 0, 1, 1), (0, 3, 2, 1, 0), (0, 0, 0, 0, 0, 1), (1, 3, 3, 1, 0),
-            (1, 0, 0, 0, 1, 1), (1, 3, 3, 1, 1), (1, 3, 5, 1, 0), (1, 3, 4, 1, 0), (1, 3, 4, 1, 2), (1, 3, 3, 1, 3),
-            (1, 1, 0, 0, 0, 1), (0, 3, 1, 1, 1), (1, 0, 0, 0, 0, 1), (1, 1, 0, 0, 1, 1), (1, 3, 4, 1, 1),
-            (0, 3, 2, 1, 1), (1, 3, 2, 1, 4), (1, 3, 4, 1, 3), (0, 0, 0, 1, 0, 1), (1, 1, 0, 1, 0, 1),
-            (0, 3, 3, 1, 1), (0, 0, 0, 1, 1, 1), (1, 0, 0, 1, 1, 1), (0, 3, 4, 1, 1), (1, 3, 5, 1, 1),
-            (1, 3, 5, 1, 2), (0, 0, 0, 0, 1, 2), (1, 3, 1, 1, 5), (1, 1, 0, 1, 1, 1), (1, 0, 0, 1, 0, 1),
-            (0, 3, 3, 1, 0), (1, 2, 2, 3), (1, 3, 2, 1, 5), (1, 3, 1, 1, 4), (0, 3, 5, 1, 0), (1, 0, 0, 0, 1, 2),
-            (1, 3, 4, 1, 5), (1, 3, 1, 1, 3), (0, 3, 5, 1, 1), (1, 3, 3, 1, 5), (1, 3, 3, 1, 2), (0, 3, 4, 1, 0),
-            (0, 0, 0, 1, 1, 2), (1, 1, 0, 1, 1, 2), (1, 3, 5, 1, 5), (1, 3, 3, 1, 4), (1, 2, 3, 2), (1, 2, 1, 2),
-            (1, 2, 0, 2), (1, 1, 0, 0, 1, 2), (1, 3, 4, 1, 4), (1, 3, 5, 1, 4), (1, 2, 4, 2), (1, 0, 0, 1, 1, 2),
-            (1, 2, 1, 0), (1, 2, 3, 0), (0, 6, 1, 0), (1, 3, 1, 0, 1), (1, 2, 1, 3), (1, 3, 1, 0, 0), (0, 6, 0, 0),
-            (1, 3, 0, 0, 0), (1, 3, 0, 0, 1), (0, 6, 0, 2), (1, 3, 0, 2, 3), (1, 3, 0, 2, 1), (1, 3, 0, 2, 2),
-            (1, 3, 0, 2, 0), (1, 3, 0, 0, 3), (1, 3, 0, 0, 2), (1, 2, 0, 0), (1, 2, 3, 3), (0, 3, 1, 0, 1),
-            (1, 2, 4, 0), (0, 3, 0, 0, 0), (0, 3, 0, 0, 1), (0, 3, 1, 0, 0), (1, 3, 0, 0, 5), (1, 2, 0, 3),
-            (1, 2, 7, 0), (1, 2, 4, 3), (1, 3, 0, 0, 4), (0, 3, 0, 2, 0), (1, 3, 0, 2, 4), (0, 3, 0, 2, 1),
-            (1, 3, 0, 2, 5), (0, 6, 2, 0), (1, 2, 5, 0), (1, 2, 7, 2), (0, 6, 1, 2), (0, 6, 0, 3), (1, 3, 0, 3, 1),
-            (1, 2, 5, 2), (1, 3, 0, 3, 0), (1, 3, 0, 3, 2), (0, 6, 1, 3), (1, 3, 0, 3, 3), (0, 6, 2, 3),
-            (1, 3, 1, 0, 5), (1, 3, 1, 0, 4), (0, 3, 0, 3, 1), (0, 3, 0, 3, 0), (1, 3, 0, 3, 4), (1, 3, 0, 3, 5),
-            (1, 3, 1, 0, 3), (1, 3, 1, 0, 2), (1, 3, 1, 2, 0), (1, 3, 1, 2, 1), (1, 3, 1, 2, 2), (1, 3, 1, 2, 3),
-            (1, 3, 1, 3, 0), (1, 2, 5, 3), (1, 3, 1, 3, 1), (1, 3, 1, 3, 3), (0, 6, 5, 2), (1, 3, 1, 3, 2),
-            (1, 2, 7, 3), (0, 3, 1, 2, 0), (0, 3, 1, 2, 1), (1, 3, 1, 2, 4), (1, 3, 1, 2, 5), (1, 3, 2, 0, 0),
-            (1, 3, 2, 0, 1), (0, 3, 1, 3, 0), (0, 6, 3, 2), (0, 3, 1, 3, 1), (1, 3, 1, 3, 5), (1, 3, 1, 3, 4),
-            (1, 3, 2, 0, 3), (0, 6, 2, 2), (1, 3, 2, 2, 1), (1, 3, 2, 2, 2), (1, 3, 2, 2, 0), (1, 3, 5, 1, 3),
-            (1, 3, 2, 0, 2), (1, 3, 2, 3, 0), (0, 3, 2, 0, 0), (0, 3, 2, 0, 1), (1, 3, 2, 3, 1), (1, 3, 2, 0, 4),
-            (1, 3, 2, 3, 3), (1, 3, 2, 2, 3), (0, 8, 0, 0), (0, 7, 0), (0, 7, 1),
-        ),
-        (
-        ),
-        (
-            (1, 3, 2, 0, 5), (0, 3, 2, 2, 1), (0, 3, 2, 2, 0), (1, 3, 2, 2, 4), (1, 3, 2, 3, 2), (1, 3, 2, 2, 5),
-        ),
-        (
-            (1, 3, 3, 2, 0), (0, 3, 2, 3, 0), (0, 3, 2, 3, 1), (1, 3, 3, 2, 1),
-        ),
-        (
-            (1, 3, 2, 3, 5), (1, 3, 2, 3, 4), (1, 3, 5, 2, 2), (1, 3, 3, 2, 3), (0, 6, 3, 0), (1, 3, 3, 0, 0),
-            (1, 3, 3, 0, 1), (1, 3, 5, 2, 1), (1, 3, 5, 2, 0), (1, 2, 6, 2), (0, 3, 3, 2, 1), (0, 6, 3, 3),
-            (1, 2, 6, 0), (0, 7, 2),
-        ),
-        (
-            (1, 3, 3, 3, 1), (1, 3, 3, 3, 0),
-        ),
-        (
-            (0, 3, 3, 2, 0),
-        ),
-        (
-        ),
-        (
-            (1, 3, 3, 2, 5), (1, 2, 6, 3), (1, 3, 3, 3, 3), (0, 4, 0, 0, 0, 2), (1, 3, 3, 0, 2), (1, 3, 3, 0, 3),
-            (0, 3, 3, 3, 1), (1, 3, 3, 3, 2), (1, 3, 5, 2, 3), (0, 5, 0, 0), (0, 5, 0, 3), (0, 3, 3, 0, 0),
-            (0, 6, 4, 2), (0, 4, 0, 0, 0, 1), (1, 4, 0, 0, 0, 2), (1, 3, 4, 2, 0), (1, 4, 0, 0, 0, 1),
-            (0, 4, 0, 0, 0, 0), (1, 3, 4, 2, 1), (0, 4, 0, 3, 0, 2), (1, 3, 4, 2, 2), (1, 4, 0, 3, 0, 2),
-            (0, 3, 3, 3, 0), (0, 4, 0, 0, 1, 1), (1, 4, 0, 0, 1, 1), (0, 3, 5, 2, 1), (0, 4, 0, 3, 0, 1),
-            (0, 5, 0, 1), (0, 3, 4, 2, 1), (0, 6, 5, 0), (0, 3, 4, 2, 0), (1, 3, 4, 2, 5), (1, 4, 0, 3, 0, 1),
-            (1, 3, 5, 0, 0), (1, 3, 3, 2, 4), (0, 3, 3, 0, 1), (1, 3, 3, 0, 5), (0, 4, 0, 0, 1, 0),
-        ),
-        (
-            (1, 0, 1, 0, 1, 0), (0, 4, 0, 3, 1, 1), (1, 3, 4, 2, 4), (1, 0, 1, 0, 0, 0), (1, 3, 5, 0, 1),
-            (0, 4, 0, 1, 0, 2), (1, 4, 0, 1, 0, 2), (1, 3, 3, 2, 2), (0, 4, 0, 3, 0, 0), (1, 3, 5, 2, 5),
-            (0, 6, 5, 3), (1, 3, 5, 3, 3), (1, 3, 5, 3, 0), (1, 3, 5, 3, 1), (1, 3, 3, 3, 5), (1, 4, 0, 3, 1, 1),
-            (1, 3, 4, 2, 3), (0, 4, 0, 1, 0, 1), (1, 3, 5, 3, 2), (1, 3, 5, 0, 3), (0, 3, 5, 2, 0), (1, 3, 5, 2, 4),
-            (1, 1, 1, 0, 0, 0), (1, 3, 3, 0, 4), (1, 4, 0, 1, 0, 1), (0, 0, 1, 0, 1, 1), (0, 5, 0, 2),
-            (1, 0, 1, 0, 1, 1), (0, 3, 5, 0, 1), (0, 3, 5, 0, 0), (1, 3, 5, 0, 5), (0, 4, 0, 2, 0, 2),
-            (0, 4, 0, 1, 1, 1), (0, 4, 0, 1, 0, 0), (1, 4, 0, 1, 1, 1), (1, 4, 0, 2, 0, 2), (0, 4, 0, 3, 1, 0),
-            (1, 1, 1, 0, 1, 1), (0, 4, 0, 2, 0, 1), (0, 4, 0, 1, 1, 0),
-        ),
-        (
-            (1, 0, 1, 1, 0, 0), (0, 3, 5, 3, 0), (1, 0, 1, 1, 1, 0), (0, 4, 0, 2, 0, 0), (1, 4, 0, 2, 0, 1),
-            (0, 4, 0, 2, 1, 1), (0, 3, 5, 3, 1), (1, 3, 5, 3, 5), (1, 3, 5, 0, 4), (0, 0, 1, 0, 0, 1),
-            (1, 0, 1, 0, 0, 1), (1, 4, 0, 2, 1, 1), (1, 3, 3, 3, 4), (0, 0, 1, 1, 1, 1), (1, 0, 1, 1, 1, 1),
-            (0, 6, 4, 0), (1, 3, 4, 0, 1), (1, 3, 5, 0, 2), (1, 3, 4, 0, 0), (0, 4, 0, 2, 1, 0), (1, 1, 1, 0, 0, 1),
-            (1, 3, 4, 0, 2),
-        ),
-        (
-            (1, 3, 4, 0, 3),
-        ),
-        (
-            (1, 1, 1, 1, 1, 1), (1, 1, 1, 3, 0, 0), (1, 0, 1, 2, 1, 0), (1, 0, 1, 2, 0, 0), (1, 0, 1, 3, 1, 0),
-            (0, 0, 1, 0, 1, 2), (1, 1, 1, 0, 1, 2), (1, 3, 5, 3, 4), (0, 0, 1, 1, 0, 1), (1, 1, 1, 1, 0, 0),
-            (1, 0, 1, 1, 0, 1), (1, 0, 1, 0, 1, 2), (0, 3, 4, 0, 1), (1, 3, 4, 0, 5), (1, 0, 1, 3, 0, 0),
-            (0, 3, 4, 0, 0), (1, 3, 4, 0, 4), (0, 0, 1, 2, 1, 1), (1, 1, 1, 2, 0, 0), (1, 0, 1, 2, 1, 1),
-            (0, 6, 4, 3), (1, 3, 4, 3, 1), (1, 3, 4, 3, 0), (1, 1, 1, 1, 0, 1), (0, 0, 1, 2, 0, 1),
-            (1, 1, 1, 2, 1, 1), (0, 0, 1, 1, 1, 2), (1, 0, 1, 2, 0, 1), (1, 3, 4, 3, 2), (1, 3, 4, 3, 3),
-            (1, 0, 1, 1, 1, 2), (0, 0, 1, 3, 1, 1), (0, 0, 1, 3, 0, 1), (1, 0, 1, 3, 0, 1), (1, 0, 1, 3, 1, 1),
-            (0, 3, 4, 3, 0), (1, 1, 1, 3, 0, 1), (0, 3, 4, 3, 1), (1, 3, 4, 3, 4), (1, 3, 4, 3, 5),
-            (0, 0, 1, 2, 1, 2), (1, 1, 1, 1, 1, 2), (1, 0, 1, 2, 1, 2), (0, 0, 1, 3, 1, 2), (1, 0, 1, 3, 1, 2),
-            (1, 1, 1, 3, 1, 1), (1, 1, 1, 3, 1, 2), (0, 8, 1, 0), (0, 7, 3), (0, 7, 4),
-        ),
-        (
-            (1, 1, 1, 2, 1, 2), (1, 1, 1, 2, 0, 1), (0, 7, 5),
+            (1, 3, 4, 1, 0), (1, 2, 1, 2), (1, 2, 1, 0), (1, 2, 3, 0), (1, 3, 0, 1, 0), (1, 2, 3, 2), (1, 2, 2, 0),
+            (1, 3, 0, 1, 1), (1, 2, 0, 0), (1, 3, 1, 1, 0), (1, 3, 2, 1, 0), (1, 3, 1, 1, 1), (1, 2, 0, 2),
+            (1, 2, 4, 2),
+        ),
+        (
+            (1, 3, 4, 1, 1), (1, 3, 2, 1, 1), (1, 0, 0, 1, 0, 0), (0, 6, 1, 0), (1, 2, 4, 0), (0, 6, 1, 2),
+            (1, 3, 1, 2, 0), (1, 3, 1, 0, 3), (1, 2, 2, 2), (1, 3, 1, 1, 3), (0, 3, 4, 1, 0), (1, 1, 0, 1, 0, 0),
+            (1, 3, 3, 1, 0), (1, 0, 0, 1, 1, 0), (0, 6, 2, 2), (1, 3, 2, 2, 1), (1, 3, 2, 2, 3), (1, 0, 0, 0, 1, 0),
+            (1, 0, 0, 0, 0, 0), (1, 3, 2, 2, 2), (1, 3, 2, 2, 0), (1, 3, 1, 2, 1), (1, 3, 1, 0, 1), (0, 3, 0, 1, 1),
+            (1, 3, 0, 1, 5), (0, 6, 0, 2), (1, 3, 0, 2, 0), (1, 3, 0, 2, 2), (1, 3, 0, 1, 3), (1, 2, 3, 3),
+            (1, 3, 1, 0, 0), (1, 3, 3, 1, 1), (1, 3, 4, 1, 3), (0, 0, 0, 1, 0, 1), (1, 1, 0, 0, 0, 0),
+            (1, 3, 1, 2, 3), (1, 0, 0, 1, 0, 1), (1, 2, 7, 0), (0, 3, 2, 1, 1), (1, 3, 0, 2, 1), (1, 3, 1, 0, 2),
+            (1, 3, 4, 1, 4), (1, 1, 0, 1, 0, 1), (0, 0, 0, 0, 0, 1), (1, 0, 0, 0, 0, 1), (0, 3, 2, 1, 0),
+            (1, 3, 2, 1, 5), (0, 3, 1, 1, 1), (1, 3, 1, 1, 5), (0, 3, 2, 2, 0), (1, 2, 6, 0), (1, 3, 0, 1, 2),
+            (1, 2, 2, 3), (0, 3, 1, 2, 1), (1, 3, 0, 2, 3), (1, 3, 2, 2, 4), (1, 2, 5, 0), (0, 3, 1, 2, 0),
+            (0, 0, 0, 1, 1, 1), (1, 0, 0, 1, 1, 1), (0, 3, 1, 1, 0), (1, 3, 1, 1, 4), (0, 6, 0, 0), (1, 3, 0, 0, 0),
+            (0, 3, 1, 0, 0), (1, 3, 0, 0, 3), (0, 6, 1, 3), (1, 3, 1, 3, 1), (0, 6, 2, 0), (1, 3, 2, 0, 0),
+            (1, 3, 1, 2, 5), (1, 3, 1, 3, 0), (1, 3, 0, 0, 2), (0, 3, 2, 2, 1), (1, 3, 2, 2, 5), (0, 3, 0, 2, 0),
+            (1, 3, 0, 2, 4), (0, 3, 0, 1, 0), (0, 3, 3, 1, 1), (0, 3, 0, 2, 1), (1, 3, 1, 2, 4), (1, 3, 1, 2, 2),
+            (1, 3, 0, 1, 4), (1, 3, 1, 3, 2), (1, 1, 0, 0, 0, 1), (1, 2, 1, 3), (0, 3, 0, 0, 0), (1, 2, 0, 3),
+            (1, 3, 2, 0, 1), (1, 2, 4, 3), (0, 0, 0, 1, 1, 2), (1, 1, 0, 1, 1, 2), (0, 0, 0, 0, 1, 1),
+            (0, 0, 0, 0, 1, 2), (1, 3, 2, 1, 3), (1, 3, 3, 1, 2), (1, 1, 0, 0, 1, 2), (1, 1, 0, 0, 1, 1),
+            (1, 0, 0, 0, 1, 2), (1, 3, 0, 0, 1), (0, 3, 3, 1, 0), (1, 3, 0, 2, 5), (0, 3, 2, 0, 0), (0, 6, 0, 3),
+            (1, 3, 0, 3, 3), (0, 3, 1, 3, 0), (1, 0, 0, 1, 1, 2), (1, 3, 0, 3, 0), (1, 3, 0, 3, 1), (1, 3, 0, 3, 2),
+            (0, 3, 1, 0, 1), (1, 1, 0, 1, 1, 1), (0, 3, 0, 0, 1), (1, 3, 1, 0, 5), (1, 3, 1, 0, 4), (1, 2, 6, 2),
+            (0, 6, 2, 3), (1, 3, 2, 3, 0), (1, 3, 2, 1, 4), (0, 3, 4, 1, 1), (1, 3, 1, 1, 2), (1, 3, 1, 3, 3),
+            (1, 3, 2, 1, 2), (1, 3, 4, 1, 2), (0, 3, 2, 0, 1), (1, 3, 0, 0, 4), (1, 0, 0, 0, 1, 1), (1, 3, 2, 3, 1),
+            (1, 2, 5, 2), (0, 3, 0, 3, 0), (1, 3, 0, 0, 5), (1, 3, 0, 3, 4), (0, 8, 0, 0), (1, 2, 7, 3), (0, 6, 4, 0),
+            (0, 6, 3, 3), (1, 3, 4, 0, 0), (0, 3, 1, 3, 1), (1, 3, 1, 3, 5), (1, 3, 1, 3, 4), (1, 2, 5, 3),
+            (0, 3, 2, 3, 0), (1, 3, 5, 1, 0), (1, 3, 5, 1, 1), (0, 3, 0, 3, 1), (1, 3, 0, 3, 5), (1, 3, 4, 0, 2),
+            (1, 3, 2, 0, 5), (0, 6, 3, 0), (1, 3, 3, 0, 1), (1, 3, 2, 3, 2), (1, 3, 4, 1, 5), (0, 6, 4, 2),
+            (1, 3, 4, 2, 3), (1, 3, 4, 2, 1), (0, 3, 5, 1, 1), (0, 6, 5, 0), (1, 3, 5, 0, 1), (1, 3, 2, 0, 3),
+            (1, 3, 3, 1, 3), (0, 7, 0), (1, 3, 3, 0, 0), (1, 3, 2, 0, 2), (1, 3, 2, 0, 4), (0, 3, 2, 3, 1),
+            (1, 3, 2, 3, 5), (0, 7, 1), (1, 3, 2, 3, 3),
+        ),
+        (
+            (1, 3, 2, 3, 4),
+        ),
+        (
+            (0, 6, 3, 2), (1, 3, 3, 2, 0), (1, 2, 7, 2), (0, 3, 5, 1, 0), (1, 2, 6, 3),
+        ),
+        (
+        ),
+        (
+            (0, 7, 2),
+        ),
+        (
+        ),
+        (
+        ),
+        (
+            (1, 3, 3, 2, 1), (1, 3, 5, 1, 5), (0, 6, 5, 3), (1, 3, 5, 3, 1), (1, 3, 5, 0, 2), (0, 6, 5, 2),
+            (1, 3, 5, 2, 1), (1, 3, 3, 3, 0), (1, 3, 5, 3, 0), (1, 3, 5, 0, 0),
+        ),
+        (
+            (1, 3, 5, 2, 3), (0, 5, 0, 0), (0, 4, 0, 0, 0, 1), (1, 4, 0, 0, 0, 1), (1, 3, 3, 3, 3), (1, 3, 4, 2, 0),
+            (0, 3, 3, 0, 1), (0, 4, 0, 0, 0, 2), (1, 4, 0, 0, 0, 2), (1, 3, 3, 3, 1), (0, 5, 0, 3), (0, 3, 4, 0, 0),
+            (0, 4, 0, 3, 0, 2), (1, 4, 0, 3, 0, 2), (0, 4, 0, 0, 1, 0), (0, 4, 0, 0, 0, 0),
+        ),
+        (
+            (1, 0, 1, 0, 1, 0), (1, 0, 1, 0, 0, 0), (0, 3, 4, 2, 1), (1, 3, 5, 2, 0), (1, 3, 4, 0, 1), (0, 5, 0, 1),
+            (1, 3, 4, 0, 4), (1, 3, 3, 0, 3), (1, 3, 5, 3, 2), (0, 5, 0, 2), (0, 4, 0, 0, 1, 1), (1, 3, 3, 1, 4),
+            (1, 3, 3, 1, 5), (1, 4, 0, 0, 1, 1), (0, 4, 0, 1, 0, 2), (1, 4, 0, 1, 0, 2), (0, 3, 3, 0, 0),
+            (0, 4, 0, 1, 0, 1), (1, 4, 0, 1, 0, 1), (1, 3, 4, 2, 2), (0, 3, 3, 3, 1), (0, 4, 0, 2, 0, 2),
+            (1, 4, 0, 2, 0, 2), (0, 3, 5, 2, 0), (1, 3, 3, 2, 3), (0, 3, 3, 2, 1), (0, 4, 0, 1, 1, 1),
+            (1, 4, 0, 1, 1, 1), (1, 3, 3, 2, 5), (1, 3, 3, 0, 2), (1, 3, 5, 1, 3), (0, 4, 0, 3, 0, 1),
+            (1, 4, 0, 3, 0, 1), (0, 4, 0, 1, 1, 0), (0, 3, 4, 2, 0), (1, 3, 5, 3, 3), (0, 3, 5, 3, 1),
+            (1, 3, 5, 3, 5), (0, 4, 0, 1, 0, 0),
+        ),
+        (
+            (1, 0, 1, 1, 1, 0), (0, 3, 5, 2, 1), (1, 3, 5, 2, 5), (1, 0, 1, 1, 0, 0), (0, 4, 0, 2, 0, 1),
+            (1, 4, 0, 2, 0, 1), (0, 4, 0, 2, 1, 1), (1, 4, 0, 2, 1, 1), (1, 3, 4, 0, 3), (0, 4, 0, 3, 1, 1),
+            (1, 3, 3, 3, 2), (0, 0, 1, 0, 0, 1), (1, 0, 1, 0, 0, 1), (1, 4, 0, 3, 1, 1), (1, 3, 5, 1, 2),
+            (1, 3, 5, 2, 2), (1, 3, 4, 2, 5), (1, 3, 5, 0, 3), (0, 0, 1, 1, 1, 1), (1, 0, 1, 1, 1, 1),
+            (0, 3, 5, 0, 0), (1, 3, 5, 0, 4), (1, 3, 3, 0, 4), (0, 0, 1, 0, 1, 1), (1, 1, 1, 0, 1, 1),
+            (1, 0, 1, 0, 1, 1), (0, 4, 0, 2, 1, 0), (0, 4, 0, 2, 0, 0),
+        ),
+        (
+            (1, 3, 5, 1, 4), (0, 0, 1, 1, 0, 1), (1, 1, 1, 1, 0, 1), (1, 1, 1, 2, 0, 0), (1, 1, 1, 0, 0, 0),
+            (0, 0, 1, 0, 1, 2), (1, 1, 1, 0, 1, 2), (1, 0, 1, 0, 1, 2), (1, 1, 1, 1, 1, 1), (0, 3, 5, 3, 0),
+            (1, 3, 5, 3, 4), (1, 0, 1, 1, 0, 1), (1, 0, 1, 2, 0, 0), (0, 4, 0, 3, 1, 0), (0, 4, 0, 3, 0, 0),
+        ),
+        (
+            (1, 1, 1, 3, 0, 0), (1, 3, 4, 2, 4), (0, 3, 4, 0, 1), (0, 3, 3, 2, 0), (1, 3, 3, 0, 5),
+            (1, 0, 1, 3, 1, 0), (1, 3, 3, 3, 5), (1, 0, 1, 2, 1, 0), (0, 6, 4, 3), (1, 3, 4, 3, 0), (1, 3, 4, 3, 1),
+            (1, 3, 4, 3, 2), (1, 3, 4, 3, 3), (1, 3, 4, 0, 5), (0, 0, 1, 2, 0, 1), (1, 0, 1, 2, 0, 1),
+            (1, 3, 3, 2, 4), (1, 0, 1, 3, 0, 0), (0, 3, 3, 3, 0), (0, 0, 1, 1, 1, 2), (1, 0, 1, 1, 1, 2),
+            (0, 0, 1, 3, 0, 1), (1, 0, 1, 3, 0, 1), (0, 0, 1, 2, 1, 1), (1, 0, 1, 2, 1, 1), (1, 1, 1, 2, 1, 1),
+            (0, 3, 5, 0, 1), (1, 3, 3, 2, 2), (1, 3, 5, 0, 5), (1, 1, 1, 2, 0, 1), (1, 1, 1, 1, 0, 0),
+            (1, 1, 1, 3, 0, 1), (1, 3, 3, 3, 4), (1, 3, 5, 2, 4), (1, 1, 1, 1, 1, 2), (0, 0, 1, 2, 1, 2),
+            (1, 0, 1, 2, 1, 2), (1, 1, 1, 0, 0, 1), (1, 1, 1, 2, 1, 2), (0, 3, 4, 3, 0), (1, 3, 4, 3, 4),
+            (0, 0, 1, 3, 1, 1), (1, 0, 1, 3, 1, 1), (0, 3, 4, 3, 1), (1, 3, 4, 3, 5), (1, 1, 1, 3, 1, 1),
+            (0, 0, 1, 3, 1, 2), (1, 0, 1, 3, 1, 2), (1, 1, 1, 3, 1, 2), (0, 7, 4), (0, 7, 3), (0, 8, 1, 0),
+        ),
+        (
+            (0, 7, 5),
         ),
         (
             (0, 8, 1, 1),
         ),
         (
-        ),
-        (
-            (0, 5, 1, 0), (0, 4, 1, 0, 0, 2), (0, 8, 1, 2),
-        ),
-        (
-            (1, 4, 1, 0, 0, 2), (0, 4, 1, 0, 0, 1),
-        ),
-        (
-            (1, 4, 1, 0, 0, 1), (0, 8, 1, 3),
-        ),
-        (
-            (0, 5, 1, 1),
-        ),
-        (
-            (0, 4, 1, 0, 0, 0), (0, 4, 1, 0, 1, 1), (0, 4, 1, 1, 0, 2), (1, 4, 1, 0, 1, 1), (1, 4, 1, 1, 0, 2),
-            (0, 4, 1, 0, 1, 0),
-        ),
-        (
-            (0, 4, 1, 1, 0, 1), (1, 4, 1, 1, 0, 1), (0, 4, 1, 2, 0, 2), (0, 5, 1, 2), (0, 5, 1, 3),
-            (1, 4, 1, 2, 0, 2), (0, 4, 1, 1, 1, 1), (1, 4, 1, 1, 1, 1), (0, 4, 1, 3, 0, 2), (1, 4, 1, 3, 0, 2),
-            (0, 4, 1, 2, 0, 1), (0, 4, 1, 1, 1, 0), (1, 4, 1, 2, 0, 1), (0, 4, 1, 2, 1, 1), (1, 4, 1, 2, 1, 1),
-            (0, 4, 1, 3, 0, 1), (1, 4, 1, 3, 0, 1), (0, 4, 1, 3, 1, 1), (1, 4, 1, 3, 1, 1), (0, 4, 1, 2, 0, 0),
-            (0, 4, 1, 1, 0, 0), (0, 4, 1, 2, 1, 0),
-        ),
-        (
-        ),
-        (
-            (0, 4, 1, 3, 0, 0), (0, 4, 1, 3, 1, 0),
+            (0, 5, 1, 0), (0, 4, 1, 0, 0, 2), (0, 8, 1, 2), (1, 4, 1, 0, 0, 2), (0, 4, 1, 0, 0, 1),
+            (1, 4, 1, 0, 0, 1),
+        ),
+        (
+        ),
+        (
+        ),
+        (
+            (0, 5, 1, 1), (0, 4, 1, 1, 0, 1), (1, 4, 1, 1, 0, 1), (0, 8, 1, 3), (0, 4, 1, 0, 0, 0),
+        ),
+        (
+            (0, 4, 1, 1, 0, 2), (0, 4, 1, 0, 1, 1), (1, 4, 1, 0, 1, 1), (1, 4, 1, 1, 0, 2), (0, 5, 1, 2),
+        ),
+        (
+            (0, 4, 1, 2, 0, 2), (1, 4, 1, 2, 0, 2), (0, 5, 1, 3), (0, 4, 1, 3, 0, 2), (1, 4, 1, 3, 0, 2),
+            (0, 4, 1, 1, 1, 1), (1, 4, 1, 1, 1, 1), (0, 4, 1, 2, 0, 1), (1, 4, 1, 2, 0, 1), (0, 4, 1, 2, 1, 1),
+            (1, 4, 1, 2, 1, 1), (0, 4, 1, 3, 0, 1), (1, 4, 1, 3, 0, 1), (0, 4, 1, 0, 1, 0),
+        ),
+        (
+            (0, 4, 1, 3, 1, 1), (1, 4, 1, 3, 1, 1), (0, 4, 1, 1, 0, 0), (0, 4, 1, 3, 0, 0), (0, 4, 1, 1, 1, 0),
+        ),
+        (
+            (0, 4, 1, 2, 1, 0), (0, 4, 1, 2, 0, 0),
+        ),
+        (
+            (0, 4, 1, 3, 1, 0),
         ),
         (
         ),

time: 124 us -> 117 us (0.944)
  Pallas kernels: 122 us -> 114 us
    pallas_call x1, Pallas kernels: 122 us -> 114 us  [body(): pl.pallas_call(functools.partial(layer_kernel, n_fs, groups), out_shape=j...]
where the time goes in v3:
time: 117 us; the launch traced here: 116 us
  Pallas kernels  114 us (97%)
  local copies, waits for them, and re-layouts  1.88 us (2%)
    pallas_call x1, Pallas kernels, body(): pl.pallas_call(functools.partial(layer_kernel, n_fs, groups), out_shape=j...  114 us

profile of v3, /device:TPU:0, one launch (start us, length us, event | category | flops | bytes accessed | tf_op | source)
XLA Modules:
  0.0 116.4 jit_solution(1544682496043975743)
XLA Ops:
  0.0 114.5 %shard_map.163 = bf16[128,2048]{1,0:T(8,128)(2,1)} custom-call(bf16[128,2048]{1,0:T(8,128)(2,1)} %tokens_in.1, f32[1,2048]{1,0:T(1,128)} %bitcast.3, bf16[128,512]{1,0:T(8,128)(2,1)} %wq.1, bf16[128,512]{1,0:T(8,128)(2,1)} %wk.1, bf16[128,1024]{1,0:T(8,128)(2,1)} %wv.1, bf16[128,1024]{1,0:T(8,128)(2,1)} %wg.1, f32[1,1024]{1,0:T(1,128)} %bitcast.5, ...), custom_call_target="tpu_custom_call" | custom-call | tf_op jit(solution)/shard_map/pallas_call | solution.py:925
  114.5 1.9 %copy.19 = bf16[128,2048]{1,0:T(8,128)(2,1)} copy(bf16[128,2048]{1,0:T(8,128)(2,1)} %shard_map.163) | data formatting | bytes 1048576

commit v4 on v3

--- a/solution.py
+++ b/solution.py
@@ -206,6 +206,8 @@
     (0, 1),
     (1, 0),
     (1, 1),
+    (8, 0),
+    (8, 1),
     (2, 0),
     (2, 1),
     (2, 2),
@@ -230,102 +232,108 @@
 PLAN = (
     (
         (
-            (1, 2, 0, 3), (1, 2, 3, 1), (1, 2, 3, 3), (1, 3, 4, 0, 0),
-        ),
-        (
-            (1, 3, 0, 0, 0), (0, 6, 1, 1), (1, 3, 1, 1, 1), (1, 3, 1, 1, 3), (1, 3, 1, 1, 2), (1, 3, 3, 0, 0),
-            (1, 3, 1, 1, 0), (1, 2, 2, 3), (1, 2, 1, 3), (1, 3, 3, 0, 1), (1, 3, 0, 0, 2), (1, 3, 1, 0, 0),
-            (1, 3, 1, 0, 1), (1, 3, 1, 0, 3), (0, 6, 1, 3), (1, 3, 1, 3, 3), (1, 3, 1, 3, 2), (1, 3, 0, 0, 1),
-            (1, 0, 0, 0, 0, 0), (1, 0, 0, 1, 0, 0), (0, 3, 0, 0, 0), (1, 3, 5, 0, 0), (1, 3, 5, 0, 1),
-            (1, 3, 1, 3, 0), (1, 3, 4, 0, 1), (0, 6, 0, 1), (1, 3, 0, 1, 2), (1, 3, 0, 1, 0), (1, 3, 0, 1, 3),
-            (1, 3, 0, 1, 1), (1, 2, 0, 1), (1, 3, 0, 0, 3), (1, 3, 1, 3, 1), (0, 3, 1, 1, 1), (1, 3, 1, 1, 5),
-            (0, 6, 2, 1), (0, 3, 3, 0, 1), (1, 3, 2, 1, 0), (1, 3, 2, 1, 3), (1, 3, 2, 1, 2), (1, 3, 1, 0, 2),
-            (0, 6, 0, 3), (1, 3, 2, 0, 0), (1, 3, 0, 3, 3), (1, 3, 0, 3, 1), (1, 3, 2, 1, 1), (1, 2, 1, 1),
-            (1, 2, 4, 3), (1, 3, 0, 3, 0), (0, 3, 0, 0, 1), (1, 3, 0, 3, 2), (1, 3, 2, 0, 2), (1, 2, 2, 1),
-            (1, 3, 0, 0, 5), (0, 3, 0, 1, 0), (1, 3, 0, 1, 4), (1, 2, 3, 2), (1, 2, 4, 1), (0, 6, 2, 3),
-            (0, 3, 1, 3, 1), (1, 3, 1, 3, 5), (1, 3, 2, 3, 1), (1, 2, 0, 2), (0, 6, 1, 2), (1, 3, 1, 2, 2),
-            (1, 3, 0, 0, 4), (1, 3, 2, 3, 3), (0, 6, 5, 1), (1, 3, 2, 3, 0), (1, 3, 1, 2, 1), (1, 3, 1, 2, 3),
-            (0, 3, 0, 1, 1), (1, 3, 0, 1, 5), (0, 3, 0, 3, 1), (1, 3, 1, 2, 0), (0, 0, 0, 0, 1, 1),
-            (1, 1, 0, 0, 1, 1), (0, 3, 1, 3, 0), (0, 3, 0, 3, 0), (1, 3, 2, 0, 1), (1, 2, 1, 2), (1, 1, 0, 1, 0, 0),
-            (0, 6, 3, 1), (1, 3, 3, 1, 2), (1, 3, 3, 1, 1), (1, 3, 3, 0, 3), (1, 3, 1, 3, 4), (1, 3, 0, 3, 4),
-            (1, 3, 0, 3, 5), (1, 1, 0, 0, 0, 0), (0, 3, 5, 0, 1), (1, 3, 5, 0, 5), (0, 6, 4, 1), (1, 3, 4, 1, 0),
-            (1, 3, 4, 1, 1), (1, 2, 2, 2), (1, 3, 3, 0, 2), (1, 2, 4, 2), (1, 2, 5, 2), (0, 3, 1, 2, 0),
-            (0, 3, 2, 0, 0), (1, 3, 3, 1, 0), (0, 3, 1, 1, 0), (1, 3, 1, 1, 4), (1, 3, 5, 1, 1), (0, 3, 1, 0, 1),
-            (1, 3, 1, 2, 4), (0, 6, 0, 2), (1, 3, 1, 0, 5), (1, 3, 0, 2, 1), (1, 2, 6, 1), (1, 3, 0, 2, 0),
-            (0, 6, 2, 2), (1, 3, 2, 2, 0), (1, 3, 2, 2, 1), (0, 3, 1, 2, 1), (0, 3, 1, 0, 0), (0, 3, 4, 0, 0),
-            (1, 3, 1, 2, 5), (0, 0, 0, 0, 1, 3), (1, 1, 0, 0, 1, 3), (1, 3, 1, 0, 4), (1, 2, 7, 1), (1, 3, 0, 2, 3),
-            (1, 3, 0, 2, 2), (0, 0, 0, 1, 1, 2), (1, 1, 0, 1, 1, 2), (0, 3, 0, 2, 1), (1, 3, 0, 2, 5),
-            (0, 3, 0, 2, 0), (1, 3, 0, 2, 4), (1, 3, 2, 2, 3), (1, 2, 5, 1), (0, 0, 0, 1, 1, 1), (1, 1, 0, 1, 1, 1),
-            (1, 3, 3, 1, 3), (0, 0, 0, 0, 1, 2), (1, 1, 0, 0, 1, 2), (0, 3, 2, 0, 1), (1, 2, 5, 3), (0, 3, 4, 1, 1),
-            (0, 3, 2, 2, 0), (1, 2, 7, 3), (1, 3, 2, 2, 4), (0, 3, 2, 2, 1), (0, 3, 2, 1, 0), (0, 3, 2, 1, 1),
-            (1, 3, 2, 3, 2), (1, 3, 2, 2, 5), (1, 3, 2, 0, 3), (0, 7, 1), (0, 0, 0, 1, 1, 3), (1, 1, 0, 1, 1, 3),
-            (0, 3, 2, 3, 1), (1, 3, 2, 3, 5), (1, 3, 2, 1, 5), (1, 3, 5, 1, 3), (1, 3, 5, 1, 0), (1, 3, 2, 0, 5),
-            (0, 3, 2, 3, 0), (1, 3, 2, 3, 4), (1, 2, 7, 2), (1, 3, 2, 2, 2), (1, 3, 2, 0, 4), (1, 3, 2, 1, 4),
-            (0, 8, 0, 0), (0, 7, 0),
-        ),
-        (
-            (0, 3, 5, 1, 1),
-        ),
-        (
-        ),
-        (
-            (1, 2, 6, 3), (1, 3, 4, 1, 2), (0, 3, 4, 0, 1), (1, 3, 4, 0, 5),
-        ),
-        (
-            (0, 3, 5, 1, 0), (1, 3, 4, 1, 5), (0, 3, 5, 0, 0), (1, 3, 4, 0, 3), (0, 6, 5, 2), (1, 3, 5, 2, 3),
-            (1, 3, 5, 1, 5), (0, 6, 3, 3), (1, 3, 5, 2, 2), (0, 7, 2),
-        ),
-        (
-            (0, 6, 3, 2), (1, 3, 3, 2, 3), (1, 3, 5, 2, 1), (1, 3, 3, 3, 0),
-        ),
-        (
-            (1, 3, 5, 2, 0),
-        ),
-        (
-            (0, 6, 5, 3), (1, 3, 5, 3, 1), (1, 3, 5, 3, 3), (1, 3, 5, 3, 0), (0, 5, 0, 0), (1, 4, 0, 0, 0, 2),
-        ),
-        (
-            (1, 4, 0, 0, 0, 3), (0, 5, 0, 3), (1, 4, 0, 3, 0, 3), (0, 3, 3, 1, 1), (1, 3, 4, 0, 4),
-            (1, 4, 0, 0, 0, 1), (1, 3, 5, 1, 2), (1, 3, 3, 2, 0), (1, 3, 3, 2, 1), (0, 6, 4, 3), (1, 3, 3, 2, 2),
-            (1, 3, 4, 3, 2), (0, 5, 0, 1), (1, 4, 0, 1, 0, 3), (1, 3, 4, 3, 1), (1, 3, 4, 3, 0), (0, 5, 0, 2),
-            (1, 3, 3, 3, 3), (1, 4, 0, 1, 0, 2), (1, 4, 0, 2, 0, 3), (0, 3, 5, 2, 1), (1, 3, 5, 0, 2), (0, 6, 4, 2),
-            (1, 3, 4, 2, 0), (1, 3, 3, 3, 2), (1, 3, 3, 3, 1), (1, 3, 4, 0, 2), (1, 3, 4, 2, 3), (1, 4, 0, 3, 0, 2),
-            (1, 3, 5, 3, 2), (1, 3, 3, 1, 5), (0, 3, 3, 2, 0), (1, 3, 3, 2, 4), (1, 3, 4, 2, 1), (1, 3, 5, 1, 4),
-            (0, 3, 3, 0, 0), (1, 4, 0, 1, 0, 1), (1, 4, 0, 2, 0, 2), (0, 4, 0, 0, 1, 0), (1, 3, 3, 0, 4),
-        ),
-        (
-            (0, 3, 4, 3, 0), (0, 0, 1, 0, 1, 1), (1, 0, 1, 0, 0, 0), (1, 3, 4, 2, 2), (0, 3, 3, 1, 0),
-            (0, 3, 3, 3, 0), (1, 3, 3, 1, 4), (1, 3, 5, 0, 3), (0, 3, 4, 2, 0), (0, 3, 4, 2, 1), (1, 3, 3, 3, 4),
-            (1, 4, 0, 3, 0, 1), (0, 3, 4, 1, 0), (1, 3, 5, 2, 5), (0, 3, 5, 3, 1), (1, 4, 0, 2, 0, 1),
+            (1, 2, 1, 3), (1, 2, 2, 3), (1, 2, 0, 3), (1, 2, 3, 3), (1, 3, 3, 0, 0), (1, 3, 3, 0, 3), (1, 3, 0, 0, 0),
+            (1, 3, 2, 0, 0), (1, 3, 2, 0, 1), (1, 3, 4, 0, 0), (0, 6, 1, 1), (1, 3, 1, 1, 3), (1, 3, 1, 1, 1),
+            (1, 3, 0, 0, 2), (1, 2, 3, 1),
+        ),
+        (
+            (1, 0, 0, 1, 0, 0), (1, 1, 0, 0, 0, 0), (1, 1, 0, 1, 0, 0), (1, 3, 5, 0, 0), (1, 2, 1, 1), (0, 6, 0, 3),
+            (1, 3, 0, 3, 1), (1, 3, 0, 3, 0), (1, 3, 0, 3, 2), (1, 3, 2, 0, 2), (1, 3, 2, 0, 3), (1, 0, 0, 0, 0, 0),
+            (1, 3, 0, 0, 1), (0, 6, 2, 1), (1, 3, 2, 1, 1), (1, 3, 0, 3, 3), (0, 3, 1, 1, 1), (0, 3, 2, 0, 1),
+            (0, 6, 1, 3), (1, 2, 0, 1), (1, 3, 1, 3, 1), (0, 3, 3, 0, 0), (0, 6, 0, 1), (1, 3, 0, 1, 1),
+            (1, 3, 3, 0, 4), (1, 3, 2, 1, 0), (1, 3, 1, 3, 0), (1, 3, 0, 1, 3), (1, 3, 1, 1, 0), (1, 3, 4, 0, 1),
+            (1, 3, 2, 1, 2), (0, 3, 0, 3, 1), (1, 3, 0, 3, 5), (1, 3, 0, 1, 0), (0, 3, 2, 0, 0), (1, 2, 4, 3),
+            (0, 3, 1, 3, 1), (1, 2, 2, 1), (1, 2, 4, 1), (1, 3, 1, 0, 0), (1, 2, 5, 1), (1, 3, 1, 1, 5),
+            (0, 3, 0, 0, 1), (1, 3, 2, 1, 3), (1, 3, 0, 0, 3), (0, 6, 1, 2), (1, 3, 1, 2, 2), (1, 3, 1, 0, 3),
+            (1, 3, 1, 0, 1), (0, 3, 0, 0, 0), (1, 3, 1, 2, 0), (0, 3, 2, 1, 0), (1, 3, 2, 1, 4), (1, 3, 1, 2, 3),
+            (1, 3, 1, 2, 1), (1, 3, 5, 0, 3), (1, 2, 3, 2), (1, 3, 0, 1, 2), (1, 3, 1, 3, 2), (0, 6, 4, 1),
+            (0, 6, 2, 3), (1, 3, 2, 3, 3), (1, 3, 2, 3, 1), (1, 3, 2, 3, 0), (1, 3, 0, 0, 5), (0, 0, 0, 0, 1, 1),
+            (0, 3, 1, 1, 0), (1, 3, 2, 3, 2), (1, 3, 4, 1, 2), (0, 6, 3, 1), (1, 3, 3, 1, 2), (1, 3, 2, 0, 4),
+            (1, 3, 5, 0, 2), (1, 2, 1, 2), (1, 2, 0, 2), (1, 3, 1, 3, 3), (0, 3, 0, 3, 0), (1, 3, 4, 1, 3),
+            (1, 3, 0, 3, 4), (1, 3, 4, 1, 0), (1, 3, 0, 0, 4), (1, 2, 2, 2), (1, 3, 1, 0, 2), (1, 3, 1, 3, 5),
+            (1, 2, 4, 2), (0, 6, 0, 2), (1, 3, 0, 2, 1), (1, 3, 0, 2, 0), (1, 3, 0, 2, 3), (0, 3, 0, 1, 0),
+            (1, 3, 2, 0, 5), (1, 3, 0, 1, 4), (0, 3, 1, 2, 1), (1, 3, 1, 2, 5), (1, 2, 5, 2), (1, 3, 0, 2, 2),
+            (0, 6, 2, 2), (1, 3, 2, 2, 1), (1, 2, 7, 1), (1, 2, 6, 1), (0, 0, 0, 0, 1, 2), (1, 1, 0, 0, 1, 2),
+            (1, 1, 0, 0, 1, 1), (1, 3, 2, 2, 3), (1, 3, 2, 2, 0), (0, 3, 0, 1, 1), (1, 3, 0, 1, 5), (0, 3, 0, 2, 1),
+            (0, 3, 0, 2, 0), (1, 3, 0, 2, 4), (1, 3, 0, 2, 5), (0, 3, 1, 3, 0), (1, 3, 1, 3, 4), (0, 0, 0, 0, 1, 3),
+            (0, 3, 2, 3, 1), (0, 3, 2, 2, 0), (1, 2, 7, 3), (1, 2, 6, 3), (0, 3, 1, 0, 0), (1, 3, 1, 0, 4),
+            (1, 3, 2, 2, 4), (0, 0, 0, 1, 1, 1), (1, 3, 2, 3, 5), (1, 1, 0, 1, 1, 1), (1, 3, 1, 1, 4),
+            (0, 3, 1, 0, 1), (1, 3, 1, 0, 5), (0, 3, 2, 2, 1), (1, 3, 2, 2, 5), (0, 3, 2, 3, 0), (1, 3, 2, 3, 4),
+            (0, 0, 0, 1, 1, 2), (1, 1, 0, 1, 1, 2), (1, 3, 1, 1, 2), (0, 3, 2, 1, 1), (1, 3, 2, 1, 5),
+            (1, 3, 2, 2, 2), (0, 3, 1, 2, 0), (1, 3, 1, 2, 4), (1, 3, 4, 0, 3), (1, 1, 0, 0, 1, 3), (1, 2, 7, 2),
+            (1, 2, 5, 3), (0, 6, 5, 1), (1, 3, 5, 1, 0), (1, 3, 5, 1, 1), (1, 3, 3, 1, 1), (0, 3, 4, 0, 1),
+            (1, 3, 4, 0, 5), (1, 3, 3, 0, 1), (0, 0, 0, 1, 1, 3), (1, 1, 0, 1, 1, 3), (0, 8, 0, 0), (0, 7, 0),
+        ),
+        (
+        ),
+        (
+        ),
+        (
+        ),
+        (
+            (0, 7, 1),
+        ),
+        (
+            (0, 7, 2),
+        ),
+        (
+        ),
+        (
+            (0, 6, 5, 3), (1, 3, 5, 3, 0), (1, 3, 5, 3, 1),
+        ),
+        (
+            (1, 3, 3, 1, 0), (0, 6, 3, 2), (0, 6, 4, 3), (1, 3, 4, 3, 2), (1, 3, 3, 2, 1), (1, 3, 4, 3, 0),
+            (1, 3, 4, 3, 3),
+        ),
+        (
+            (0, 3, 5, 0, 0), (1, 3, 5, 0, 4), (1, 3, 3, 0, 2), (1, 3, 5, 1, 2), (0, 5, 0, 0), (1, 4, 0, 0, 0, 2),
+            (0, 3, 5, 1, 0),
+        ),
+        (
+            (1, 4, 0, 0, 0, 3), (1, 3, 3, 2, 3), (0, 5, 0, 3), (1, 4, 0, 3, 0, 3), (1, 4, 0, 0, 0, 1),
+            (1, 3, 3, 2, 0), (1, 3, 3, 1, 3), (1, 3, 5, 3, 2), (0, 5, 0, 1), (0, 3, 4, 1, 0), (1, 3, 4, 1, 4),
+            (0, 3, 3, 2, 1), (1, 3, 3, 2, 5), (0, 6, 3, 3), (1, 3, 3, 3, 0), (1, 3, 3, 3, 3), (1, 4, 0, 1, 0, 3),
+            (1, 3, 3, 3, 2), (1, 4, 0, 1, 0, 2), (0, 6, 4, 2), (1, 3, 4, 2, 1), (0, 3, 4, 3, 0), (1, 3, 4, 3, 4),
+            (1, 3, 4, 2, 0), (1, 3, 4, 3, 1), (1, 3, 4, 1, 1), (1, 3, 4, 2, 3), (0, 3, 3, 0, 1), (0, 6, 5, 2),
+            (1, 3, 5, 2, 3), (0, 5, 0, 2), (1, 4, 0, 2, 0, 3), (1, 4, 0, 3, 0, 2), (1, 3, 3, 3, 1), (1, 3, 5, 2, 1),
+            (1, 3, 5, 0, 1), (1, 3, 5, 2, 0), (1, 4, 0, 1, 0, 1), (0, 3, 5, 3, 1), (1, 3, 5, 3, 5), (0, 3, 5, 1, 1),
+            (1, 3, 5, 1, 5), (1, 3, 5, 1, 3), (0, 3, 3, 1, 0), (1, 3, 3, 2, 2), (1, 4, 0, 2, 0, 2),
+            (0, 4, 0, 0, 1, 0),
+        ),
+        (
+            (1, 0, 1, 0, 0, 0), (0, 3, 4, 1, 1), (1, 3, 5, 3, 3), (0, 3, 5, 3, 0), (1, 3, 5, 3, 4), (0, 3, 4, 2, 0),
+            (1, 1, 1, 0, 0, 0), (1, 3, 4, 1, 5), (1, 3, 4, 0, 2), (1, 4, 0, 3, 0, 1), (0, 3, 5, 2, 0),
+            (1, 3, 4, 2, 4), (1, 3, 5, 2, 4), (0, 3, 3, 1, 1), (1, 3, 3, 1, 5), (1, 4, 0, 2, 0, 1),
             (0, 4, 0, 1, 1, 0),
         ),
         (
-            (1, 1, 1, 1, 0, 0), (1, 3, 4, 2, 4), (0, 3, 3, 3, 1), (1, 0, 1, 1, 0, 0), (1, 2, 6, 2),
-            (1, 1, 1, 0, 0, 0), (1, 3, 4, 3, 4), (1, 3, 4, 2, 5), (0, 3, 4, 3, 1), (1, 3, 4, 3, 5), (1, 3, 5, 3, 5),
-            (1, 3, 3, 3, 5), (1, 3, 4, 3, 3), (0, 3, 5, 2, 0), (1, 3, 5, 2, 4), (0, 3, 3, 2, 1), (0, 3, 5, 3, 0),
-            (1, 3, 3, 2, 5), (0, 4, 0, 2, 1, 0),
-        ),
-        (
-            (1, 3, 4, 1, 4), (1, 0, 1, 2, 0, 0), (0, 4, 0, 3, 1, 0), (1, 3, 4, 1, 3), (1, 3, 5, 3, 4),
-        ),
-        (
-            (1, 0, 1, 3, 0, 0), (1, 1, 1, 3, 0, 0), (1, 3, 3, 0, 5), (1, 1, 1, 0, 1, 1), (0, 0, 1, 1, 1, 1),
-            (1, 3, 5, 0, 4), (0, 0, 1, 1, 1, 2), (0, 0, 1, 0, 1, 2), (1, 1, 1, 1, 1, 2), (1, 1, 1, 0, 1, 2),
-            (0, 0, 1, 0, 1, 3), (1, 1, 1, 0, 1, 3), (0, 8, 1, 0), (0, 7, 3), (0, 7, 4),
-        ),
-        (
-            (0, 7, 5), (1, 1, 1, 1, 1, 1),
-        ),
-        (
-            (0, 0, 1, 1, 1, 3), (1, 1, 1, 1, 1, 3), (1, 1, 1, 2, 0, 0), (0, 5, 1, 0), (1, 4, 1, 0, 0, 2),
-            (1, 4, 1, 0, 0, 1), (0, 8, 1, 1),
-        ),
-        (
-        ),
-        (
-            (1, 4, 1, 0, 0, 3), (0, 0, 1, 2, 1, 3), (1, 1, 1, 2, 1, 3), (0, 0, 1, 2, 1, 2), (0, 0, 1, 3, 1, 1),
-            (1, 1, 1, 3, 1, 1), (1, 1, 1, 2, 1, 2), (0, 0, 1, 2, 1, 1), (1, 1, 1, 2, 1, 1), (0, 5, 1, 1),
-            (1, 4, 1, 1, 0, 2), (0, 0, 1, 3, 1, 2), (1, 1, 1, 3, 1, 2), (1, 4, 1, 1, 0, 3), (1, 4, 1, 1, 0, 1),
+            (1, 0, 1, 1, 0, 0), (1, 2, 6, 2), (1, 1, 1, 1, 0, 0), (1, 3, 5, 2, 2), (1, 3, 3, 0, 5), (0, 3, 4, 0, 0),
+            (1, 3, 4, 0, 4), (0, 3, 4, 3, 1), (0, 3, 3, 3, 0), (1, 3, 4, 3, 5), (0, 3, 4, 2, 1), (0, 4, 0, 2, 1, 0),
+        ),
+        (
+            (1, 0, 1, 2, 0, 0), (1, 3, 4, 2, 2), (0, 3, 5, 2, 1), (1, 3, 5, 2, 5), (0, 0, 1, 1, 1, 1),
+            (1, 1, 1, 1, 1, 1), (0, 3, 3, 2, 0), (1, 3, 4, 2, 5), (1, 3, 3, 1, 4), (0, 3, 3, 3, 1), (1, 3, 3, 3, 5),
+            (0, 4, 0, 3, 1, 0), (1, 3, 3, 3, 4),
+        ),
+        (
+            (1, 0, 1, 3, 0, 0), (1, 3, 3, 2, 4), (0, 3, 5, 0, 1), (1, 3, 5, 0, 5), (0, 0, 1, 0, 1, 2),
+            (1, 1, 1, 0, 1, 2), (1, 3, 5, 1, 4), (0, 0, 1, 0, 1, 1), (1, 1, 1, 0, 1, 1), (0, 0, 1, 0, 1, 3),
+            (1, 1, 1, 0, 1, 3), (0, 0, 1, 1, 1, 2), (1, 1, 1, 1, 1, 2), (0, 0, 1, 3, 1, 1), (1, 1, 1, 3, 1, 1),
+            (1, 1, 1, 3, 0, 0), (0, 8, 1, 0), (0, 7, 3), (0, 7, 4),
+        ),
+        (
+            (0, 7, 5),
+        ),
+        (
+            (0, 0, 1, 1, 1, 3), (1, 1, 1, 1, 1, 3), (1, 1, 1, 2, 0, 0), (0, 0, 1, 2, 1, 2), (1, 1, 1, 2, 1, 2),
+            (0, 5, 1, 0), (1, 4, 1, 0, 0, 2), (0, 8, 1, 1),
+        ),
+        (
+            (0, 0, 1, 2, 1, 1),
+        ),
+        (
+            (1, 4, 1, 0, 0, 3), (1, 1, 1, 2, 1, 1), (1, 4, 1, 0, 0, 1), (0, 0, 1, 2, 1, 3), (1, 1, 1, 2, 1, 3),
+            (0, 0, 1, 3, 1, 2), (1, 1, 1, 3, 1, 2), (0, 5, 1, 1), (1, 4, 1, 1, 0, 3), (1, 4, 1, 1, 0, 2),
             (0, 0, 1, 3, 1, 3), (1, 1, 1, 3, 1, 3), (0, 8, 1, 2),
         ),
         (
@@ -340,7 +348,7 @@
             (1, 4, 1, 3, 0, 2), (0, 4, 1, 0, 1, 0),
         ),
         (
-            (1, 4, 1, 2, 0, 1), (1, 4, 1, 3, 0, 1), (0, 4, 1, 1, 1, 0),
+            (1, 4, 1, 3, 0, 1), (1, 4, 1, 1, 0, 1), (1, 4, 1, 2, 0, 1), (0, 4, 1, 1, 1, 0),
         ),
         (
             (0, 4, 1, 2, 1, 0),
@@ -353,99 +361,103 @@
     ),
     (
         (
-            (1, 3, 4, 1, 0), (1, 2, 1, 2), (1, 2, 1, 0), (1, 2, 3, 0), (1, 3, 0, 1, 0), (1, 2, 3, 2), (1, 2, 2, 0),
-            (1, 3, 0, 1, 1), (1, 2, 0, 0), (1, 3, 1, 1, 0), (1, 3, 2, 1, 0), (1, 3, 1, 1, 1), (1, 2, 0, 2),
-            (1, 2, 4, 2),
-        ),
-        (
-            (1, 3, 4, 1, 1), (1, 3, 2, 1, 1), (1, 0, 0, 1, 0, 0), (0, 6, 1, 0), (1, 2, 4, 0), (0, 6, 1, 2),
-            (1, 3, 1, 2, 0), (1, 3, 1, 0, 3), (1, 2, 2, 2), (1, 3, 1, 1, 3), (0, 3, 4, 1, 0), (1, 1, 0, 1, 0, 0),
-            (1, 3, 3, 1, 0), (1, 0, 0, 1, 1, 0), (0, 6, 2, 2), (1, 3, 2, 2, 1), (1, 3, 2, 2, 3), (1, 0, 0, 0, 1, 0),
-            (1, 0, 0, 0, 0, 0), (1, 3, 2, 2, 2), (1, 3, 2, 2, 0), (1, 3, 1, 2, 1), (1, 3, 1, 0, 1), (0, 3, 0, 1, 1),
-            (1, 3, 0, 1, 5), (0, 6, 0, 2), (1, 3, 0, 2, 0), (1, 3, 0, 2, 2), (1, 3, 0, 1, 3), (1, 2, 3, 3),
-            (1, 3, 1, 0, 0), (1, 3, 3, 1, 1), (1, 3, 4, 1, 3), (0, 0, 0, 1, 0, 1), (1, 1, 0, 0, 0, 0),
-            (1, 3, 1, 2, 3), (1, 0, 0, 1, 0, 1), (1, 2, 7, 0), (0, 3, 2, 1, 1), (1, 3, 0, 2, 1), (1, 3, 1, 0, 2),
-            (1, 3, 4, 1, 4), (1, 1, 0, 1, 0, 1), (0, 0, 0, 0, 0, 1), (1, 0, 0, 0, 0, 1), (0, 3, 2, 1, 0),
-            (1, 3, 2, 1, 5), (0, 3, 1, 1, 1), (1, 3, 1, 1, 5), (0, 3, 2, 2, 0), (1, 2, 6, 0), (1, 3, 0, 1, 2),
-            (1, 2, 2, 3), (0, 3, 1, 2, 1), (1, 3, 0, 2, 3), (1, 3, 2, 2, 4), (1, 2, 5, 0), (0, 3, 1, 2, 0),
-            (0, 0, 0, 1, 1, 1), (1, 0, 0, 1, 1, 1), (0, 3, 1, 1, 0), (1, 3, 1, 1, 4), (0, 6, 0, 0), (1, 3, 0, 0, 0),
-            (0, 3, 1, 0, 0), (1, 3, 0, 0, 3), (0, 6, 1, 3), (1, 3, 1, 3, 1), (0, 6, 2, 0), (1, 3, 2, 0, 0),
-            (1, 3, 1, 2, 5), (1, 3, 1, 3, 0), (1, 3, 0, 0, 2), (0, 3, 2, 2, 1), (1, 3, 2, 2, 5), (0, 3, 0, 2, 0),
-            (1, 3, 0, 2, 4), (0, 3, 0, 1, 0), (0, 3, 3, 1, 1), (0, 3, 0, 2, 1), (1, 3, 1, 2, 4), (1, 3, 1, 2, 2),
-            (1, 3, 0, 1, 4), (1, 3, 1, 3, 2), (1, 1, 0, 0, 0, 1), (1, 2, 1, 3), (0, 3, 0, 0, 0), (1, 2, 0, 3),
-            (1, 3, 2, 0, 1), (1, 2, 4, 3), (0, 0, 0, 1, 1, 2), (1, 1, 0, 1, 1, 2), (0, 0, 0, 0, 1, 1),
-            (0, 0, 0, 0, 1, 2), (1, 3, 2, 1, 3), (1, 3, 3, 1, 2), (1, 1, 0, 0, 1, 2), (1, 1, 0, 0, 1, 1),
-            (1, 0, 0, 0, 1, 2), (1, 3, 0, 0, 1), (0, 3, 3, 1, 0), (1, 3, 0, 2, 5), (0, 3, 2, 0, 0), (0, 6, 0, 3),
-            (1, 3, 0, 3, 3), (0, 3, 1, 3, 0), (1, 0, 0, 1, 1, 2), (1, 3, 0, 3, 0), (1, 3, 0, 3, 1), (1, 3, 0, 3, 2),
-            (0, 3, 1, 0, 1), (1, 1, 0, 1, 1, 1), (0, 3, 0, 0, 1), (1, 3, 1, 0, 5), (1, 3, 1, 0, 4), (1, 2, 6, 2),
-            (0, 6, 2, 3), (1, 3, 2, 3, 0), (1, 3, 2, 1, 4), (0, 3, 4, 1, 1), (1, 3, 1, 1, 2), (1, 3, 1, 3, 3),
-            (1, 3, 2, 1, 2), (1, 3, 4, 1, 2), (0, 3, 2, 0, 1), (1, 3, 0, 0, 4), (1, 0, 0, 0, 1, 1), (1, 3, 2, 3, 1),
-            (1, 2, 5, 2), (0, 3, 0, 3, 0), (1, 3, 0, 0, 5), (1, 3, 0, 3, 4), (0, 8, 0, 0), (1, 2, 7, 3), (0, 6, 4, 0),
-            (0, 6, 3, 3), (1, 3, 4, 0, 0), (0, 3, 1, 3, 1), (1, 3, 1, 3, 5), (1, 3, 1, 3, 4), (1, 2, 5, 3),
-            (0, 3, 2, 3, 0), (1, 3, 5, 1, 0), (1, 3, 5, 1, 1), (0, 3, 0, 3, 1), (1, 3, 0, 3, 5), (1, 3, 4, 0, 2),
-            (1, 3, 2, 0, 5), (0, 6, 3, 0), (1, 3, 3, 0, 1), (1, 3, 2, 3, 2), (1, 3, 4, 1, 5), (0, 6, 4, 2),
-            (1, 3, 4, 2, 3), (1, 3, 4, 2, 1), (0, 3, 5, 1, 1), (0, 6, 5, 0), (1, 3, 5, 0, 1), (1, 3, 2, 0, 3),
-            (1, 3, 3, 1, 3), (0, 7, 0), (1, 3, 3, 0, 0), (1, 3, 2, 0, 2), (1, 3, 2, 0, 4), (0, 3, 2, 3, 1),
-            (1, 3, 2, 3, 5), (0, 7, 1), (1, 3, 2, 3, 3),
-        ),
-        (
-            (1, 3, 2, 3, 4),
-        ),
-        (
-            (0, 6, 3, 2), (1, 3, 3, 2, 0), (1, 2, 7, 2), (0, 3, 5, 1, 0), (1, 2, 6, 3),
-        ),
-        (
-        ),
-        (
-            (0, 7, 2),
-        ),
-        (
-        ),
-        (
-        ),
-        (
-            (1, 3, 3, 2, 1), (1, 3, 5, 1, 5), (0, 6, 5, 3), (1, 3, 5, 3, 1), (1, 3, 5, 0, 2), (0, 6, 5, 2),
-            (1, 3, 5, 2, 1), (1, 3, 3, 3, 0), (1, 3, 5, 3, 0), (1, 3, 5, 0, 0),
-        ),
-        (
-            (1, 3, 5, 2, 3), (0, 5, 0, 0), (0, 4, 0, 0, 0, 1), (1, 4, 0, 0, 0, 1), (1, 3, 3, 3, 3), (1, 3, 4, 2, 0),
-            (0, 3, 3, 0, 1), (0, 4, 0, 0, 0, 2), (1, 4, 0, 0, 0, 2), (1, 3, 3, 3, 1), (0, 5, 0, 3), (0, 3, 4, 0, 0),
-            (0, 4, 0, 3, 0, 2), (1, 4, 0, 3, 0, 2), (0, 4, 0, 0, 1, 0), (0, 4, 0, 0, 0, 0),
-        ),
-        (
-            (1, 0, 1, 0, 1, 0), (1, 0, 1, 0, 0, 0), (0, 3, 4, 2, 1), (1, 3, 5, 2, 0), (1, 3, 4, 0, 1), (0, 5, 0, 1),
-            (1, 3, 4, 0, 4), (1, 3, 3, 0, 3), (1, 3, 5, 3, 2), (0, 5, 0, 2), (0, 4, 0, 0, 1, 1), (1, 3, 3, 1, 4),
-            (1, 3, 3, 1, 5), (1, 4, 0, 0, 1, 1), (0, 4, 0, 1, 0, 2), (1, 4, 0, 1, 0, 2), (0, 3, 3, 0, 0),
-            (0, 4, 0, 1, 0, 1), (1, 4, 0, 1, 0, 1), (1, 3, 4, 2, 2), (0, 3, 3, 3, 1), (0, 4, 0, 2, 0, 2),
-            (1, 4, 0, 2, 0, 2), (0, 3, 5, 2, 0), (1, 3, 3, 2, 3), (0, 3, 3, 2, 1), (0, 4, 0, 1, 1, 1),
-            (1, 4, 0, 1, 1, 1), (1, 3, 3, 2, 5), (1, 3, 3, 0, 2), (1, 3, 5, 1, 3), (0, 4, 0, 3, 0, 1),
-            (1, 4, 0, 3, 0, 1), (0, 4, 0, 1, 1, 0), (0, 3, 4, 2, 0), (1, 3, 5, 3, 3), (0, 3, 5, 3, 1),
-            (1, 3, 5, 3, 5), (0, 4, 0, 1, 0, 0),
-        ),
-        (
-            (1, 0, 1, 1, 1, 0), (0, 3, 5, 2, 1), (1, 3, 5, 2, 5), (1, 0, 1, 1, 0, 0), (0, 4, 0, 2, 0, 1),
-            (1, 4, 0, 2, 0, 1), (0, 4, 0, 2, 1, 1), (1, 4, 0, 2, 1, 1), (1, 3, 4, 0, 3), (0, 4, 0, 3, 1, 1),
-            (1, 3, 3, 3, 2), (0, 0, 1, 0, 0, 1), (1, 0, 1, 0, 0, 1), (1, 4, 0, 3, 1, 1), (1, 3, 5, 1, 2),
-            (1, 3, 5, 2, 2), (1, 3, 4, 2, 5), (1, 3, 5, 0, 3), (0, 0, 1, 1, 1, 1), (1, 0, 1, 1, 1, 1),
-            (0, 3, 5, 0, 0), (1, 3, 5, 0, 4), (1, 3, 3, 0, 4), (0, 0, 1, 0, 1, 1), (1, 1, 1, 0, 1, 1),
-            (1, 0, 1, 0, 1, 1), (0, 4, 0, 2, 1, 0), (0, 4, 0, 2, 0, 0),
-        ),
-        (
-            (1, 3, 5, 1, 4), (0, 0, 1, 1, 0, 1), (1, 1, 1, 1, 0, 1), (1, 1, 1, 2, 0, 0), (1, 1, 1, 0, 0, 0),
-            (0, 0, 1, 0, 1, 2), (1, 1, 1, 0, 1, 2), (1, 0, 1, 0, 1, 2), (1, 1, 1, 1, 1, 1), (0, 3, 5, 3, 0),
-            (1, 3, 5, 3, 4), (1, 0, 1, 1, 0, 1), (1, 0, 1, 2, 0, 0), (0, 4, 0, 3, 1, 0), (0, 4, 0, 3, 0, 0),
-        ),
-        (
-            (1, 1, 1, 3, 0, 0), (1, 3, 4, 2, 4), (0, 3, 4, 0, 1), (0, 3, 3, 2, 0), (1, 3, 3, 0, 5),
-            (1, 0, 1, 3, 1, 0), (1, 3, 3, 3, 5), (1, 0, 1, 2, 1, 0), (0, 6, 4, 3), (1, 3, 4, 3, 0), (1, 3, 4, 3, 1),
-            (1, 3, 4, 3, 2), (1, 3, 4, 3, 3), (1, 3, 4, 0, 5), (0, 0, 1, 2, 0, 1), (1, 0, 1, 2, 0, 1),
-            (1, 3, 3, 2, 4), (1, 0, 1, 3, 0, 0), (0, 3, 3, 3, 0), (0, 0, 1, 1, 1, 2), (1, 0, 1, 1, 1, 2),
-            (0, 0, 1, 3, 0, 1), (1, 0, 1, 3, 0, 1), (0, 0, 1, 2, 1, 1), (1, 0, 1, 2, 1, 1), (1, 1, 1, 2, 1, 1),
-            (0, 3, 5, 0, 1), (1, 3, 3, 2, 2), (1, 3, 5, 0, 5), (1, 1, 1, 2, 0, 1), (1, 1, 1, 1, 0, 0),
-            (1, 1, 1, 3, 0, 1), (1, 3, 3, 3, 4), (1, 3, 5, 2, 4), (1, 1, 1, 1, 1, 2), (0, 0, 1, 2, 1, 2),
-            (1, 0, 1, 2, 1, 2), (1, 1, 1, 0, 0, 1), (1, 1, 1, 2, 1, 2), (0, 3, 4, 3, 0), (1, 3, 4, 3, 4),
-            (0, 0, 1, 3, 1, 1), (1, 0, 1, 3, 1, 1), (0, 3, 4, 3, 1), (1, 3, 4, 3, 5), (1, 1, 1, 3, 1, 1),
-            (0, 0, 1, 3, 1, 2), (1, 0, 1, 3, 1, 2), (1, 1, 1, 3, 1, 2), (0, 7, 4), (0, 7, 3), (0, 8, 1, 0),
+            (1, 3, 5, 1, 0), (1, 3, 5, 1, 1), (1, 3, 5, 1, 3), (1, 3, 1, 1, 0), (1, 3, 1, 1, 1), (1, 3, 2, 1, 0),
+            (1, 3, 2, 1, 3), (1, 3, 0, 1, 0), (1, 3, 0, 1, 3), (1, 3, 2, 1, 2), (1, 3, 5, 1, 2), (1, 3, 1, 1, 3),
+            (1, 2, 4, 2), (1, 2, 3, 0), (1, 2, 0, 0), (1, 3, 4, 1, 0), (1, 2, 2, 2), (1, 3, 2, 1, 1),
+        ),
+        (
+            (1, 2, 4, 0), (1, 2, 2, 0), (1, 0, 0, 1, 0, 0), (1, 3, 3, 1, 0), (0, 6, 2, 2), (1, 3, 2, 2, 2),
+            (1, 3, 2, 2, 1), (1, 3, 3, 1, 1), (1, 2, 0, 2), (1, 3, 0, 1, 2), (1, 2, 1, 0), (1, 2, 3, 2),
+            (1, 3, 2, 2, 3), (1, 2, 1, 2), (1, 3, 0, 1, 1), (1, 0, 0, 1, 1, 0), (0, 6, 1, 0), (1, 3, 1, 0, 2),
+            (1, 3, 1, 0, 0), (1, 0, 0, 0, 0, 0), (0, 3, 2, 1, 0), (1, 3, 2, 2, 0), (1, 3, 1, 1, 2),
+            (1, 0, 0, 0, 1, 0), (1, 2, 3, 3), (0, 3, 2, 1, 1), (0, 6, 0, 2), (1, 3, 0, 2, 3), (1, 3, 1, 0, 1),
+            (1, 3, 0, 2, 1), (1, 3, 0, 2, 2), (1, 3, 2, 1, 4), (1, 3, 0, 2, 0), (0, 0, 0, 0, 0, 1), (1, 2, 5, 0),
+            (0, 0, 0, 1, 0, 1), (1, 0, 0, 1, 0, 1), (1, 0, 0, 0, 0, 1), (0, 6, 1, 2), (1, 3, 1, 2, 2), (1, 2, 6, 0),
+            (0, 3, 0, 1, 1), (1, 3, 1, 2, 3), (0, 3, 4, 1, 0), (0, 3, 0, 1, 0), (0, 3, 5, 1, 1), (0, 3, 1, 0, 0),
+            (1, 3, 2, 1, 5), (1, 3, 0, 1, 5), (0, 0, 0, 1, 1, 1), (1, 0, 0, 1, 1, 1), (1, 1, 0, 1, 1, 1),
+            (0, 0, 0, 0, 1, 1), (0, 6, 0, 0), (1, 0, 0, 0, 1, 1), (1, 3, 0, 0, 2), (1, 3, 0, 0, 0), (1, 3, 4, 1, 1),
+            (0, 6, 2, 0), (0, 3, 0, 2, 1), (1, 3, 0, 2, 5), (0, 3, 2, 2, 0), (1, 3, 0, 0, 1), (1, 3, 2, 0, 0),
+            (1, 2, 0, 3), (1, 3, 2, 2, 4), (1, 2, 2, 3), (0, 3, 4, 1, 1), (0, 3, 0, 2, 0), (1, 3, 0, 2, 4),
+            (1, 2, 1, 3), (1, 3, 0, 1, 4), (1, 3, 1, 2, 1), (1, 3, 1, 2, 0), (1, 2, 4, 3), (0, 3, 0, 0, 1),
+            (0, 6, 1, 3), (1, 3, 1, 3, 1), (1, 3, 4, 1, 3), (1, 3, 4, 1, 2), (1, 3, 1, 3, 0), (1, 3, 1, 0, 4),
+            (1, 3, 1, 3, 3), (1, 3, 0, 0, 3), (0, 0, 0, 0, 1, 2), (1, 0, 0, 0, 1, 2), (1, 3, 1, 3, 2),
+            (0, 3, 1, 2, 0), (0, 6, 0, 3), (1, 3, 0, 3, 0), (1, 3, 0, 3, 3), (0, 0, 0, 1, 1, 2), (1, 3, 0, 3, 1),
+            (0, 3, 1, 0, 1), (1, 3, 1, 0, 5), (1, 1, 0, 1, 0, 0), (1, 2, 7, 0), (1, 0, 0, 1, 1, 2), (1, 3, 0, 3, 2),
+            (1, 3, 2, 0, 1), (1, 2, 5, 2), (0, 3, 0, 0, 0), (0, 6, 2, 3), (1, 3, 2, 3, 1), (1, 3, 2, 3, 0),
+            (1, 3, 2, 0, 3), (1, 2, 6, 2), (1, 2, 5, 3), (0, 3, 1, 1, 1), (1, 3, 1, 1, 5), (0, 3, 2, 2, 1),
+            (1, 3, 0, 0, 4), (1, 3, 2, 2, 5), (1, 3, 0, 0, 5), (0, 6, 3, 3), (0, 3, 0, 3, 1), (1, 3, 0, 3, 5),
+            (0, 6, 3, 0), (0, 6, 3, 2), (1, 3, 3, 3, 0), (1, 3, 5, 1, 5), (0, 3, 2, 3, 1), (0, 3, 2, 0, 1),
+            (1, 3, 2, 0, 5), (0, 3, 1, 3, 0), (1, 3, 2, 3, 3), (0, 3, 2, 3, 0), (1, 3, 2, 3, 4), (0, 3, 2, 0, 0),
+            (1, 3, 2, 0, 4), (1, 3, 1, 0, 3), (0, 3, 0, 3, 0), (1, 3, 0, 3, 4), (0, 3, 1, 2, 1), (0, 3, 1, 3, 1),
+            (1, 3, 1, 3, 5), (1, 3, 1, 2, 5), (0, 6, 5, 0), (1, 3, 1, 3, 4), (1, 3, 5, 0, 0), (1, 3, 2, 0, 2),
+            (1, 3, 1, 2, 4), (1, 1, 0, 1, 1, 2), (1, 3, 3, 0, 1), (1, 3, 2, 3, 2), (0, 3, 1, 1, 0), (1, 3, 1, 1, 4),
+            (1, 1, 0, 0, 0, 0), (1, 1, 0, 0, 1, 2), (1, 1, 0, 1, 0, 1), (1, 1, 0, 0, 1, 1), (1, 1, 0, 0, 0, 1),
+            (0, 8, 0, 0), (1, 3, 2, 3, 5), (1, 3, 3, 0, 2), (0, 7, 0), (0, 6, 4, 0), (1, 3, 4, 0, 2), (1, 3, 5, 0, 2),
+        ),
+        (
+        ),
+        (
+            (1, 2, 7, 2), (1, 2, 6, 3), (1, 3, 3, 2, 1), (1, 3, 4, 0, 3), (1, 3, 4, 0, 1), (1, 3, 4, 0, 0),
+            (0, 6, 4, 2),
+        ),
+        (
+            (1, 3, 4, 2, 1), (1, 3, 4, 2, 2), (0, 3, 3, 1, 1), (1, 3, 5, 0, 3), (0, 3, 5, 0, 0),
+        ),
+        (
+            (0, 6, 5, 3), (1, 3, 5, 3, 0), (1, 3, 5, 3, 2), (1, 3, 5, 3, 1), (0, 7, 1), (1, 3, 4, 2, 0),
+            (1, 3, 3, 3, 1),
+        ),
+        (
+        ),
+        (
+            (1, 3, 3, 2, 0), (0, 7, 2),
+        ),
+        (
+            (1, 2, 7, 3), (1, 3, 3, 0, 3), (1, 3, 5, 0, 1), (0, 6, 5, 2), (1, 3, 5, 2, 1),
+        ),
+        (
+        ),
+        (
+            (0, 4, 0, 0, 0, 1), (0, 5, 0, 0), (1, 4, 0, 0, 0, 1), (0, 5, 0, 1), (1, 3, 3, 0, 0),
+        ),
+        (
+            (0, 4, 0, 0, 0, 2), (1, 4, 0, 0, 0, 2), (1, 3, 5, 2, 2), (1, 3, 3, 3, 2), (0, 5, 0, 3), (0, 5, 0, 2),
+            (1, 3, 5, 2, 0), (1, 3, 5, 3, 3), (0, 4, 0, 3, 0, 2), (0, 3, 5, 3, 0), (1, 4, 0, 3, 0, 2),
+            (0, 4, 0, 0, 0, 0), (0, 4, 0, 0, 1, 0),
+        ),
+        (
+            (1, 0, 1, 0, 0, 0), (0, 4, 0, 0, 1, 1), (1, 4, 0, 0, 1, 1), (1, 0, 1, 0, 1, 0), (0, 4, 0, 1, 0, 2),
+            (1, 3, 3, 2, 2), (1, 4, 0, 1, 0, 2), (1, 3, 5, 3, 4), (0, 3, 3, 1, 0), (1, 3, 3, 1, 4), (0, 3, 3, 0, 0),
+            (0, 3, 4, 2, 0), (0, 3, 3, 0, 1), (0, 3, 5, 1, 0), (1, 3, 5, 2, 3), (0, 4, 0, 3, 1, 1), (0, 3, 4, 2, 1),
+            (0, 4, 0, 1, 0, 1), (1, 4, 0, 1, 0, 1), (1, 3, 5, 1, 4), (1, 4, 0, 3, 1, 1), (0, 4, 0, 2, 0, 2),
+            (1, 4, 0, 2, 0, 2), (1, 3, 4, 1, 5), (1, 3, 4, 2, 3), (0, 4, 0, 3, 0, 1), (1, 4, 0, 3, 0, 1),
+            (0, 4, 0, 1, 1, 1), (1, 4, 0, 1, 1, 1), (0, 4, 0, 1, 1, 0), (0, 3, 3, 3, 0), (0, 4, 0, 1, 0, 0),
+        ),
+        (
+            (1, 0, 1, 1, 0, 0), (1, 0, 1, 1, 1, 0), (0, 3, 5, 2, 0), (1, 3, 3, 2, 3), (0, 3, 3, 3, 1),
+            (0, 3, 5, 2, 1), (1, 3, 5, 2, 5), (1, 3, 4, 2, 5), (1, 3, 4, 1, 4), (0, 4, 0, 2, 0, 1),
+            (1, 4, 0, 2, 0, 1), (1, 3, 4, 2, 4), (0, 3, 3, 2, 1), (1, 3, 3, 2, 5), (0, 4, 0, 2, 1, 1),
+            (1, 4, 0, 2, 1, 1), (1, 3, 3, 3, 5), (0, 3, 3, 2, 0), (1, 3, 5, 2, 4), (0, 0, 1, 0, 0, 1),
+            (1, 0, 1, 0, 0, 1), (1, 3, 3, 2, 4), (1, 3, 3, 1, 5), (1, 3, 3, 3, 4), (0, 0, 1, 0, 1, 1),
+            (1, 0, 1, 0, 1, 1), (0, 0, 1, 1, 1, 1), (1, 0, 1, 1, 1, 1), (1, 1, 1, 0, 1, 1), (1, 3, 5, 0, 4),
+            (0, 4, 0, 2, 1, 0), (1, 3, 3, 0, 5), (0, 3, 5, 3, 1), (1, 3, 5, 3, 5), (0, 3, 4, 0, 0), (1, 3, 4, 0, 4),
+            (1, 1, 1, 0, 0, 0), (0, 4, 0, 2, 0, 0),
+        ),
+        (
+            (1, 0, 1, 2, 1, 0), (1, 1, 1, 2, 0, 0), (0, 0, 1, 1, 0, 1), (1, 0, 1, 1, 0, 1), (0, 0, 1, 0, 1, 2),
+            (1, 0, 1, 0, 1, 2), (1, 1, 1, 0, 0, 1), (1, 1, 1, 1, 0, 1), (0, 4, 0, 3, 0, 0), (0, 4, 0, 3, 1, 0),
+        ),
+        (
+            (1, 1, 1, 1, 1, 1), (1, 0, 1, 2, 0, 0), (1, 3, 3, 0, 4), (1, 0, 1, 3, 0, 0), (1, 0, 1, 3, 1, 0),
+            (0, 6, 4, 3), (1, 3, 4, 3, 1), (1, 3, 4, 3, 0), (1, 1, 1, 3, 0, 0), (1, 3, 3, 1, 2), (1, 3, 4, 3, 2),
+            (1, 3, 3, 1, 3), (0, 3, 4, 0, 1), (1, 3, 4, 0, 5), (0, 0, 1, 2, 0, 1), (1, 1, 1, 2, 0, 1),
+            (1, 0, 1, 2, 0, 1), (0, 0, 1, 1, 1, 2), (1, 0, 1, 1, 1, 2), (1, 3, 3, 3, 3), (0, 0, 1, 3, 0, 1),
+            (1, 1, 1, 3, 0, 1), (1, 0, 1, 3, 0, 1), (0, 0, 1, 2, 1, 1), (1, 0, 1, 2, 1, 1), (1, 1, 1, 2, 1, 1),
+            (1, 3, 4, 3, 3), (0, 3, 4, 3, 0), (1, 3, 4, 3, 4), (1, 1, 1, 1, 0, 0), (0, 0, 1, 3, 1, 1),
+            (1, 0, 1, 3, 1, 1), (0, 3, 4, 3, 1), (1, 3, 4, 3, 5), (0, 3, 5, 0, 1), (1, 3, 5, 0, 5),
+            (1, 1, 1, 1, 1, 2), (1, 1, 1, 3, 1, 1), (0, 0, 1, 2, 1, 2), (1, 1, 1, 2, 1, 2), (1, 0, 1, 2, 1, 2),
+            (0, 0, 1, 3, 1, 2), (1, 1, 1, 3, 1, 2), (1, 0, 1, 3, 1, 2), (0, 7, 3), (1, 1, 1, 0, 1, 2), (0, 8, 1, 0),
+            (0, 7, 4),
         ),
         (
             (0, 7, 5),
@@ -454,32 +466,33 @@
             (0, 8, 1, 1),
         ),
         (
-            (0, 5, 1, 0), (0, 4, 1, 0, 0, 2), (0, 8, 1, 2), (1, 4, 1, 0, 0, 2), (0, 4, 1, 0, 0, 1),
-            (1, 4, 1, 0, 0, 1),
-        ),
-        (
-        ),
-        (
-        ),
-        (
-            (0, 5, 1, 1), (0, 4, 1, 1, 0, 1), (1, 4, 1, 1, 0, 1), (0, 8, 1, 3), (0, 4, 1, 0, 0, 0),
-        ),
-        (
-            (0, 4, 1, 1, 0, 2), (0, 4, 1, 0, 1, 1), (1, 4, 1, 0, 1, 1), (1, 4, 1, 1, 0, 2), (0, 5, 1, 2),
-        ),
-        (
-            (0, 4, 1, 2, 0, 2), (1, 4, 1, 2, 0, 2), (0, 5, 1, 3), (0, 4, 1, 3, 0, 2), (1, 4, 1, 3, 0, 2),
-            (0, 4, 1, 1, 1, 1), (1, 4, 1, 1, 1, 1), (0, 4, 1, 2, 0, 1), (1, 4, 1, 2, 0, 1), (0, 4, 1, 2, 1, 1),
-            (1, 4, 1, 2, 1, 1), (0, 4, 1, 3, 0, 1), (1, 4, 1, 3, 0, 1), (0, 4, 1, 0, 1, 0),
-        ),
-        (
-            (0, 4, 1, 3, 1, 1), (1, 4, 1, 3, 1, 1), (0, 4, 1, 1, 0, 0), (0, 4, 1, 3, 0, 0), (0, 4, 1, 1, 1, 0),
+            (0, 5, 1, 0), (0, 4, 1, 0, 0, 1), (0, 4, 1, 0, 0, 2), (1, 4, 1, 0, 0, 2),
+        ),
+        (
+            (1, 4, 1, 0, 0, 1), (0, 8, 1, 2),
+        ),
+        (
+        ),
+        (
+            (0, 5, 1, 1), (0, 4, 1, 1, 0, 2), (1, 4, 1, 1, 0, 2), (0, 8, 1, 3),
+        ),
+        (
+            (0, 4, 1, 0, 1, 1), (1, 4, 1, 0, 1, 1), (0, 4, 1, 1, 0, 1), (1, 4, 1, 1, 0, 1),
+        ),
+        (
+            (0, 4, 1, 2, 0, 2), (0, 5, 1, 2), (1, 4, 1, 2, 0, 2), (0, 4, 1, 1, 1, 1), (1, 4, 1, 1, 1, 1),
+            (0, 5, 1, 3), (0, 4, 1, 3, 0, 2), (1, 4, 1, 3, 0, 2), (0, 4, 1, 2, 0, 1), (1, 4, 1, 2, 0, 1),
+            (0, 4, 1, 0, 0, 0), (0, 4, 1, 2, 1, 1), (1, 4, 1, 2, 1, 1), (0, 4, 1, 1, 1, 0), (0, 4, 1, 3, 1, 1),
+            (1, 4, 1, 3, 1, 1), (0, 4, 1, 3, 0, 1), (1, 4, 1, 3, 0, 1), (0, 4, 1, 0, 1, 0),
+        ),
+        (
+            (0, 4, 1, 1, 0, 0),
         ),
         (
             (0, 4, 1, 2, 1, 0), (0, 4, 1, 2, 0, 0),
         ),
         (
-            (0, 4, 1, 3, 1, 0),
+            (0, 4, 1, 3, 0, 0), (0, 4, 1, 3, 1, 0),
         ),
         (
         ),
@@ -530,6 +543,7 @@
     nt,
     nm,
     qkvg,
+    held_kept,
     hid,
     gated,
     part1,
@@ -784,8 +798,23 @@
     def project(at):
         span = rows(at, chunk)
         qkvg[span, :] = jnp.dot(
-            nt[span, :], w1[...], preferred_element_type=jnp.float32
+            nt[span, :], w1[:, pl.ds(0, 2 * cq + cv)], preferred_element_type=jnp.float32
         ).astype(jnp.bfloat16)
+
+    def gate(at):
+        span = rows(at, chunk)
+        gates = jnp.dot(
+            nt[span, :], w1[:, pl.ds(2 * cq + cv, cv)], preferred_element_type=jnp.float32
+        ).astype(jnp.bfloat16).astype(jnp.float32)
+        whole = (held_kept[span, :] * mixer_gain[:, lanes(z, cv)] * silu(gates)).astype(jnp.bfloat16)
+        for i in range(chunk // length):
+            for c in range(CHUNKS):
+                first = i * length + c * span_c
+                hid[rows(at * (chunk // length) + i + c * groups, span_c), :] = whole[first : first + span_c]
+
+    def two_parts(x):
+        high = x.astype(jnp.bfloat16)
+        return high, (x - high.astype(jnp.float32)).astype(jnp.bfloat16)
 
     def retain(first):
         log_gamma = gammas[pl.ds(head, 1), :]
@@ -798,25 +827,28 @@
         @pl.loop(first * groups // 2, (first + 1) * groups // 2)
         def _(at):
             span = rows(at, length)
-            held = qkvg[span, :].astype(jnp.float32)
+            held = qkvg[span, pl.ds(0, 2 * cq)].astype(jnp.float32)
 
             def turn(x):
                 return x * cos_t[...] + pltpu.roll(x, cq // 2, 1) * sin_t[...]
 
             rq = turn(held[:, :cq])
             rk = turn(held[:, cq : 2 * cq])
+            q_high, q_low = two_parts(rq)
+            k_high, k_low = two_parts(rk)
             scores = lax.dot_general(
-                rq, rk, (((1,), (1,)), ((), ())), precision=highest, preferred_element_type=jnp.float32
+                jnp.concatenate([q_high, q_high, q_low], axis=1),
+                jnp.concatenate([k_high, k_low, k_high], axis=1),
+                (((1,), (1,)), ((), ())), preferred_element_type=jnp.float32,
             ) * decay
+            s_high, s_low = two_parts(scores)
+            v_exact = qkvg[span, pl.ds(2 * cq, cv)]
             kept = jnp.dot(
-                scores, held[:, 2 * cq : 2 * cq + cv], precision=highest,
-                preferred_element_type=jnp.float32,
+                jnp.concatenate([s_high, s_low], axis=1),
+                jnp.concatenate([v_exact, v_exact], axis=0), preferred_element_type=jnp.float32,
             )
             kept = kept * lax.rsqrt(jnp.mean(kept * kept, axis=-1, keepdims=True) + 1e-06)
-            gain = mixer_gain[:, lanes(z, cv)]
-            whole = (kept * gain * silu(held[:, 2 * cq + cv :])).astype(jnp.bfloat16)
-            for c in range(CHUNKS):
-                hid[rows(at + c * groups, span_c), :] = whole[c * span_c : (c + 1) * span_c]
+            held_kept[span, :] = kept
 
     def renorm(c):
         middle = (
@@ -866,6 +898,7 @@
         lambda c: multiply(gated, wdown, 1, c),
         finish,
         prepare,
+        gate,
     )
     perform(0)
     for stage, (name, index) in enumerate(STAGES):
@@ -943,7 +976,8 @@
             pltpu.VMEM((cf, width), bf),
             pltpu.VMEM((groups * length, width), bf),
             pltpu.VMEM((groups * length, width), bf),
-            pltpu.VMEM((groups * length, 2 * cq + 2 * cv), bf),
+            pltpu.VMEM((groups * length, 2 * cq + cv), bf),
+            pltpu.VMEM((groups * length, cv), f32),
             pltpu.VMEM((groups * length, cv), bf),
             pltpu.VMEM((groups * length, cf), bf),
             pltpu.VMEM((CHUNKS, 2, groups, few, width), bf),

time: 117 us -> 113 us (0.966)
  Pallas kernels: 114 us -> 111 us
    pallas_call x1, Pallas kernels: 114 us -> 111 us  [body(): pl.pallas_call(functools.partial(layer_kernel, n_fs, groups), out_shape=j...]
where the time goes in v4:
time: 113 us; the launch traced here: 112 us
  Pallas kernels  111 us (98%)
  local copies, waits for them, and re-layouts  1.88 us (2%)
    pallas_call x1, Pallas kernels, body(): pl.pallas_call(functools.partial(layer_kernel, n_fs, groups), out_shape=j...  111 us

profile of v4, /device:TPU:0, one launch (start us, length us, event | category | flops | bytes accessed | tf_op | source)
XLA Modules:
  0.0 112.4 jit_solution(5155425839882397955)
XLA Ops:
  0.0 110.5 %shard_map.163 = bf16[128,2048]{1,0:T(8,128)(2,1)} custom-call(bf16[128,2048]{1,0:T(8,128)(2,1)} %tokens_in.1, f32[1,2048]{1,0:T(1,128)} %bitcast.3, bf16[128,512]{1,0:T(8,128)(2,1)} %wq.1, bf16[128,512]{1,0:T(8,128)(2,1)} %wk.1, bf16[128,1024]{1,0:T(8,128)(2,1)} %wv.1, bf16[128,1024]{1,0:T(8,128)(2,1)} %wg.1, f32[1,1024]{1,0:T(1,128)} %bitcast.5, ...), custom_call_target="tpu_custom_call" | custom-call | tf_op jit(solution)/shard_map/pallas_call | solution.py:958
  110.5 1.9 %copy.19 = bf16[128,2048]{1,0:T(8,128)(2,1)} copy(bf16[128,2048]{1,0:T(8,128)(2,1)} %shard_map.163) | data formatting | bytes 1048576

commit v5 on v4

--- a/solution.py
+++ b/solution.py
@@ -694,13 +694,13 @@
         return part[which][c, tp, g].astype(jnp.float32) + xb[which][c, g].astype(jnp.float32)
 
     def exchange(which, c):
-        return remote(part[which].at[c, other], xb[which].at[c], x_send.at[which], x_recv.at[which, c], partner)
+        return remote(part[which].at[c, other], xb[which].at[c], x_send.at[which], x_recv.at[c], partner)
 
     def gather_copy(me, key, c, side, d, landing=False):
         move = 1 - 2 * side
         source = real(me - move * d)
         ref = block(key, c, source, tp)
-        at = c + key * NT_PARTS
+        at = c
         device = partner if landing else zdev(real(me + move))
         return remote(ref, ref, a_send.at[key], a_recv.at[at, source], device)
 
@@ -726,7 +726,7 @@
         ref = sb[which].at[c, flip(side), d]
         at = d if landing else d - 1
         device = partner if landing else zdev(real(me + 1 - 2 * side))
-        return remote(ref, rb[which].at[c, flip(side), at], r_send.at[which], r_recv.at[which, c, flip(side), at], device)
+        return remote(ref, rb[which].at[c, flip(side), at], r_send.at[which], r_recv.at[c, flip(side), at], device)
 
     makers = (gather_copy, core_copy, weight_copy, hop_copy, sum_copy)
 
@@ -999,13 +999,13 @@
             dma((classes, groups, 2)),
             dma((classes,)),
             dma((2,)),
-            dma((NT_PARTS + CHUNKS, groups)),
+            dma((max(NT_PARTS, CHUNKS), groups)),
             dma((2,)),
             dma((1 + CHUNKS,)),
             dma((2,)),
-            dma((2, CHUNKS)),
+            dma((CHUNKS,)),
             dma((2,)),
-            dma((2, CHUNKS, 2, groups - 1)),
+            dma((CHUNKS, 2, groups - 1)),
             dma((1,)),
             dma((1,)),
             dma((9,)),

time: 113 us -> 112 us (level)
  no operation moved by 1% of the time
where the time goes in v5:
time: 112 us
  Pallas kernels  110 us (98%)
  local copies, waits for them, and re-layouts  1.88 us (2%)
    pallas_call x1, Pallas kernels, body(): pl.pallas_call(functools.partial(layer_kernel, n_fs, groups), out_shape=j...  110 us

profile of v5, /device:TPU:0, one launch (start us, length us, event | category | flops | bytes accessed | tf_op | source)
XLA Modules:
  0.0 112.1 jit_solution(3665349383454138609)
XLA Ops:
  0.0 110.2 %shard_map.163 = bf16[128,2048]{1,0:T(8,128)(2,1)} custom-call(bf16[128,2048]{1,0:T(8,128)(2,1)} %tokens_in.1, f32[1,2048]{1,0:T(1,128)} %bitcast.3, bf16[128,512]{1,0:T(8,128)(2,1)} %wq.1, bf16[128,512]{1,0:T(8,128)(2,1)} %wk.1, bf16[128,1024]{1,0:T(8,128)(2,1)} %wv.1, bf16[128,1024]{1,0:T(8,128)(2,1)} %wg.1, f32[1,1024]{1,0:T(1,128)} %bitcast.5, ...), custom_call_target="tpu_custom_call" | custom-call | tf_op jit(solution)/shard_map/pallas_call | solution.py:958
  110.2 1.9 %copy.19 = bf16[128,2048]{1,0:T(8,128)(2,1)} copy(bf16[128,2048]{1,0:T(8,128)(2,1)} %shard_map.163) | data formatting | bytes 1048576
